TPU v7x, 128 devices: a whole 4x4x4 slice. The times are simulated.
128 devices in a mesh: sp: 64 (over z, y, x), tp: 2 (over core).
Axes of the slice: x: 4, y: 4, z: 4, core: 2. Of those that a mesh axis runs over, the one named last changes fastest.
Arguments:
- stream: bfloat16 [16384, 2048], P(('sp', 'tp')), may hold values from -6 to 6
- head_input_signal: bfloat16 [16384, 2048], P('sp', 'tp'), may hold values from -6 to 6
- write_input_vectors: bfloat16 [16384, 512], P('sp', 'tp'), may hold values from -6 to 6
- read_input_vectors: bfloat16 [16384, 512], P('sp', 'tp'), may hold values from -6 to 6
- output_gate_input: bfloat16 [16384, 2048], P('sp', 'tp'), may hold values from -6 to 6
- step_size_input: bfloat16 [16384, 32], P('sp', 'tp'), may hold values from -5 to 5.5
- position_log_decay: float32 [16384, 32], P('sp', 'tp'), may hold values from -0.7 to 0
- signal_filter_taps: bfloat16 [4, 2048], P(None, 'tp'), may hold values from -3 to 3
- write_filter_taps: bfloat16 [4, 512], P(None, 'tp'), may hold values from -3 to 3
- read_filter_taps: bfloat16 [4, 512], P(None, 'tp'), may hold values from -3 to 3
- step_size_bias: float32 [32], P('tp'), may hold values from -1 to 1
- head_decay_rate: float32 [32], P('tp'), may hold values from 6.1035156e-07 to 0.03
- head_direct_term: float32 [32], P('tp'), may hold values from 0.5 to 2
- grouped_norm_gain: float32 [2048], P('tp'), may hold values from 0.1 to 1.9
- mixer_output_weight: bfloat16 [2048, 2048], P('tp'), may hold values from -0.125 to 0.125
- expert_norm_gain: float32 [2048], replicated, may hold values from 0.1 to 1.9
- chosen_expert_index: int32 [16384, 4], P(('sp', 'tp')), may hold values from 0 to 127, all different within a row; in each aligned block of 128 rows (0 to 127, 128 to 255, ...) at most 6 rows name the same one
- chosen_expert_weight: float32 [16384, 4], P(('sp', 'tp')), may hold values from 0.1 to 1
- routed_gate_weight: bfloat16 [128, 2048, 512], P(('sp', 'tp')), may hold values from -0.125 to 0.125
- routed_up_weight: bfloat16 [128, 2048, 512], P(('sp', 'tp')), may hold values from -0.125 to 0.125
- routed_down_weight: bfloat16 [128, 512, 2048], P(('sp', 'tp')), may hold values from -0.25 to 0.25
- common_gate_weight: bfloat16 [2048, 512], replicated, may hold values from -0.125 to 0.125
- common_up_weight: bfloat16 [2048, 512], replicated, may hold values from -0.125 to 0.125
- common_down_weight: bfloat16 [512, 2048], replicated, may hold values from -0.25 to 0.25
Outputs:
- layer_out: bfloat16 [16384, 2048], P(('sp', 'tp'))
Inputs may be any that keep to these rules, and one draw needn't show every extreme that they name: `chosen_expert_index`: each row names 4 different experts. Among the 128 rows of one device (aligned blocks of 128 rows) no expert is named more than 6 times; in some block one expert is named exactly 6 times.
All inputs are finite; a program needn't handle non-finite values.
Results may differ from a plain program's by a relative error of at most 0.015.
Values may be sent and summed in bfloat16 or wider, within the bound.
No kernel may reach another device: no remote copies, remote signals or barrier semaphores. Data moves between devices by JAX's collectives and lax.ppermute only.
A program may use at most 128 MiB of HBM per device.

v0:
```python
import jax
import jax.numpy as jnp
from jax import lax
from jax.sharding import Mesh
from jax.sharding import PartitionSpec as P

HEAD_DIM = 64
STATE = 128
BLK = 128
SP = ("sp_0", "sp_1", "sp_2")
SP_TP = ("sp_0", "sp_1", "sp_2", "tp")


def from_behind(block, axis, distance):
    devices = range(lax.axis_size(axis))
    route = [(i - distance, i) for i in devices if i - distance in devices]
    return lax.ppermute(block, axis, route)


def nothing_yet(value, identity):
    return jax.tree.map(
        lambda a, e: jnp.broadcast_to(jnp.asarray(e, a.dtype), a.shape), value, identity
    )


def carried_in(value, axes, combine, identity):
    before = start = nothing_yet(value, identity)
    subtotal = value
    for axis in reversed(axes):
        count, index = (lax.axis_size(axis), lax.axis_index(axis))
        pieces = jax.tree.map(lambda part: lax.all_gather(part, axis), subtotal)
        inside, subtotal = (start, start)
        for k in range(count):
            passed = k < index
            subtotal = combine(subtotal, jax.tree.map(lambda part: part[k], pieces))
            inside = jax.tree.map(lambda new, old: jnp.where(passed, new, old), subtotal, inside)
        before = combine(inside, before)
    return before


def in_blocks(value, dim, count):
    lengths = value.shape
    tiles = value.reshape(*lengths[:dim], count, lengths[dim] // count, *lengths[dim + 1 :])
    return jnp.moveaxis(tiles, dim, 0)


def sent_and_summed(value, axis, dim):
    tiles = in_blocks(value, dim, lax.axis_size(axis))
    arrived = lax.all_to_all(tiles, axis, split_axis=0, concat_axis=0, tiled=True)
    return arrived.astype(jnp.float32).sum(axis=0)


def causal_conv(previous, current, weight):
    stacked = jnp.concatenate([previous, current], axis=0).astype(jnp.float32)
    weight = weight.astype(jnp.float32)
    kernel_len = weight.shape[0]
    length = current.shape[0]
    summed_taps = weight[0] * stacked[0:length]
    for offset in range(1, kernel_len):
        summed_taps = summed_taps + weight[offset] * stacked[offset : offset + length]
    return jax.nn.silu(summed_taps)


def combine(earlier, latter):
    return (earlier[0] * latter[0], earlier[1] * latter[0][..., None, None] + latter[1])


def advance(carry_state, inputs):
    block_piece, decay_factor = inputs
    return (carry_state * decay_factor[..., None, None] + block_piece, carry_state)


def on_device(
    stream,
    head_input_signal,
    write_input_vectors,
    read_input_vectors,
    output_gate_input,
    step_size_input,
    position_log_decay,
    signal_filter_taps,
    write_filter_taps,
    read_filter_taps,
    step_size_bias,
    head_decay_rate,
    head_direct_term,
    grouped_norm_gain,
    mixer_output_weight,
    expert_norm_gain,
    chosen_expert_index,
    chosen_expert_weight,
    routed_gate_weight,
    routed_up_weight,
    routed_down_weight,
    common_gate_weight,
    common_up_weight,
    common_down_weight,
):
    length = head_input_signal.shape[0]
    margin = signal_filter_taps.shape[0] - 1
    head_count = step_size_input.shape[1]
    groups = write_input_vectors.shape[1] // STATE
    per_group = head_count // groups
    blocks = length // BLK
    rim_rows = (
        head_input_signal[length - margin :],
        write_input_vectors[length - margin :],
        read_input_vectors[length - margin :],
    )
    before = from_behind((rim_rows[0], rim_rows[1], rim_rows[2]), SP, 1)
    signal = causal_conv(before[0], head_input_signal, signal_filter_taps)
    write_vec = causal_conv(before[1], write_input_vectors, write_filter_taps)
    read_vec = causal_conv(before[2], read_input_vectors, read_filter_taps)
    time_position = jax.nn.softplus(step_size_input.astype(jnp.float32) + step_size_bias)
    decay_logarithm = position_log_decay - head_decay_rate * time_position
    signal_heads = signal.reshape(blocks, BLK, groups, per_group, HEAD_DIM)
    scaled_blocks = signal_heads * time_position.reshape(blocks, BLK, groups, per_group)[..., None]
    write_blocks = write_vec.reshape(blocks, BLK, groups, STATE)
    read_blocks = read_vec.reshape(blocks, BLK, groups, STATE)
    within_cum = jnp.cumsum(decay_logarithm.reshape(blocks, BLK, groups, per_group), axis=1)
    block_total = within_cum[:, -1]
    running = jnp.cumsum(block_total, axis=0)
    device_total = running[-1]
    causal = jnp.arange(BLK)[:, None] >= jnp.arange(BLK)[None, :]
    cum_heads = jnp.transpose(within_cum, (0, 2, 3, 1))
    differences = cum_heads[..., :, None] - cum_heads[..., None, :]
    decay_matrix = jnp.exp(jnp.where(causal, differences, -jnp.inf))
    intersection = jnp.einsum("btgn,bsgn->bgts", read_blocks, write_blocks)
    intra_out = jnp.einsum("bgts,bgets,bsgep->btgep", intersection, decay_matrix, scaled_blocks)
    tail_decay = jnp.exp(block_total[:, None] - within_cum)
    block_states = jnp.einsum("bsgn,bsge,bsgep->bgepn", write_blocks, tail_decay, scaled_blocks)
    device_state = jnp.einsum(
        "bgepn,bge->gepn", block_states, jnp.exp(device_total[None] - running)
    )
    identity = (jnp.ones_like(device_total), jnp.zeros_like(device_state))
    incoming = carried_in((jnp.exp(device_total), device_state), SP, combine, identity)[1]
    readout_scale = jnp.exp(within_cum)
    start_states = lax.scan(
        advance, jnp.zeros_like(device_state), (block_states, jnp.exp(block_total))
    )[1]
    near_out = jnp.einsum("btgn,bgepn,btge->btgep", read_blocks, start_states, readout_scale)
    device_scale = jnp.exp(within_cum + (running - block_total)[:, None])
    far_out = jnp.einsum("btgn,gepn,btge->btgep", read_blocks, incoming, device_scale)
    ssd_out = intra_out + near_out + far_out
    ssd_out = ssd_out + head_direct_term.reshape(groups, per_group)[:, :, None] * signal_heads
    gated = ssd_out.reshape(length, groups, per_group * HEAD_DIM) * jax.nn.silu(
        output_gate_input.astype(jnp.float32)
    ).reshape(length, groups, per_group * HEAD_DIM)
    norm_scale = lax.rsqrt(jnp.mean(gated * gated, axis=-1, keepdims=True) + 1e-06)
    mixer_out = ((gated * norm_scale).reshape(length, -1) * grouped_norm_gain).astype(jnp.bfloat16)
    row_count = stream.shape[0]
    summed = sent_and_summed(
        jnp.dot(mixer_out, mixer_output_weight, preferred_element_type=jnp.float32).astype(
            jnp.bfloat16
        ),
        "tp",
        0,
    )
    residual = (stream.astype(jnp.float32) + summed).astype(jnp.bfloat16)
    widened = residual.astype(jnp.float32)
    normed = (
        widened
        * lax.rsqrt(jnp.mean(widened * widened, axis=-1, keepdims=True) + 1e-06)
        * expert_norm_gain
    ).astype(jnp.bfloat16)
    shared_hidden = (
        jax.nn.silu(jnp.dot(normed, common_gate_weight, preferred_element_type=jnp.float32))
        * jnp.dot(normed, common_up_weight, preferred_element_type=jnp.float32)
    ).astype(jnp.bfloat16)
    shared = jnp.dot(shared_hidden, common_down_weight, preferred_element_type=jnp.float32)
    sp_count = lax.axis_size(SP)
    tp_count = lax.axis_size("tp")
    experts = sp_count * tp_count
    fanout = chosen_expert_index.shape[1]
    capacity = max(2, (3 * row_count * fanout + 2 * experts - 1) // (2 * experts))
    chosen = chosen_expert_index.reshape(-1)
    one_hot = (chosen[:, None] == jnp.arange(experts, dtype=jnp.int32)[None, :]).astype(jnp.int32)
    slot_index = jnp.sum((jnp.cumsum(one_hot, axis=0) - one_hot) * one_hot, axis=1)
    position = chosen * capacity + slot_index
    source_row = jnp.arange(row_count * fanout, dtype=jnp.int32) // fanout
    slot_table = jnp.full((experts * capacity,), row_count, jnp.int32).at[position].set(source_row)
    padded = jnp.concatenate([normed, jnp.zeros((1, normed.shape[1]), jnp.bfloat16)], axis=0)
    outgoing = padded[slot_table].reshape(experts, capacity, -1)
    arrived = lax.all_to_all(outgoing, SP_TP, split_axis=0, concat_axis=0, tiled=True)
    flat_rows = arrived.reshape(-1, arrived.shape[-1])
    hidden = (
        jax.nn.silu(jnp.dot(flat_rows, routed_gate_weight[0], preferred_element_type=jnp.float32))
        * jnp.dot(flat_rows, routed_up_weight[0], preferred_element_type=jnp.float32)
    ).astype(jnp.bfloat16)
    returned = lax.all_to_all(
        jnp.dot(hidden, routed_down_weight[0], preferred_element_type=jnp.float32)
        .astype(jnp.bfloat16)
        .reshape(arrived.shape),
        SP_TP,
        split_axis=0,
        concat_axis=0,
        tiled=True,
    )
    gathered = returned.reshape(experts * capacity, -1)[position].reshape(row_count, fanout, -1)
    routed = widened + shared
    for column in range(fanout):
        routed = routed + chosen_expert_weight[:, column, None] * gathered[:, column].astype(
            jnp.float32
        )
    return routed.astype(jnp.bfloat16)


def solution(mesh):
    split = Mesh(mesh.devices.reshape(4, 4, 4, mesh.shape["tp"]), ("sp_0", "sp_1", "sp_2", "tp"))
    return jax.shard_map(
        on_device,
        mesh=split,
        in_specs=(
            P(SP_TP, None),
            P(SP, "tp"),
            P(SP, "tp"),
            P(SP, "tp"),
            P(SP, "tp"),
            P(SP, "tp"),
            P(SP, "tp"),
            P(None, "tp"),
            P(None, "tp"),
            P(None, "tp"),
            P("tp"),
            P("tp"),
            P("tp"),
            P("tp"),
            P("tp", None),
            P(),
            P(SP_TP, None),
            P(SP_TP, None),
            P(SP_TP, None, None),
            P(SP_TP, None, None),
            P(SP_TP, None, None),
            P(),
            P(),
            P(),
        ),
        out_specs=P(SP_TP, None),
        check_vma=False,
    )
```

profile of v0, /device:TPU:1, one launch (start us, length us, event | category | flops | bytes accessed | tf_op | source)
XLA Modules:
  0.0 350.1 jit_solution(2889156641957486147)
XLA Ops:
  8.3 3.9 %collective-permute-start.2 = (bf16[3,1024]{0,1:T(8,128)(2,1)}, bf16[3,1024]{0,1:T(8,128)(2,1)S(1)}, u32[]{:S(2)}, u32[]{:S(2)}) collective-permute-start(bf16[3,1024]{0,1:T(8,128)(2,1)} %copy.71), channel_id=1, source_target_pairs={{0,2},{2,4},{4,6},{6,8},{8,10},{10,12},{12,14},{14,16},{16,18},{18... | collective-permute-start | bytes 18440 | tf_op jit(solution)/shard_map/ppermute | solution.py:17
  39.8 7.2 %all_gather.26 = f32[4,2,8]{2,1,0:T(2,128)S(1)} all-gather(f32[1,2,8]{2,1,0:T(2,128)S(1)} %copy-done.29), channel_id=1, replica_groups=mesh['sp_0'=4,'sp_1'=4,'sp_2'=4,'tp'=2] {'sp_2'}, dimensions={0}, use_global_device_ids=true | all-gather | bytes 320 | tf_op jit(solution)/shard_map/all_gather | solution.py:31
  47.0 8.0 %all_gather.27 = f32[4,2,8]{2,1,0:T(2,128)S(1)} all-gather(f32[1,2,8]{2,1,0:T(2,128)S(1)} %get-tuple-element.92), channel_id=1, replica_groups=mesh['sp_0'=4,'sp_1'=4,'sp_2'=4,'tp'=2] {'sp_1'}, dimensions={0}, use_global_device_ids=true | all-gather | bytes 320 | tf_op jit(solution)/shard_map/all_gather | solution.py:31
  55.6 16.7 %all-gather.9.cloned.1.call-done = f32[8,8,64,128]{3,2,1,0:T(8,128)} async-done(((f32[2,8,64,128]{3,2,1,0:T(8,128)}), f32[8,8,64,128]{3,2,1,0:T(8,128)}) %all-gather.9.cloned.1.call-update) | async-done | bytes 2097168 | tf_op jit(solution)/shard_map/all_gather | solution.py:31
  83.9 7.9 %all_gather.28 = f32[4,2,8]{2,1,0:T(2,128)S(1)} all-gather(f32[1,2,8]{2,1,0:T(2,128)S(1)} %get-tuple-element.86), channel_id=1, replica_groups=mesh['sp_0'=4,'sp_1'=4,'sp_2'=4,'tp'=2] {'sp_0'}, dimensions={0}, use_global_device_ids=true | all-gather | bytes 320 | tf_op jit(solution)/shard_map/all_gather | solution.py:31
  93.7 12.1 %all-gather.5.cloned.1.call-done = f32[4,2,8,64,128]{4,3,2,1,0:T(8,128)} async-done(((f32[1,2,8,64,128]{4,3,2,1,0:T(8,128)}), f32[4,2,8,64,128]{4,3,2,1,0:T(8,128)}) %all-gather.5.cloned.1.call-update) | async-done | bytes 2097168 | tf_op jit(solution)/shard_map/all_gather | solution.py:31
  120.4 5.2 %while.13 = (s32[]{:T(128)}, f32[2,8,64,128]{3,2,1,0:T(8,128)S(1)}, bf16[2,2,8,64,128]{4,3,2,1,0:T(8,128)(2,1)}, f32[2,2,8]{2,1,0:T(2,128)}, f32[2,2,8,64,128]{4,3,2,1,0:T(8,128)}, /*index=5*/s32[]{:T(128)}, s32[]{:T(128)}) while((s32[]{:T(128)}, f32[2,8,64,128]{3,2,1,0:T(8,128)S(1)}, bf16[2,2,8,64,128]{4,3,2,1,0:T(8,128)(2,1)}, ...), condition=%wide.region_2.3_spmd.clone, body=%wide.region_1.2_spmd.clone.sunk | while | flops 524291 | bytes 2359596 | solution.py:138
  130.2 9.3 %all-gather.7.cloned.1.call-done = f32[4,2,8,64,128]{4,3,2,1,0:T(8,128)} async-done(((f32[1,2,8,64,128]{4,3,2,1,0:T(8,128)}), f32[4,2,8,64,128]{4,3,2,1,0:T(8,128)}) %all-gather.7.cloned.1.call-update) | async-done | bytes 2097168 | tf_op jit(solution)/shard_map/all_gather | solution.py:31
  139.7 4.8 %fusion.41 = (f32[2,128,2]{1,2,0:T(2,128)S(1)}, f32[2,128,2,8,64]{1,4,3,2,0:T(8,128)S(1)}) fusion(f32[2,128,2,8,64]{1,0,4,3,2:T(2,128)} %reshape.216, f32[2,128,2,8,64]{1,0,4,3,2:T(2,128)} %reshape.214, f32[2,8]{1,0:T(2,128)S(1)} %copy-done.39, f32[2,128,2,8,64]{1,4,3,2,0:T(8,128)} %fusion.20, bf16[2,128,2,128,1]{3,2,1,0,4:T(2,128)(2,1)S(1)} %bitcast.321, ...), kind=kOutput, calls=%fused_computation.63 | convolution fusion | flops 73793024 | bytes 10636236 | tf_op jit(solution)/shard_map/btgn,gepn,btge->btgep/dot_general | solution.py:143
  147.9 5.2 %all_to_all.15 = bf16[2,128,2048]{2,1,0:T(8,128)(2,1)S(1)} all-to-all(bf16[2,128,2048]{2,1,0:T(8,128)(2,1)S(1)} %bitcast.323), channel_id=1, replica_groups=mesh['sp_0'=4,'sp_1'=4,'sp_2'=4,'tp'=2] {'tp'}, dimensions={0} | all-to-all | bytes 2097152 | tf_op jit(solution)/shard_map/all_to_all | solution.py:49
  154.1 4.3 %gather_fusion = bf16[768,2048]{1,0:T(8,128)(2,1)} fusion(bf16[129,2048]{1,0:T(8,128)(2,1)S(1)} %concatenate.15, s32[1024]{0:T(1024)S(1)} %copy-done.7), kind=kCustom, calls=%fused_computation | custom fusion | bytes 6294528 | tf_op jit(solution)/shard_map/gather | solution.py:183
  158.3 6.2 %reshape.219 = bf16[128,6,2048]{2,1,0:T(8,128)(2,1)} reshape(bf16[768,2048]{1,0:T(8,128)(2,1)} %gather_fusion) | data formatting | bytes 6291456 | tf_op jit(solution)/shard_map/reshape | solution.py:183
  164.6 60.9 %all_to_all.16 = bf16[128,6,2048]{2,1,0:T(8,128)(2,1)} all-to-all(bf16[128,6,2048]{2,1,0:T(8,128)(2,1)} %reshape.219), channel_id=1, replica_groups=mesh['sp_0'=4,'sp_1'=4,'sp_2'=4,'tp'=2] {'sp_0','sp_1','sp_2','tp'}, dimensions={0} | all-to-all | bytes 6291456 | tf_op jit(solution)/shard_map/all_to_all | solution.py:184
  225.5 6.3 %reshape.220 = bf16[768,2048]{1,0:T(8,128)(2,1)} reshape(bf16[128,6,2048]{2,1,0:T(8,128)(2,1)} %all_to_all.16) | data formatting | bytes 6291456 | tf_op jit(solution)/shard_map/reshape | solution.py:185
  231.8 5.5 %fusion.8 = f32[768,512]{1,0:T(8,128)} fusion(bf16[768,2048]{1,0:T(8,128)(2,1)} %reshape.220, bf16[1,2048,512]{2,1,0:T(8,128)(2,1)} %param.44), kind=kOutput, calls=%fused_computation.17 | convolution fusion | flops 1610612736 | bytes 6815744 | tf_op jit(solution)/shard_map/dot_general | solution.py:187
  237.3 8.1 %convolution_convert_fusion = bf16[768,2048]{1,0:T(8,128)(2,1)} fusion(bf16[1,512,2048]{2,1,0:T(8,128)(2,1)S(1)} %copy-done, f32[768,512]{1,0:T(8,128)} %fusion.8, bf16[768,2048]{1,0:T(8,128)(2,1)} %reshape.220, bf16[1,2048,512]{2,1,0:T(8,128)(2,1)} %param.45), kind=kOutput, calls=%fused_computation.6 | convolution fusion | flops 3225157632 | bytes 12058624 | tf_op jit(solution)/shard_map/dot_general | solution.py:191
  245.4 6.3 %reshape.221 = bf16[128,6,2048]{2,1,0:T(8,128)(2,1)} reshape(bf16[768,2048]{1,0:T(8,128)(2,1)} %convolution_convert_fusion) | data formatting | bytes 6291456 | tf_op jit(solution)/shard_map/reshape | solution.py:193
  251.7 5.6 %all-to-all-start.2 = ((bf16[128,6,2048]{2,1,0:T(8,128)(2,1)}), bf16[128,6,2048]{2,1,0:T(8,128)(2,1)}, u32[]{:S(2)}, u32[]{:S(2)}) async-start(bf16[128,6,2048]{2,1,0:T(8,128)(2,1)} %reshape.221), calls=%async_computation.2 | async-start | bytes 8388608 | tf_op jit(solution)/shard_map/all_to_all | solution.py:190
  259.4 50.6 %all-to-all-done.2 = bf16[128,6,2048]{2,1,0:T(8,128)(2,1)} async-done(((bf16[128,6,2048]{2,1,0:T(8,128)(2,1)}), bf16[128,6,2048]{2,1,0:T(8,128)(2,1)}, u32[]{:S(2)}, u32[]{:S(2)}) %all-to-all-start.2) | async-done | bytes 3145760 | tf_op jit(solution)/shard_map/all_to_all | solution.py:190
  310.0 6.3 %reshape.222 = bf16[768,2048]{1,0:T(8,128)(2,1)} reshape(bf16[128,6,2048]{2,1,0:T(8,128)(2,1)} %all-to-all-done.2) | data formatting | bytes 6291456 | tf_op jit(solution)/shard_map/reshape | solution.py:199
  316.3 7.5 %gather_fusion.1 = bf16[512,2048]{1,0:T(8,128)(2,1)} fusion(bf16[768,2048]{1,0:T(8,128)(2,1)} %reshape.222, s32[1024]{0:T(1024)S(1)} %pad_clamp_fusion), kind=kCustom, calls=%fused_computation.1 | custom fusion | bytes 4196352 | tf_op jit(solution)/shard_map/gather | solution.py:199
  323.9 4.1 %reshape.223 = bf16[128,4,2048]{2,1,0:T(4,128)(2,1)} reshape(bf16[512,2048]{1,0:T(8,128)(2,1)} %gather_fusion.1) | data formatting | bytes 4194304 | tf_op jit(solution)/shard_map/reshape | solution.py:199
  328.0 9.4 %fusion.180 = (bf16[128,1,2048]{2,1,0:T(2,128)(2,1)}, bf16[128,1,2048]{2,1,0:T(2,128)(2,1)}, bf16[128,1,2048]{2,1,0:T(2,128)(2,1)}, bf16[128,1,2048]{2,1,0:T(2,128)(2,1)}) fusion(bf16[128,4,2048]{2,1,0:T(4,128)(2,1)} %reshape.223), kind=kLoop, calls=%fused_computation.274 | loop fusion | bytes 4194304 | tf_op jit(solution)/shard_map/slice | solution.py:202
  337.4 6.2 %fusion.4 = bf16[128,2048]{1,0:T(8,128)(2,1)} fusion(bf16[512,2048]{1,0:T(8,128)(2,1)} %param.49, bf16[128,2048]{1,0:T(8,128)(2,1)S(1)} %get-tuple-element.62, bf16[2048,512]{1,0:T(8,128)(2,1)} %param.48, bf16[128,1,2048]{2,1,0:T(2,128)(2,1)} %get-tuple-element.70, bf16[128,1,2048]{2,1,0:T(2,128)(2,1)} %get-tuple-element.68, ...), kind=kOutput, calls=%fused_computation.13 | convolution fusion | flops 542244864 | bytes 7612928 | tf_op jit(solution)/shard_map/dot_general | solution.py:170
  (180 shorter events, 73.8 us)
Async XLA Ops:
  6.5 230.7 %copy-start = (bf16[1,512,2048]{2,1,0:T(8,128)(2,1)S(1)}, bf16[1,512,2048]{2,1,0:T(8,128)(2,1)}, u32[]{:S(2)}) copy-start(bf16[1,512,2048]{2,1,0:T(8,128)(2,1)} %param.46) | copy-start | bytes 6291460
  6.5 21.6 %copy-start.4 = (bf16[256,256]{1,0:T(8,128)(2,1)S(1)}, bf16[256,256]{1,0:T(8,128)(2,1)}, u32[]{:S(2)}) copy-start(bf16[256,256]{1,0:T(8,128)(2,1)} %param.28) | copy-start | bytes 393220
  6.5 65.7 %all-gather.9.cloned.1.call-start = ((), (), s32[]{:S(2)}) async-start(), calls=%async_computation.5 | async-start | bytes 2621440 | tf_op jit(solution)/shard_map/all_gather | solution.py:31
  8.3 21.4 %collective-permute-start.2 = (bf16[3,1024]{0,1:T(8,128)(2,1)}, bf16[3,1024]{0,1:T(8,128)(2,1)S(1)}, u32[]{:S(2)}, u32[]{:S(2)}) collective-permute-start(bf16[3,1024]{0,1:T(8,128)(2,1)} %copy.71), channel_id=1, source_target_pairs={{0,2},{2,4},{4,6},{6,8},{8,10},{10,12},{12,14},{14,16},{16,18},{18... | collective-permute-start | bytes 18440 | tf_op jit(solution)/shard_map/ppermute | solution.py:17
  13.5 14.7 %collective-permute-start.1 = (bf16[3,256]{1,0:T(4,128)(2,1)}, bf16[3,256]{1,0:T(4,128)(2,1)}, u32[]{:S(2)}, u32[]{:S(2)}) collective-permute-start(bf16[3,256]{1,0:T(4,128)(2,1)} %slice.199), channel_id=1, source_target_pairs={{0,2},{2,4},{4,6},{6,8},{8,10},{10,12},{12,14},{14,16},{16,18},{18... | collective-permute-start | bytes 4616 | tf_op jit(solution)/shard_map/ppermute | solution.py:17
  39.6 39.3 %copy-start.10 = (s32[128,4]{0,1:T(4,128)S(1)}, s32[128,4]{0,1:T(4,128)}, u32[]{:S(2)}) copy-start(s32[128,4]{0,1:T(4,128)} %param.42) | copy-start | bytes 6148
  39.7 66.1 %all-gather.5.cloned.1.call-start = ((), (), s32[]{:S(2)}) async-start(), calls=%async_computation.3 | async-start | bytes 2621440 | tf_op jit(solution)/shard_map/all_gather | solution.py:31
  47.0 29.2 %copy-start.16 = (f32[2,8]{1,0:T(2,128)}, f32[2,8]{1,0:T(2,128)S(1)}, u32[]{:S(2)}) copy-start(f32[2,8]{1,0:T(2,128)S(1)} %get-tuple-element.93) | copy-start | bytes 196
  47.0 29.2 %copy-start.18 = (f32[2,8]{1,0:T(2,128)}, f32[2,8]{1,0:T(2,128)S(1)}, u32[]{:S(2)}) copy-start(f32[2,8]{1,0:T(2,128)S(1)} %get-tuple-element.94) | copy-start | bytes 196
  47.0 29.2 %copy-start.20 = (f32[2,8]{1,0:T(2,128)}, f32[2,8]{1,0:T(2,128)S(1)}, u32[]{:S(2)}) copy-start(f32[2,8]{1,0:T(2,128)S(1)} %get-tuple-element.95) | copy-start | bytes 196
  55.5 20.6 %copy-start.13 = (f32[2,8]{1,0:T(2,128)}, f32[2,8]{1,0:T(2,128)S(1)}, u32[]{:S(2)}) copy-start(f32[2,8]{1,0:T(2,128)S(1)} %get-tuple-element.90) | copy-start | bytes 196
  74.8 18.3 %copy-start.12 = (bf16[4,256]{1,0:T(4,128)(2,1)S(1)}, bf16[4,256]{1,0:T(4,128)(2,1)}, u32[]{:S(2)}) copy-start(bf16[4,256]{1,0:T(4,128)(2,1)} %param.35) | copy-start | bytes 6148
  74.8 64.7 %all-gather.7.cloned.1.call-start = ((), (), s32[]{:S(2)}) async-start(), calls=%async_computation.4 | async-start | bytes 2621440 | tf_op jit(solution)/shard_map/all_gather | solution.py:31
  76.2 41.5 %collective-permute-start = (bf16[3,256]{1,0:T(4,128)(2,1)}, bf16[3,256]{1,0:T(4,128)(2,1)}, u32[]{:S(2)}, u32[]{:S(2)}) collective-permute-start(bf16[3,256]{1,0:T(4,128)(2,1)} %slice.190), channel_id=1, source_target_pairs={{0,2},{2,4},{4,6},{6,8},{8,10},{10,12},{12,14},{14,16},{16,18},{18... | collective-permute-start | bytes 4616 | tf_op jit(solution)/shard_map/ppermute | solution.py:17
  81.4 26.9 %copy-start.8 = (s32[512,1]{0,1:T(1,128)}, s32[512,1]{0,1:T(1,128)S(1)}, u32[]{:S(2)}) copy-start(s32[512,1]{0,1:T(1,128)S(1)} %compare_select_fusion.1) | copy-start | bytes 6148
  83.9 26.3 %copy-start.22 = (f32[2,8]{1,0:T(2,128)}, f32[2,8]{1,0:T(2,128)S(1)}, u32[]{:S(2)}) copy-start(f32[2,8]{1,0:T(2,128)S(1)} %get-tuple-element.87) | copy-start | bytes 196
  83.9 26.3 %copy-start.24 = (f32[2,8]{1,0:T(2,128)}, f32[2,8]{1,0:T(2,128)S(1)}, u32[]{:S(2)}) copy-start(f32[2,8]{1,0:T(2,128)S(1)} %get-tuple-element.88) | copy-start | bytes 196
  83.9 26.3 %copy-start.26 = (f32[2,8]{1,0:T(2,128)}, f32[2,8]{1,0:T(2,128)S(1)}, u32[]{:S(2)}) copy-start(f32[2,8]{1,0:T(2,128)S(1)} %get-tuple-element.89) | copy-start | bytes 196
  127.0 12.6 %copy-start.6 = (f32[2,128,2,8]{1,3,2,0:T(8,128)S(1)}, f32[2,128,2,8]{1,3,2,0:T(8,128)}, u32[]{:S(2)}) copy-start(f32[2,128,2,8]{1,3,2,0:T(8,128)} %copy.81) | copy-start | bytes 49156
  127.0 12.5 %copy-start.14 = (f32[2,8]{1,0:T(2,128)S(1)}, f32[2,8]{1,0:T(2,128)}, u32[]{:S(2)}) copy-start(f32[2,8]{1,0:T(2,128)} %copy-done.13) | copy-start | bytes 196
  127.0 12.5 %copy-start.15 = (f32[2,8]{1,0:T(2,128)S(1)}, f32[2,8]{1,0:T(2,128)}, u32[]{:S(2)}) copy-start(f32[2,8]{1,0:T(2,128)} %get-tuple-element.91) | copy-start | bytes 196
  127.0 12.5 %copy-start.17 = (f32[2,8]{1,0:T(2,128)S(1)}, f32[2,8]{1,0:T(2,128)}, u32[]{:S(2)}) copy-start(f32[2,8]{1,0:T(2,128)} %copy-done.16) | copy-start | bytes 196
  127.0 12.5 %copy-start.19 = (f32[2,8]{1,0:T(2,128)S(1)}, f32[2,8]{1,0:T(2,128)}, u32[]{:S(2)}) copy-start(f32[2,8]{1,0:T(2,128)} %copy-done.18) | copy-start | bytes 196
  251.7 58.4 %all-to-all-start.2 = ((bf16[128,6,2048]{2,1,0:T(8,128)(2,1)}), bf16[128,6,2048]{2,1,0:T(8,128)(2,1)}, u32[]{:S(2)}, u32[]{:S(2)}) async-start(bf16[128,6,2048]{2,1,0:T(8,128)(2,1)} %reshape.221), calls=%async_computation.2 | async-start | bytes 8388608 | tf_op jit(solution)/shard_map/all_to_all | solution.py:190
  (23 other events, 177.8 us)
Sparse Core Ops, SparseCore 0:
  39.8 32.4 all-gather.8
  74.9 30.8 all-gather.4
  108.5 30.9 all-gather.6
where the time goes:
time: 352 us; the launch traced here: 350 us
  blocking collectives  89.2 us (25%)
  waiting for transfers between devices  88.8 us (25%)
  local copies, waits for them, and re-layouts  80.9 us (23%)
  matrix products  35.3 us (10%)
  other arithmetic  26.2 us (7%)
  starting transfers between devices  16 us (5%)
  between operations  13.8 us (4%)
    all_to_all x1, blocking collectives, on_device(): lax.all_to_all(outgoing, SP_TP, split_axis=0, concat_axis=0, tiled=True)  60.9 us
    all_to_all x1, waiting for transfers between devices, on_device(): lax.all_to_all(jnp.dot(hidden, routed_down_weight[0], preferred_element_t...  50.6 us
    all_gather x3, waiting for transfers between devices, carried_in(): pieces = jax.tree.map(lambda part: lax.all_gather(part, axis), subtotal)  38.1 us
    all_gather x3, blocking collectives, carried_in(): pieces = jax.tree.map(lambda part: lax.all_gather(part, axis), subtotal)  23.1 us
    reshape x2, local copies, waits for them, and re-layouts, on_device(): returned.reshape(experts * capacity, -1)[position]  10.4 us
    ppermute x3, starting transfers between devices, from_behind(): return lax.ppermute(block, axis, route)  10.3 us
    slice x1, local copies, waits for them, and re-layouts, on_device(): gathered[:, column].astype(jnp.float32)  9.39 us
    dot_general x1, matrix products, on_device(): jnp.dot(hidden, routed_down_weight[0], preferred_element_type=jnp.float32)  8.11 us
  transfers between devices with their start and end apart: 7, of which 4 were waited for; matrix products, arithmetic and copies ran while one was open for 14% of the time, Pallas kernels for 0%

commit v1 on v0

v1 whole, which is shorter than its diff:
```python
import jax
import jax.numpy as jnp
from jax import lax
from jax.experimental import pallas as pl
from jax.experimental.pallas import tpu as pltpu
from jax.sharding import Mesh
from jax.sharding import PartitionSpec as P

HEAD_DIM = 64
STATE = 128
BLK = 128
LANES = 128
SLOTS = 6
WIDE = 8
SP = ("sp_0", "sp_1", "sp_2")
PLANE = ("sp_1", "sp_2")
SP_TP = ("sp_0", "sp_1", "sp_2", "tp")
F32 = jnp.float32
BF16 = jnp.bfloat16


def mm(a, b, dims=((1,), (0,)), precision=None):
    return lax.dot_general(a, b, (dims, ((), ())), precision=precision, preferred_element_type=F32)


def iota(shape, dim):
    return lax.broadcasted_iota(jnp.int32, shape, dim)


def head_lanes(width):
    return jnp.where(iota((LANES, width), 1) // HEAD_DIM == iota((LANES, width), 0), 1.0, 0.0).astype(BF16)


def spread(values, lanes):
    high = values.astype(BF16)
    low = (values - high.astype(F32)).astype(BF16)
    return mm(high, lanes) + mm(low, lanes)


def silu(v):
    return v * (1.0 / (1.0 + jnp.exp(-v)))


def whole(shape):
    return pl.BlockSpec(shape, lambda *_: (0,) * len(shape))


def front_kernel(x_ref, b_ref, c_ref, rim_ref, dt_ref, pld_ref, tx_ref, tb_ref, tc_ref, bias_ref, rate_ref,
                 sig_ref, wv_ref, rv_ref, cum_ref, dtv_ref, s0_ref, send_ref, ext_ref):
    length, chans = x_ref.shape
    vecs = b_ref.shape[1]
    heads = dt_ref.shape[1]
    groups = vecs // STATE
    width = chans // groups
    sources = ((x_ref, tx_ref, 0, chans, sig_ref), (b_ref, tb_ref, chans, vecs, wv_ref), (c_ref, tc_ref, chans + vecs, vecs, rv_ref))
    for src, taps, start, size, dst in sources:
        ext_ref[0:8, start : start + size] = rim_ref[:, start : start + size].astype(F32)
        ext_ref[8 : 8 + length, start : start + size] = src[...].astype(F32)
        for at in range(0, size, 256):
            lanes = slice(start + at, start + at + 256)
            weight = taps[:, at : at + 256].astype(F32)
            total = weight[0:1] * ext_ref[5 : 5 + length, lanes]
            for k in range(1, 4):
                total = total + weight[k : k + 1] * ext_ref[5 + k : 5 + k + length, lanes]
            dst[:, at : at + 256] = silu(total).astype(dst.dtype)
    v = dt_ref[...].astype(F32) + bias_ref[...]
    step = jnp.maximum(v, 0.0) + jnp.log(1.0 + jnp.exp(-jnp.abs(v)))
    logs = pld_ref[...] - rate_ref[...] * step
    dtv_ref[...] = jnp.zeros_like(dtv_ref)
    cum_ref[...] = jnp.zeros_like(cum_ref)
    dtv_ref[:, 0:heads] = step
    cum_ref[:, 0:heads] = logs
    lower = jnp.where(iota((length, length), 0) >= iota((length, length), 1), 1.0, 0.0)
    cum = mm(lower, cum_ref[...], precision=lax.Precision.HIGHEST)
    cum_ref[...] = cum
    half_end, end = cum[BLK - 1 : BLK], cum[length - 1 : length]
    ends = jnp.where(iota((length, LANES), 0) < BLK, half_end, end)
    lanes = head_lanes(chans)
    scaled = (sig_ref[...] * spread(dtv_ref[...] * jnp.exp(ends - cum), lanes)).astype(BF16)
    passing = spread(jnp.broadcast_to(jnp.exp(end - half_end), (8, LANES)), lanes)[0:1]
    for g in range(groups):
        part = slice(g * width, (g + 1) * width)
        vec = slice(g * STATE, (g + 1) * STATE)
        first = mm(wv_ref[0:BLK, vec], scaled[0:BLK, part], ((0,), (0,)))
        second = mm(wv_ref[BLK:length, vec], scaled[BLK:length, part], ((0,), (0,)))
        s0_ref[:, part] = first
        send_ref[:, part] = (first * passing[:, part] + second).astype(BF16)
    high = end.astype(BF16).astype(F32)
    mid = (end - high).astype(BF16).astype(F32)
    low = (end - high - mid).astype(BF16).astype(F32)
    row = iota((STATE, LANES), 0) % 8
    send_ref[:, chans : chans + LANES] = jnp.where(
        row == 0, high, jnp.where(row == 1, mid, jnp.where(row == 2, low, 0.0))
    ).astype(BF16)


def plane_kernel(got_ref, pin_ref, pdec_ref, send_ref):
    count = got_ref.shape[0] // 8
    chans = got_ref.shape[1] - LANES
    logs = jnp.sum(got_ref[:, chans:].astype(F32).reshape(count, 8, LANES), axis=1)
    lanes = head_lanes(chans)
    decay = spread(jnp.exp(logs), lanes)
    state = jnp.zeros((8, chans), F32)
    sofar = jnp.zeros((1, LANES), F32)
    before = []
    for i in range(count):
        pin_ref[8 * i : 8 * i + 8, :] = state
        before.append(sofar)
        state = state * decay[i : i + 1] + got_ref[8 * i : 8 * i + 8, 0:chans].astype(F32)
        sofar = sofar + logs[i : i + 1]
    pdec_ref[...] = spread(jnp.exp(jnp.concatenate(before, axis=0)), lanes)
    send_ref[:, 0:chans] = state
    send_ref[:, chans:] = jnp.broadcast_to(sofar, (8, LANES))


def planes_kernel(pin_ref, pdec_ref, one_ref, two_ref, three_ref, out_ref):
    chans = pin_ref.shape[1]
    count = pin_ref.shape[0] // 8
    lanes = head_lanes(chans)
    near = spread(jnp.exp(one_ref[:, chans:]), lanes)
    far = spread(jnp.exp(two_ref[:, chans:]), lanes)
    state = one_ref[:, 0:chans] + near * (two_ref[:, 0:chans] + far * three_ref[:, 0:chans])
    for i in range(0, count, 2):
        pair = [pin_ref[8 * k : 8 * k + 8, :] + state * pdec_ref[k : k + 1, :] for k in (i, i + 1)]
        out_ref[8 * i : 8 * i + 16, :] = jnp.concatenate(pair, axis=0).astype(BF16)


def near_kernel(sig_ref, wv_ref, rv_ref, cum_ref, dtv_ref, s0_ref, direct_ref, y_ref, pad_ref):
    length, chans = sig_ref.shape
    heads = direct_ref.shape[1]
    groups = wv_ref.shape[1] // STATE
    width = chans // groups
    lanes = head_lanes(chans)
    cum = cum_ref[...]
    cum_rows = cum.T
    pad_ref[...] = jnp.zeros_like(pad_ref)
    pad_ref[:, 0:heads] = jnp.broadcast_to(direct_ref[...], (8, heads))
    direct = spread(pad_ref[...], lanes)[0:1]
    scaled = (sig_ref[...] * spread(dtv_ref[...], lanes)).astype(BF16)
    causal = iota((BLK, BLK), 0) >= iota((BLK, BLK), 1)
    left = iota((BLK, LANES), 1) < HEAD_DIM
    into = spread(jnp.exp(cum[BLK:length] - cum[BLK - 1 : BLK]), lanes)
    for b in range(length // BLK):
        rows = slice(b * BLK, (b + 1) * BLK)
        for g in range(groups):
            vec = slice(g * STATE, (g + 1) * STATE)
            part = slice(g * width, (g + 1) * width)
            products = mm(rv_ref[rows, vec], wv_ref[rows, vec], ((1,), (1,)))
            if b == 1:
                carried = mm(rv_ref[rows, vec], s0_ref[:, part].astype(BF16)) * into[:, part]
            for j in range(width // LANES):
                at = g * width + j * LANES
                mats = []
                for h in (at // HEAD_DIM, at // HEAD_DIM + 1):
                    gap = cum[rows, h : h + 1] - cum_rows[h : h + 1, rows]
                    mats.append((products * jnp.exp(jnp.where(causal, gap, -1e30))).astype(BF16))
                pair = scaled[rows, at : at + LANES]
                zero = jnp.zeros_like(pair)
                stacked = jnp.concatenate([jnp.where(left, pair, zero), jnp.where(left, zero, pair)], axis=0)
                out = mm(jnp.concatenate(mats, axis=1), stacked)
                out = out + direct[:, at : at + LANES] * sig_ref[rows, at : at + LANES]
                if b == 1:
                    out = out + carried[:, j * LANES : (j + 1) * LANES]
                y_ref[rows, at : at + LANES] = out


def project_kernel(half_ref, y_ref, state_ref, rv_ref, cum_ref, gate_ref, gain_ref, w_ref, own_ref, other_ref, mix_ref, res_ref):
    length, chans = y_ref.shape
    groups = rv_ref.shape[1] // STATE
    width = chans // groups
    rows = own_ref.shape[0]

    @pl.when(pl.program_id(0) == 0)
    def _():
        scale = spread(jnp.exp(cum_ref[...]), head_lanes(chans))
        for g in range(groups):
            part = slice(g * width, (g + 1) * width)
            far = mm(rv_ref[:, g * STATE : (g + 1) * STATE], state_ref[:, part])
            gated = (y_ref[:, part] + far * scale[:, part]) * silu(gate_ref[:, part].astype(F32))
            mean = jnp.sum(gated * gated, axis=1, keepdims=True) * (1.0 / width)
            mix_ref[:, part] = (gated * lax.rsqrt(mean + 1e-06) * gain_ref[:, part]).astype(BF16)

    res_ref[...] = mm(mix_ref[...], w_ref[...])
    half = half_ref[0]
    own_ref[...] = res_ref[pl.ds(pl.multiple_of(half * rows, rows), rows), :]
    other_ref[...] = res_ref[pl.ds(pl.multiple_of((1 - half) * rows, rows), rows), :].astype(BF16)


def slot_table(chosen, experts):
    count = chosen.shape[0]
    expert = iota((count, experts), 1)
    named = jnp.zeros((count, experts), F32)
    for k in range(chosen.shape[1]):
        named = named + jnp.where(chosen[:, k : k + 1] == expert, 1.0, 0.0)
    earlier = jnp.where(iota((count, count), 0) > iota((count, count), 1), 1.0, 0.0).astype(BF16)
    rank = mm(earlier, named.astype(BF16))
    return named * (rank + 1.0)


def expert_rows(experts):
    return jnp.where(iota((experts * WIDE, experts), 0) // WIDE == iota((experts * WIDE, experts), 1), 1.0, 0.0).astype(BF16)


def dispatch_kernel(own_ref, got_ref, stream_ref, gain_ref, chosen_ref, residual_ref, normed_ref, out_ref, both_ref):
    rows, dim = own_ref.shape
    third = out_ref.shape[1] // 3
    experts = out_ref.shape[0] // WIDE
    residual = (stream_ref[...].astype(F32) + own_ref[...] + got_ref[...].astype(F32)).astype(BF16)
    residual_ref[...] = residual
    wide = residual.astype(F32)
    mean = jnp.sum(wide * wide, axis=1, keepdims=True) * (1.0 / dim)
    normed_ref[...] = (wide * lax.rsqrt(mean + 1e-06) * gain_ref[...]).astype(BF16)
    table = slot_table(chosen_ref[...], experts)
    slots = mm(expert_rows(experts), table.astype(BF16), ((1,), (1,)))
    place = (iota(slots.shape, 0) % WIDE).astype(F32)
    main = jnp.where(slots == place + 1.0, 1.0, 0.0)
    for q in range(3):
        tail = jnp.where((place >= 6.0) & (slots == 3.0 * place + (q - 17.0)), 1.0, 0.0)
        both_ref[:, 0:rows] = main.astype(BF16)
        both_ref[:, rows:] = tail.astype(BF16)
        source = jnp.concatenate([normed_ref[:, q * third : (q + 1) * third], normed_ref[:, 3 * third :]], axis=0)
        out_ref[:, q * third : (q + 1) * third] = mm(both_ref[...], source).astype(BF16)


def shared_kernel(normed_ref, residual_ref, gate_ref, up_ref, down_ref, out_ref):
    @pl.when(pl.program_id(0) == 0)
    def _():
        out_ref[...] = residual_ref[...].astype(F32)

    normed = normed_ref[...]
    hidden = (silu(mm(normed, gate_ref[...])) * mm(normed, up_ref[...])).astype(BF16)
    out_ref[...] += mm(hidden, down_ref[...])


def expert_kernel(x_ref, gate_ref, up_ref, down_ref, out_ref, full_ref):
    rows, wide = x_ref.shape
    third = wide // 3
    row, col = iota((LANES, LANES), 0), iota((LANES, LANES), 1)
    same = row // WIDE == col // WIDE
    r, c = row % WIDE, col % WIDE
    unpack = [jnp.where(same & (c >= 6) & (r == 3 * (c - 6) + q), 1.0, 0.0).astype(BF16) for q in range(3)]
    pack = [jnp.where(same & (r >= 6) & (c == 3 * (r - 6) + q), 1.0, 0.0).astype(BF16) for q in range(3)]
    unpack, pack = jnp.concatenate(unpack, axis=1), jnp.concatenate(pack, axis=0)
    full_ref[:, 0:wide] = x_ref[...]
    for at in range(0, rows, LANES):
        pieces = [x_ref[at : at + LANES, q * third : (q + 1) * third] for q in range(3)]
        full_ref[at : at + LANES, wide:] = mm(unpack, jnp.concatenate(pieces, axis=0)).astype(BF16)
    full = full_ref[...]
    hidden = (silu(mm(full, gate_ref[...])) * mm(full, up_ref[...])).astype(BF16)
    tail = mm(hidden, down_ref[:, wide:]).astype(BF16)
    inside = iota((LANES, third), 0) % WIDE < SLOTS
    packed = [mm(pack, tail[at : at + LANES]) for at in range(0, rows, LANES)]
    for q in range(3):
        part = slice(q * third, (q + 1) * third)
        result = mm(hidden, down_ref[:, part])
        for k, at in enumerate(range(0, rows, LANES)):
            extra = packed[k][q * LANES : (q + 1) * LANES]
            out_ref[at : at + LANES, part] = jnp.where(inside, result[at : at + LANES], extra).astype(BF16)


def combine_kernel(got_ref, base_ref, chosen_ref, weight_ref, out_ref, mats_ref, tail_ref):
    rows, dim = base_ref.shape
    third = got_ref.shape[1]
    experts = got_ref.shape[0] // WIDE
    q = pl.program_id(0)

    @pl.when(q == 0)
    def _():
        chosen = chosen_ref[...]
        table = slot_table(chosen, experts)
        expert = iota((rows, experts), 1)
        weights = jnp.zeros((rows, experts), F32)
        for k in range(chosen.shape[1]):
            weights = weights + jnp.where(chosen[:, k : k + 1] == expert, weight_ref[:, k : k + 1], 0.0)
        lanes = expert_rows(experts)
        slots = mm(table.astype(BF16), lanes, ((1,), (1,)))
        spread_weights = mm(weights.astype(BF16), lanes, ((1,), (1,)))
        place = (iota(slots.shape, 1) % WIDE).astype(F32)
        mats_ref[0:rows, :] = jnp.where(slots == place + 1.0, spread_weights, 0.0).astype(BF16)
        for k in range(3):
            hit = (place >= 6.0) & (slots == 3.0 * place + (k - 17.0))
            mats_ref[rows * (k + 1) : rows * (k + 2), :] = jnp.where(hit, spread_weights, 0.0).astype(BF16)
        tail_ref[...] = base_ref[:, 3 * third :]

    got = got_ref[...]
    tail_ref[...] += mm(mats_ref[pl.ds(pl.multiple_of(rows * (q + 1), rows), rows), :], got)
    main = mm(mats_ref[0:rows, :], got)
    for k in range(3):
        @pl.when(q == k)
        def _():
            part = slice(k * third, (k + 1) * third)
            out_ref[:, part] = (base_ref[:, part] + main).astype(BF16)

    @pl.when(q == 2)
    def _():
        out_ref[:, 3 * third :] = tail_ref[...].astype(BF16)


def shape(dims, dtype=F32):
    return jax.ShapeDtypeStruct(dims, dtype)


def on_device(
    stream,
    head_input_signal,
    write_input_vectors,
    read_input_vectors,
    output_gate_input,
    step_size_input,
    position_log_decay,
    signal_filter_taps,
    write_filter_taps,
    read_filter_taps,
    step_size_bias,
    head_decay_rate,
    head_direct_term,
    grouped_norm_gain,
    mixer_output_weight,
    expert_norm_gain,
    chosen_expert_index,
    chosen_expert_weight,
    routed_gate_weight,
    routed_up_weight,
    routed_down_weight,
    common_gate_weight,
    common_up_weight,
    common_down_weight,
):
    length, chans = head_input_signal.shape
    vecs = write_input_vectors.shape[1]
    rows, dim = stream.shape
    hidden = common_gate_weight.shape[1]
    experts = lax.axis_size(SP_TP)
    wide = dim * SLOTS // WIDE

    rim = jnp.concatenate([head_input_signal[length - 8 :], write_input_vectors[length - 8 :], read_input_vectors[length - 8 :]], axis=1)
    devices = lax.axis_size(SP)
    rim = lax.ppermute(rim, SP, [(i, i + 1) for i in range(devices - 1)])
    sig, wv, rv, cum, dtv, s0, send = pl.pallas_call(
        front_kernel,
        out_shape=(
            shape((length, chans)), shape((length, vecs), BF16), shape((length, vecs), BF16), shape((length, LANES)),
            shape((length, LANES)), shape((STATE, chans)), shape((STATE, chans + LANES), BF16),
        ),
        scratch_shapes=[pltpu.VMEM((length + 8, chans + 2 * vecs), F32)],
        name="front",
    )(
        head_input_signal, write_input_vectors, read_input_vectors, rim, step_size_input, position_log_decay,
        signal_filter_taps, write_filter_taps, read_filter_taps, step_size_bias[None], head_decay_rate[None],
    )
    in_plane = lax.axis_size(PLANE)
    got = lax.all_to_all(send, PLANE, split_axis=0, concat_axis=0, tiled=True)
    near = pl.pallas_call(
        near_kernel,
        out_shape=shape((length, chans)),
        scratch_shapes=[pltpu.VMEM((8, LANES), F32)],
        cost_estimate=pl.CostEstimate(flops=400_000_000, transcendentals=1_000_000, bytes_accessed=4_000_000),
        name="near",
    )(sig, wv, rv, cum, dtv, s0, head_direct_term[None])
    pin, pdec, total = pl.pallas_call(
        plane_kernel,
        out_shape=(shape((STATE, chans)), shape((in_plane, chans)), shape((STATE // in_plane, chans + LANES))),
        name="plane",
    )(got)
    planes = lax.axis_size("sp_0")
    lower = [lax.ppermute(total, "sp_0", [(i, i + s) for i in range(planes - s)]) for s in (1, 2, 3)]
    back = pl.pallas_call(planes_kernel, out_shape=shape((STATE, chans), BF16), name="planes")(pin, pdec, *lower)
    incoming = lax.all_to_all(back, PLANE, split_axis=0, concat_axis=0, tiled=True)

    step = 512
    half = lax.axis_index("tp").astype(jnp.int32).reshape(1)
    own, other = pl.pallas_call(
        project_kernel,
        grid=(dim // step,),
        in_specs=[
            pl.BlockSpec(memory_space=pltpu.SMEM),
            whole((length, chans)), whole((STATE, chans)), whole((length, vecs)), whole((length, LANES)),
            whole((length, chans)), whole((1, chans)), pl.BlockSpec((chans, step), lambda n: (0, n)),
        ],
        out_specs=(pl.BlockSpec((rows, step), lambda n: (0, n)), pl.BlockSpec((rows, step), lambda n: (0, n))),
        out_shape=(shape((rows, dim)), shape((rows, dim), BF16)),
        scratch_shapes=[pltpu.VMEM((length, chans), BF16), pltpu.VMEM((length, step), F32)],
        name="project",
    )(half, near, incoming, rv, cum, output_gate_input, grouped_norm_gain[None], mixer_output_weight)
    partner = lax.ppermute(other, "tp", [(0, 1), (1, 0)])

    residual, normed, outgoing = pl.pallas_call(
        dispatch_kernel,
        out_shape=(shape((rows, dim), BF16), shape((rows, dim), BF16), shape((experts * WIDE, wide), BF16)),
        scratch_shapes=[pltpu.VMEM((experts * WIDE, 2 * rows), BF16)],
        name="dispatch",
    )(own, partner, stream, expert_norm_gain[None], chosen_expert_index)
    arrived = lax.all_to_all(outgoing, SP_TP, split_axis=0, concat_axis=0, tiled=True)

    part = 128
    base = pl.pallas_call(
        shared_kernel,
        grid=(hidden // part,),
        in_specs=[
            whole((rows, dim)), whole((rows, dim)), pl.BlockSpec((dim, part), lambda n: (0, n)),
            pl.BlockSpec((dim, part), lambda n: (0, n)), pl.BlockSpec((part, dim), lambda n: (n, 0)),
        ],
        out_specs=whole((rows, dim)),
        out_shape=shape((rows, dim)),
        cost_estimate=pl.CostEstimate(flops=800_000_000, transcendentals=70_000, bytes_accessed=8_000_000),
        name="shared",
    )(normed, residual, common_gate_weight, common_up_weight, common_down_weight)

    tall = 256
    inner = routed_gate_weight.shape[2]
    served = pl.pallas_call(
        expert_kernel,
        grid=(experts * WIDE // tall,),
        in_specs=[
            pl.BlockSpec((tall, wide), lambda m: (m, 0)),
            pl.BlockSpec((None, dim, inner), lambda m: (0, 0, 0)),
            pl.BlockSpec((None, dim, inner), lambda m: (0, 0, 0)),
            pl.BlockSpec((None, inner, dim), lambda m: (0, 0, 0)),
        ],
        out_specs=pl.BlockSpec((tall, wide), lambda m: (m, 0)),
        out_shape=shape((experts * WIDE, wide), BF16),
        scratch_shapes=[pltpu.VMEM((tall, dim), BF16)],
        name="experts",
    )(arrived, routed_gate_weight, routed_up_weight, routed_down_weight)
    returned = lax.all_to_all(served, SP_TP, split_axis=0, concat_axis=0, tiled=True)

    fanout = chosen_expert_index.shape[1]
    return pl.pallas_call(
        combine_kernel,
        grid=(3,),
        in_specs=[
            pl.BlockSpec((experts * WIDE, wide // 3), lambda q: (0, q)),
            whole((rows, dim)), whole((rows, fanout)), whole((rows, fanout)),
        ],
        out_specs=whole((rows, dim)),
        out_shape=shape((rows, dim), BF16),
        scratch_shapes=[pltpu.VMEM((4 * rows, experts * WIDE), BF16), pltpu.VMEM((rows, wide // 3), F32)],
        name="combine",
    )(returned, base, chosen_expert_index, chosen_expert_weight)


def solution(mesh):
    split = Mesh(mesh.devices.reshape(4, 4, 4, mesh.shape["tp"]), ("sp_0", "sp_1", "sp_2", "tp"))
    return jax.shard_map(
        on_device,
        mesh=split,
        in_specs=(
            P(SP_TP, None),
            P(SP, "tp"),
            P(SP, "tp"),
            P(SP, "tp"),
            P(SP, "tp"),
            P(SP, "tp"),
            P(SP, "tp"),
            P(None, "tp"),
            P(None, "tp"),
            P(None, "tp"),
            P("tp"),
            P("tp"),
            P("tp"),
            P("tp"),
            P("tp", None),
            P(),
            P(SP_TP, None),
            P(SP_TP, None),
            P(SP_TP, None, None),
            P(SP_TP, None, None),
            P(SP_TP, None, None),
            P(),
            P(),
            P(),
        ),
        out_specs=P(SP_TP, None),
        check_vma=False,
    )
```

time: 352 us -> 191 us (0.54)
  local copies, waits for them, and re-layouts: 80.9 us -> 10.8 us
  Pallas kernels: 0 us -> 49.5 us
  waiting for transfers between devices: 88.8 us -> 40.3 us
  matrix products: 35.3 us -> 0 us
  blocking collectives: 89.2 us -> 61.8 us
  other arithmetic: 26.2 us -> 0.01 us
  between operations: 13.8 us -> 0.1 us
  starting transfers between devices: 16 us -> 27.8 us
    pallas_call x0 -> x9, Pallas kernels: none -> 49.5 us  [the longest x1 13.3 us: on_device(): pl.pallas_call(expert_kernel, grid=(experts * WIDE // tall,), in_specs=[p...]
    all_gather x3 -> x0, waiting for transfers between devices: 38.1 us -> none  [carried_in(): pieces = jax.tree.map(lambda part: lax.all_gather(part, axis), subtotal)]
    dot_general x11 -> x0, matrix products: 35.3 us -> none  [the longest x1 8.11 us: on_device(): jnp.dot(hidden, routed_down_weight[0], preferred_element_type=jnp.float32)]
    reshape x10 -> x0, local copies, waits for them, and re-layouts: 33.7 us -> none  [the longest x2 10.4 us: on_device(): returned.reshape(experts * capacity, -1)[position]]
    all_gather x3 -> x0, blocking collectives: 23.1 us -> none  [carried_in(): pieces = jax.tree.map(lambda part: lax.all_gather(part, axis), subtotal)]
    slice x8 -> x3, local copies, waits for them, and re-layouts: 17.2 us -> 2.09 us  [the longest x1 0.72 us: on_device(): head_input_signal[length - 8:]]
    all_to_all x1, blocking collectives: 60.9 us -> 47.4 us  [on_device(): lax.all_to_all(outgoing, SP_TP, split_axis=0, concat_axis=0, tiled=True)]
    all_to_all x1 -> x2, waiting for transfers between devices: 50.6 us -> 37.9 us  [the longest x1 34.4 us: on_device(): lax.all_to_all(served, SP_TP, split_axis=0, concat_axis=0, tiled=True)]
  transfers between devices with their start and end apart: 7 -> 7, of which waited for: 4 -> 4; matrix products, arithmetic and copies ran while one was open for 14% -> 2% of each run, Pallas kernels for 0% -> 6%
where the time goes in v1:
time: 191 us; the launch traced here: 190 us
  blocking collectives  61.8 us (32%)
  Pallas kernels  49.5 us (26%)
  waiting for transfers between devices  40.3 us (21%)
  starting transfers between devices  27.8 us (15%)
  local copies, waits for them, and re-layouts  10.8 us (6%)
    all_to_all x1, blocking collectives, on_device(): lax.all_to_all(outgoing, SP_TP, split_axis=0, concat_axis=0, tiled=True)  47.4 us
    all_to_all x1, waiting for transfers between devices, on_device(): lax.all_to_all(served, SP_TP, split_axis=0, concat_axis=0, tiled=True)  34.4 us
    all_to_all x1, blocking collectives, on_device(): got = lax.all_to_all(send, PLANE, split_axis=0, concat_axis=0, tiled=True)  14.4 us
    pallas_call x1, Pallas kernels, on_device(): pl.pallas_call(expert_kernel, grid=(experts * WIDE // tall,), in_specs=[p...  13.3 us
    ppermute x3, starting transfers between devices, on_device(): lax.ppermute(total, 'sp_0', [(i, i + s) for i in range(planes - s)])  10.5 us
    unnamed x22, local copies, waits for them, and re-layouts  8.7 us
    pallas_call x1, Pallas kernels, on_device(): pl.pallas_call(shared_kernel, grid=(hidden // part,), in_specs=[whole((ro...  6.47 us
    pallas_call x1, Pallas kernels, on_device(): pl.pallas_call(project_kernel, grid=(dim // step,), in_specs=[pl.BlockSpe...  6.47 us
  transfers between devices with their start and end apart: 7, of which 4 were waited for; matrix products, arithmetic and copies ran while one was open for 2% of the time, Pallas kernels for 6%

profile of v1, /device:TPU:1, one launch (start us, length us, event | category | flops | bytes accessed | tf_op | source)
XLA Modules:
  0.0 190.3 jit_solution(3066559271959848406)
XLA Ops:
  2.1 3.9 %collective-permute-start = (bf16[8,1536]{1,0:T(8,128)(2,1)S(1)}, bf16[8,1536]{1,0:T(8,128)(2,1)S(1)}, u32[]{:S(2)}, u32[]{:S(2)}) collective-permute-start(bf16[8,1536]{1,0:T(8,128)(2,1)S(1)} %pad_maximum_fusion), channel_id=1, source_target_pairs={{0,2},{2,4},{4,6},{6,8},{8,10},{10,12},{12,14},{14,16},{16,18},{18... | collective-permute-start | bytes 73736 | tf_op jit(solution)/shard_map/ppermute | solution.py:338
  6.0 1.5 copy.26.pld_ref
  7.5 1.4 copy.25.dt_ref
  9.5 4.7 %front.1 = (f32[256,1024]{1,0:T(8,128)}, bf16[256,256]{1,0:T(8,128)(2,1)}, bf16[256,256]{1,0:T(8,128)(2,1)}, f32[256,128]{1,0:T(8,128)}, f32[256,128]{1,0:T(8,12...) custom-call(bf16[256,1024]{1,0:T(8,128)(2,1)} %x_ref.1, bf16[256,256]{1,0:T(8,128)(2,1)} %b_ref.1, ...), custom_call_target="tpu_custom_call" | custom-call | tf_op jit(solution)/shard_map/front/pallas_call | solution.py:339
  14.3 14.4 %all_to_all.44 = bf16[16,8,1152]{2,1,0:T(8,128)(2,1)} all-to-all(bf16[16,8,1152]{2,1,0:T(8,128)(2,1)} %bitcast.21), channel_id=1, replica_groups=mesh['sp_0'=4,'sp_1'=4,'sp_2'=4,'tp'=2] {'sp_1','sp_2'}, dimensions={0} | all-to-all | bytes 589824 | tf_op jit(solution)/shard_map/all_to_all | solution.py:352
  28.6 2.0 %plane.1 = (f32[128,1024]{1,0:T(8,128)}, f32[16,1024]{1,0:T(8,128)}, f32[8,1152]{1,0:T(8,128)}) custom-call(bf16[128,1152]{1,0:T(8,128)(2,1)} %bitcast.18), custom_call_target="tpu_custom_call" | custom-call | tf_op jit(solution)/shard_map/plane/pallas_call | solution.py:360
  30.7 4.0 %collective-permute-start.1 = (f32[8,1152]{1,0:T(8,128)}, f32[8,1152]{1,0:T(8,128)S(1)}, u32[]{:S(2)}, u32[]{:S(2)}) collective-permute-start(f32[8,1152]{1,0:T(8,128)} %get-tuple-element.29), channel_id=1, source_target_pairs={{0,32},{32,64},{64,96},{1,33},{33,65},{65,97},{2,34},{34,66},{66,9... | collective-permute-start | bytes 110600 | tf_op jit(solution)/shard_map/ppermute | solution.py:366
  34.7 5.2 %collective-permute-start.2 = (f32[8,1152]{1,0:T(8,128)}, f32[8,1152]{1,0:T(8,128)S(1)}, u32[]{:S(2)}, u32[]{:S(2)}) collective-permute-start(f32[8,1152]{1,0:T(8,128)} %get-tuple-element.29), channel_id=1, source_target_pairs={{0,64},{32,96},{1,65},{33,97},{2,66},{34,98},{3,67},{35,99},{4,68}... | collective-permute-start | bytes 110600 | tf_op jit(solution)/shard_map/ppermute | solution.py:366
  39.9 1.3 collective-permute-start.3
  41.3 1.3 collective-permute-done.3.three_ref
  43.2 2.1 %planes.1 = bf16[128,1024]{1,0:T(8,128)(2,1)} custom-call(f32[128,1024]{1,0:T(8,128)} %get-tuple-element.27.pin_ref, f32[16,1024]{1,0:T(8,128)} %get-tuple-element.28.pdec_ref, f32[8,1152]{1,0:T(8,128)} %copy-done.3, f32[8,1152]{1,0:T(8,128)} %copy-done.4, f32[8,1152]{1,0:T(8,128)} %copy-done.5), custom_call_target="tpu_custom_call" | custom-call | tf_op jit(solution)/shard_map/planes/pallas_call | solution.py:367
  45.3 3.5 %all-to-all-start.1 = ((bf16[16,8,1024]{2,1,0:T(8,128)(2,1)}), bf16[16,8,1024]{2,1,0:T(8,128)(2,1)S(1)}, u32[]{:S(2)}, u32[]{:S(2)}) async-start(bf16[16,8,1024]{2,1,0:T(8,128)(2,1)} %bitcast.20), calls=%async_computation.1 | async-start | bytes 524288 | tf_op jit(solution)/shard_map/all_to_all | solution.py:368
  48.8 4.0 %near.1.y_ref = f32[256,1024]{1,0:T(8,128)} custom-call(f32[256,1024]{1,0:T(8,128)} %get-tuple-element.20.sig_ref, bf16[256,256]{1,0:T(8,128)(2,1)} %get-tuple-element.21.wv_ref, bf16[256,256]{1,0:T(8,128)(2,1)} %get-tuple-element.22.rv_ref, f32[256,128]{1,0:T(8,128)} %get-tuple-element.23.cum_ref, f32[256,128]{1,0:T(8,128)} %get-tuple-element.24.dtv_ref, ...), custom_call_target="tpu_custom_call" | custom-call | flops 400000000 | bytes 4000000 | tf_op jit(solution)/shard_map/near/pallas_call | solution.py:353
  52.8 3.5 %all-to-all-done.1 = bf16[16,8,1024]{2,1,0:T(8,128)(2,1)S(1)} async-done(((bf16[16,8,1024]{2,1,0:T(8,128)(2,1)}), bf16[16,8,1024]{2,1,0:T(8,128)(2,1)S(1)}, u32[]{:S(2)}, u32[]{:S(2)}) %all-to-all-start.1) | async-done | bytes 262176 | tf_op jit(solution)/shard_map/all_to_all | solution.py:368
  57.0 6.5 %project.1 = (f32[128,2048]{1,0:T(8,128)}, bf16[128,2048]{1,0:T(8,128)(2,1)}) custom-call(s32[1]{0:T(128)} %bitcast.half_ref, f32[256,1024]{1,0:T(8,128)} %near.1.y_ref, bf16[128,1024]{1,0:T(8,128)(2,1)} %bitcast.19, bf16[256,256]{1,0:T(8,128)(2,1)} %get-tuple-element.22.rv_ref, f32[256,128]{1,0:T(8,128)} %get-tuple-element.23.cum_ref, ...), custom_call_target="tpu_custom_call" | custom-call | tf_op jit(solution)/shard_map/project/pallas_call | solution.py:372
  63.5 5.1 %collective-permute-start.4 = (bf16[128,2048]{1,0:T(8,128)(2,1)}, bf16[128,2048]{1,0:T(8,128)(2,1)S(1)}, u32[]{:S(2)}, u32[]{:S(2)}) collective-permute-start(bf16[128,2048]{1,0:T(8,128)(2,1)} %get-tuple-element.31), channel_id=1, source_target_pairs={{0,1},{1,0},{2,3},{3,2},{4,5},{5,4},{6,7},{7,6},{8,9},{9,8},{10,11... | collective-permute-start | bytes 1572872 | tf_op jit(solution)/shard_map/ppermute | solution.py:385
  71.1 5.1 %dispatch.1 = (bf16[128,2048]{1,0:T(8,128)(2,1)}, bf16[128,2048]{1,0:T(8,128)(2,1)}, bf16[1024,1536]{1,0:T(8,128)(2,1)}) custom-call(f32[128,2048]{1,0:T(8,128)} %get-tuple-element.30.own_ref, bf16[128,2048]{1,0:T(8,128)(2,1)} %copy-done.2, bf16[128,2048]{1,0:T(8,128)(2,1)} %stream_ref.1, f32[1,2048]{1,0:T(1,128)} %bitcast.22, s32[128,4]{1,0:T(8,128)} %copy.27.chosen_ref), custom_call_target="tpu_custom_call" | custom-call | tf_op jit(solution)/shard_map/dispatch/pallas_call | solution.py:387
  76.2 47.4 %all_to_all.45 = bf16[128,8,1536]{2,1,0:T(8,128)(2,1)} all-to-all(bf16[128,8,1536]{2,1,0:T(8,128)(2,1)} %bitcast.17), channel_id=1, replica_groups=mesh['sp_0'=4,'sp_1'=4,'sp_2'=4,'tp'=2] {'sp_0','sp_1','sp_2','tp'}, dimensions={0} | all-to-all | bytes 6291456 | tf_op jit(solution)/shard_map/all_to_all | solution.py:393
  123.6 13.3 %experts.1 = bf16[1024,1536]{1,0:T(8,128)(2,1)} custom-call(bf16[1024,1536]{1,0:T(8,128)(2,1)} %bitcast.16, bf16[1,2048,512]{2,1,0:T(8,128)(2,1)} %gate_ref.4, bf16[1,2048,512]{2,1,0:T(8,128)(2,1)} %up_ref.2, bf16[1,512,2048]{2,1,0:T(8,128)(2,1)} %down_ref.2), custom_call_target="tpu_custom_call" | custom-call | tf_op jit(solution)/shard_map/experts/pallas_call | solution.py:411
  137.0 4.8 %all-to-all-start.3 = ((bf16[128,8,1536]{2,1,0:T(8,128)(2,1)}), bf16[128,8,1536]{2,1,0:T(8,128)(2,1)S(1)}, u32[]{:S(2)}, u32[]{:S(2)}) async-start(bf16[128,8,1536]{2,1,0:T(8,128)(2,1)} %bitcast.15), calls=%async_computation.3 | async-start | bytes 6291456 | tf_op jit(solution)/shard_map/all_to_all | solution.py:425
  142.5 6.5 %shared.1.base_ref = f32[128,2048]{1,0:T(8,128)} custom-call(bf16[128,2048]{1,0:T(8,128)(2,1)} %get-tuple-element.33.normed_ref, bf16[128,2048]{1,0:T(8,128)(2,1)} %get-tuple-element.34.residual_ref, bf16[2048,512]{1,0:T(8,128)(2,1)} %gate_ref.5, bf16[2048,512]{1,0:T(8,128)(2,1)} %up_ref.3, bf16[512,2048]{1,0:T(8,128)(2,1)} %down_ref.3), custom_call_target="tpu_custom_call" | custom-call | flops 800000000 | bytes 8000000 | tf_op jit(solution)/shard_map/shared/pallas_call | solution.py:396
  149.0 34.4 %all-to-all-done.3 = bf16[128,8,1536]{2,1,0:T(8,128)(2,1)S(1)} async-done(((bf16[128,8,1536]{2,1,0:T(8,128)(2,1)}), bf16[128,8,1536]{2,1,0:T(8,128)(2,1)S(1)}, u32[]{:S(2)}, u32[]{:S(2)}) %all-to-all-start.3) | async-done | bytes 3145760 | tf_op jit(solution)/shard_map/all_to_all | solution.py:425
  183.4 1.6 copy-done
  185.0 5.3 %combine.1 = bf16[128,2048]{1,0:T(8,128)(2,1)} custom-call(bf16[1024,1536]{1,0:T(8,128)(2,1)} %bitcast.14, f32[128,2048]{1,0:T(8,128)} %shared.1.base_ref, s32[128,4]{1,0:T(8,128)} %copy.27.chosen_ref, f32[128,4]{1,0:T(8,128)} %copy.29.weight_ref), custom_call_target="tpu_custom_call" | custom-call | tf_op jit(solution)/shard_map/combine/pallas_call | solution.py:428
  (27 shorter events, 7.3 us)
Async XLA Ops:
  2.1 6.8 %collective-permute-start = (bf16[8,1536]{1,0:T(8,128)(2,1)S(1)}, bf16[8,1536]{1,0:T(8,128)(2,1)S(1)}, u32[]{:S(2)}, u32[]{:S(2)}) collective-permute-start(bf16[8,1536]{1,0:T(8,128)(2,1)S(1)} %pad_maximum_fusion), channel_id=1, source_target_pairs={{0,2},{2,4},{4,6},{6,8},{8,10},{10,12},{12,14},{14,16},{16,18},{18... | collective-permute-start | bytes 73736 | tf_op jit(solution)/shard_map/ppermute | solution.py:338
  8.9 0.6 copy-start.6
  30.7 10.6 %collective-permute-start.1 = (f32[8,1152]{1,0:T(8,128)}, f32[8,1152]{1,0:T(8,128)S(1)}, u32[]{:S(2)}, u32[]{:S(2)}) collective-permute-start(f32[8,1152]{1,0:T(8,128)} %get-tuple-element.29), channel_id=1, source_target_pairs={{0,32},{32,64},{64,96},{1,33},{33,65},{65,97},{2,34},{34,66},{66,9... | collective-permute-start | bytes 110600 | tf_op jit(solution)/shard_map/ppermute | solution.py:366
  34.7 6.6 %collective-permute-start.2 = (f32[8,1152]{1,0:T(8,128)}, f32[8,1152]{1,0:T(8,128)S(1)}, u32[]{:S(2)}, u32[]{:S(2)}) collective-permute-start(f32[8,1152]{1,0:T(8,128)} %get-tuple-element.29), channel_id=1, source_target_pairs={{0,64},{32,96},{1,65},{33,97},{2,66},{34,98},{3,67},{35,99},{4,68}... | collective-permute-start | bytes 110600 | tf_op jit(solution)/shard_map/ppermute | solution.py:366
  39.9 2.7 %collective-permute-start.3 = (f32[8,1152]{1,0:T(8,128)}, f32[8,1152]{1,0:T(8,128)S(1)}, u32[]{:S(2)}, u32[]{:S(2)}) collective-permute-start(f32[8,1152]{1,0:T(8,128)} %get-tuple-element.29), channel_id=1, source_target_pairs={{0,96},{1,97},{2,98},{3,99},{4,100},{5,101},{6,102},{7,103},{8,104... | collective-permute-start | bytes 110600 | tf_op jit(solution)/shard_map/ppermute | solution.py:366
  41.2 1.4 copy-start.3
  41.3 1.3 copy-start.4
  42.6 0.6 copy-start.5
  45.3 11.0 %all-to-all-start.1 = ((bf16[16,8,1024]{2,1,0:T(8,128)(2,1)}), bf16[16,8,1024]{2,1,0:T(8,128)(2,1)S(1)}, u32[]{:S(2)}, u32[]{:S(2)}) async-start(bf16[16,8,1024]{2,1,0:T(8,128)(2,1)} %bitcast.20), calls=%async_computation.1 | async-start | bytes 524288 | tf_op jit(solution)/shard_map/all_to_all | solution.py:368
  56.3 0.7 copy-start.1
  57.0 11.6 %copy-start.7 = (s32[128,4]{0,1:T(4,128)S(1)}, s32[128,4]{0,1:T(4,128)}, u32[]{:S(2)}) copy-start(s32[128,4]{0,1:T(4,128)} %param.40) | copy-start | bytes 6148
  63.5 6.8 %collective-permute-start.4 = (bf16[128,2048]{1,0:T(8,128)(2,1)}, bf16[128,2048]{1,0:T(8,128)(2,1)S(1)}, u32[]{:S(2)}, u32[]{:S(2)}) collective-permute-start(bf16[128,2048]{1,0:T(8,128)(2,1)} %get-tuple-element.31), channel_id=1, source_target_pairs={{0,1},{1,0},{2,3},{3,2},{4,5},{5,4},{6,7},{7,6},{8,9},{9,8},{10,11... | collective-permute-start | bytes 1572872 | tf_op jit(solution)/shard_map/ppermute | solution.py:385
  70.3 0.8 copy-start.2
  137.0 4.8 %copy-start.8 = (f32[128,4]{0,1:T(4,128)S(1)}, f32[128,4]{0,1:T(4,128)}, u32[]{:S(2)}) copy-start(f32[128,4]{0,1:T(4,128)} %param.41) | copy-start | bytes 6148
  137.0 46.4 %all-to-all-start.3 = ((bf16[128,8,1536]{2,1,0:T(8,128)(2,1)}), bf16[128,8,1536]{2,1,0:T(8,128)(2,1)S(1)}, u32[]{:S(2)}, u32[]{:S(2)}) async-start(bf16[128,8,1536]{2,1,0:T(8,128)(2,1)} %bitcast.15), calls=%async_computation.3 | async-start | bytes 6291456 | tf_op jit(solution)/shard_map/all_to_all | solution.py:425
  183.4 1.6 copy-start

commit v2 on v1

v2 whole, which is shorter than its diff:
```python
import jax
import jax.numpy as jnp
from jax import lax
from jax.experimental import pallas as pl
from jax.experimental.pallas import tpu as pltpu
from jax.sharding import Mesh
from jax.sharding import PartitionSpec as P

HEAD_DIM = 64
STATE = 128
BLK = 128
HEAD = 16
LANES = 128
SLOTS = 6
WIDE = 8
SP = ("sp_0", "sp_1", "sp_2")
PLANE = ("sp_1", "sp_2")
SP_TP = ("sp_0", "sp_1", "sp_2", "tp")
F32 = jnp.float32
BF16 = jnp.bfloat16


def mm(a, b, dims=((1,), (0,)), precision=None):
    return lax.dot_general(a, b, (dims, ((), ())), precision=precision, preferred_element_type=F32)


def iota(shape, dim):
    return lax.broadcasted_iota(jnp.int32, shape, dim)


def head_lanes(width):
    return jnp.where(iota((LANES, width), 1) // HEAD_DIM == iota((LANES, width), 0), 1.0, 0.0).astype(BF16)


def spread(values, lanes):
    high = values.astype(BF16)
    low = (values - high.astype(F32)).astype(BF16)
    return mm(high, lanes) + mm(low, lanes)


def silu(v):
    return v * (1.0 / (1.0 + jnp.exp(-v)))


def onchip(count):
    return [pl.BlockSpec(memory_space=pltpu.VMEM)] * count


def offchip(count):
    return [pl.BlockSpec(memory_space=pltpu.HBM)] * count


def stay(*arrays):
    return [pltpu.with_memory_space_constraint(array, pltpu.HBM) for array in arrays]


def room(mebibytes):
    return pltpu.CompilerParams(vmem_limit_bytes=mebibytes << 20)


def whole(shape):
    return pl.BlockSpec(shape, lambda *_: (0,) * len(shape))


def fetch(pairs, sems):
    copies = [pltpu.make_async_copy(src, dst, sems.at[i]) for i, (src, dst) in enumerate(pairs)]
    for copy in copies:
        copy.start()
    return copies


def rim_kernel(x_ref, b_ref, c_ref, out_ref, sems):
    start, pairs = 0, []
    for ref in (x_ref, b_ref, c_ref):
        rows, size = ref.shape
        pairs.append((ref.at[rows - 8 : rows, :], out_ref.at[:, start : start + size]))
        start += size
    for copy in fetch(pairs, sems):
        copy.wait()


def filtered(ext_ref, taps, lanes, first, count):
    total = taps[0:1] * ext_ref[first : first + count, lanes]
    for k in range(1, 4):
        total = total + taps[k : k + 1] * ext_ref[first + k : first + k + count, lanes]
    return silu(total)


def front_kernel(x_hbm, b_hbm, c_hbm, dt_hbm, pld_hbm, tx_hbm, tb_hbm, tc_hbm, bias_hbm, rate_hbm,
                 sig_ref, wv_ref, rv_ref, cum_ref, rows_ref, dtv_ref, s0_ref, s1_ref, begin_ref, taps_ref,
                 x_ref, b_ref, c_ref, dt_ref, pld_ref, tx_ref, tb_ref, tc_ref, bias_ref, rate_ref, ext_ref, wide_ref, sems):
    length, chans = x_ref.shape
    vecs = b_ref.shape[1]
    heads = dt_ref.shape[0]
    groups = vecs // STATE
    width = chans // groups
    copies = fetch((
        (bias_hbm, bias_ref), (rate_hbm, rate_ref), (dt_hbm, dt_ref), (pld_hbm, pld_ref), (tx_hbm, tx_ref), (tb_hbm, tb_ref),
        (tc_hbm, tc_ref), (b_hbm, b_ref), (c_hbm, c_ref), (x_hbm, x_ref),
    ), sems)
    for copy in copies[0:4]:
        copy.wait()
    wide_ref[...] = jnp.zeros_like(wide_ref)
    wide_ref[0:1, 0:heads] = bias_ref[...]
    wide_ref[1:2, 0:heads] = rate_ref[...]
    columns = wide_ref[:, 0:LANES].T
    v = dt_ref[...].astype(F32) + columns[0:heads, 0:1]
    step = jnp.maximum(v, 0.0) + jnp.log(1.0 + jnp.exp(-jnp.abs(v)))
    logs = pld_ref[...] - columns[0:heads, 1:2] * step
    upper = jnp.where(iota((length, length), 0) <= iota((length, length), 1), 1.0, 0.0)
    sums = mm(logs, upper, precision=lax.Precision.HIGHEST)
    rows_ref[...] = sums
    wide_ref[0:heads, :] = step
    dtv_ref[...] = wide_ref[...].T
    wide_ref[0:heads, :] = sums
    cum = wide_ref[...].T
    cum_ref[...] = cum
    half_end, end = cum[BLK - 1 : BLK], cum[length - 1 : length]
    ends = jnp.where(iota((length, LANES), 0) < BLK, half_end, end)
    weights = jnp.where(iota((length, LANES), 0) < HEAD, 0.0, dtv_ref[...] * jnp.exp(ends - cum))
    scale = spread(weights, head_lanes(chans))
    for copy in copies[4:7]:
        copy.wait()
    taps_ref[...] = jnp.zeros_like(taps_ref)
    sources = (
        (b_ref, tb_ref, chans, vecs, wv_ref, copies[7]), (c_ref, tc_ref, chans + vecs, vecs, rv_ref, copies[8]),
        (x_ref, tx_ref, 0, chans, sig_ref, copies[9]),
    )
    ext_ref[0:8, :] = jnp.zeros((8, ext_ref.shape[1]), F32)
    for src, taps, start, size, dst, copy in sources:
        taps_ref[0:4, start : start + size] = taps[...].astype(F32)
        copy.wait()
        ext_ref[8 : 8 + length, start : start + size] = src[...].astype(F32)
        begin_ref[:, start : start + size] = src[0:HEAD, :].astype(F32)
        for at in range(0, size, 256):
            lanes = slice(start + at, start + at + 256)
            dst[:, at : at + 256] = filtered(ext_ref, taps_ref[:, lanes], lanes, 5, length).astype(dst.dtype)
    for g in range(groups):
        part = slice(g * width, (g + 1) * width)
        vec = slice(g * STATE, (g + 1) * STATE)
        scaled = (sig_ref[:, part] * scale[:, part]).astype(BF16)
        s0_ref[:, part] = mm(wv_ref[0:BLK, vec], scaled[0:BLK], ((0,), (0,)))
        s1_ref[:, part] = mm(wv_ref[BLK:length, vec], scaled[BLK:length], ((0,), (0,)))


def head_kernel(rim_ref, begin_ref, taps_ref, siga_ref, wva_ref, rva_ref, cum_ref, dtv_ref, s0a_ref, s1_ref,
                sig_ref, wv_ref, rv_ref, s0_ref, send_ref, ext_ref):
    length, chans = siga_ref.shape
    vecs = wva_ref.shape[1]
    groups = vecs // STATE
    width = chans // groups
    ext_ref[0:8, :] = rim_ref[...].astype(F32)
    ext_ref[8 : 8 + HEAD, :] = begin_ref[...]
    for start, size, old, new in ((0, chans, siga_ref, sig_ref), (chans, vecs, wva_ref, wv_ref), (chans + vecs, vecs, rva_ref, rv_ref)):
        lanes = slice(start, start + size)
        new[0:HEAD, :] = filtered(ext_ref, taps_ref[:, lanes], lanes, 5, HEAD).astype(new.dtype)
        new[HEAD:, :] = old[HEAD:, :]
    half_end, end = cum_ref[BLK - 1 : BLK, :], cum_ref[length - 1 : length, :]
    lanes = head_lanes(chans)
    scale = spread(dtv_ref[0:HEAD, :] * jnp.exp(half_end - cum_ref[0:HEAD, :]), lanes)
    passing = spread(jnp.broadcast_to(jnp.exp(end - half_end), (8, LANES)), lanes)[0:1]
    scaled = (sig_ref[0:HEAD, :] * scale).astype(BF16)
    for g in range(groups):
        part = slice(g * width, (g + 1) * width)
        first = s0a_ref[:, part] + mm(wv_ref[0:HEAD, g * STATE : (g + 1) * STATE], scaled[:, part], ((0,), (0,)))
        s0_ref[:, part] = first
        send_ref[:, part] = (first * passing[:, part] + s1_ref[:, part]).astype(BF16)
    high = end.astype(BF16).astype(F32)
    mid = (end - high).astype(BF16).astype(F32)
    low = (end - high - mid).astype(BF16).astype(F32)
    row = iota((STATE, LANES), 0) % 8
    send_ref[:, chans : chans + LANES] = jnp.where(
        row == 0, high, jnp.where(row == 1, mid, jnp.where(row == 2, low, 0.0))
    ).astype(BF16)


def plane_kernel(got_ref, pin_ref, pdec_ref, send_ref):
    count = got_ref.shape[0] // 8
    chans = got_ref.shape[1] - LANES
    logs = jnp.sum(got_ref[:, chans:].astype(F32).reshape(count, 8, LANES), axis=1)
    lanes = head_lanes(chans)
    decay = spread(jnp.exp(logs), lanes)
    state = jnp.zeros((8, chans), F32)
    sofar = jnp.zeros((1, LANES), F32)
    before = []
    for i in range(count):
        pin_ref[8 * i : 8 * i + 8, :] = state
        before.append(sofar)
        state = state * decay[i : i + 1] + got_ref[8 * i : 8 * i + 8, 0:chans].astype(F32)
        sofar = sofar + logs[i : i + 1]
    pdec_ref[...] = spread(jnp.exp(jnp.concatenate(before, axis=0)), lanes)
    send_ref[:, 0:chans] = state
    send_ref[:, chans:] = jnp.broadcast_to(sofar, (8, LANES))


def planes_kernel(pin_ref, pdec_ref, one_ref, two_ref, three_ref, out_ref):
    chans = pin_ref.shape[1]
    count = pin_ref.shape[0] // 8
    lanes = head_lanes(chans)
    near = spread(jnp.exp(one_ref[:, chans:]), lanes)
    far = spread(jnp.exp(two_ref[:, chans:]), lanes)
    state = one_ref[:, 0:chans] + near * (two_ref[:, 0:chans] + far * three_ref[:, 0:chans])
    for i in range(0, count, 2):
        pair = [pin_ref[8 * k : 8 * k + 8, :] + state * pdec_ref[k : k + 1, :] for k in (i, i + 1)]
        out_ref[8 * i : 8 * i + 16, :] = jnp.concatenate(pair, axis=0).astype(BF16)


def near_kernel(sig_ref, wv_ref, rv_ref, cum_ref, rows_ref, dtv_ref, s0_ref, direct_ref, y_ref, pad_ref):
    length, chans = sig_ref.shape
    heads = direct_ref.shape[1]
    groups = wv_ref.shape[1] // STATE
    width = chans // groups
    lanes = head_lanes(chans)
    cum = cum_ref[...]
    cum_rows = rows_ref[...]
    pad_ref[...] = jnp.zeros_like(pad_ref)
    pad_ref[:, 0:heads] = jnp.broadcast_to(direct_ref[...], (8, heads))
    direct = spread(pad_ref[...], lanes)[0:1]
    scaled = (sig_ref[...] * spread(dtv_ref[...], lanes)).astype(BF16)
    causal = iota((BLK, BLK), 0) >= iota((BLK, BLK), 1)
    left = iota((BLK, LANES), 1) < HEAD_DIM
    into = spread(jnp.exp(cum[BLK:length] - cum[BLK - 1 : BLK]), lanes)
    for b in range(length // BLK):
        rows = slice(b * BLK, (b + 1) * BLK)
        for g in range(groups):
            vec = slice(g * STATE, (g + 1) * STATE)
            part = slice(g * width, (g + 1) * width)
            products = mm(rv_ref[rows, vec], wv_ref[rows, vec], ((1,), (1,)))
            if b == 1:
                carried = mm(rv_ref[rows, vec], s0_ref[:, part].astype(BF16)) * into[:, part]
            for j in range(width // LANES):
                at = g * width + j * LANES
                mats = []
                for h in (at // HEAD_DIM, at // HEAD_DIM + 1):
                    gap = cum[rows, h : h + 1] - cum_rows[h : h + 1, rows]
                    mats.append((products * jnp.exp(jnp.where(causal, gap, -1e30))).astype(BF16))
                pair = scaled[rows, at : at + LANES]
                zero = jnp.zeros_like(pair)
                stacked = jnp.concatenate([jnp.where(left, pair, zero), jnp.where(left, zero, pair)], axis=0)
                out = mm(jnp.concatenate(mats, axis=1), stacked)
                out = out + direct[:, at : at + LANES] * sig_ref[rows, at : at + LANES]
                if b == 1:
                    out = out + carried[:, j * LANES : (j + 1) * LANES]
                y_ref[rows, at : at + LANES] = out


def project_kernel(half_ref, y_ref, state_ref, rv_ref, cum_ref, gate_hbm, gain_hbm, w_hbm, own_ref, other_ref,
                   gate_ref, gain_ref, w_ref, mix_ref, res_ref, sems):
    length, chans = y_ref.shape
    groups = rv_ref.shape[1] // STATE
    width = chans // groups
    rows = own_ref.shape[0]
    dim = own_ref.shape[1]
    parts = 4
    pairs = [(gate_hbm, gate_ref), (gain_hbm, gain_ref)]
    for k in range(parts):
        part = pl.ds(k * (dim // parts), dim // parts)
        pairs.append((w_hbm.at[:, part], w_ref.at[:, part]))
    copies = fetch(pairs, sems)
    scale = spread(jnp.exp(cum_ref[...]), head_lanes(chans))
    for g in range(groups):
        part = slice(g * width, (g + 1) * width)
        far = mm(rv_ref[:, g * STATE : (g + 1) * STATE], state_ref[:, part])
        inner = y_ref[:, part] + far * scale[:, part]
        if g == 0:
            copies[0].wait()
            copies[1].wait()
        gated = inner * silu(gate_ref[:, part].astype(F32))
        mean = jnp.sum(gated * gated, axis=1, keepdims=True) * (1.0 / width)
        mix_ref[:, part] = (gated * lax.rsqrt(mean + 1e-06) * gain_ref[:, part]).astype(BF16)
    half = half_ref[0]
    for k in range(parts):
        part = slice(k * (dim // parts), (k + 1) * (dim // parts))
        copies[2 + k].wait()
        res_ref[...] = mm(mix_ref[...], w_ref[:, part])
        own_ref[:, part] = res_ref[pl.ds(pl.multiple_of(half * rows, rows), rows), :]
        other_ref[:, part] = res_ref[pl.ds(pl.multiple_of((1 - half) * rows, rows), rows), :].astype(BF16)


def slot_table(chosen, experts):
    count = chosen.shape[1]
    expert = iota((experts, count), 0)
    named = jnp.zeros((experts, count), F32)
    for k in range(chosen.shape[0]):
        named = named + jnp.where(chosen[k : k + 1, :] == expert, 1.0, 0.0)
    earlier = jnp.where(iota((count, count), 0) < iota((count, count), 1), 1.0, 0.0).astype(BF16)
    return named * (mm(named.astype(BF16), earlier) + 1.0)


def expert_rows(experts):
    return jnp.where(iota((experts * WIDE, experts), 0) // WIDE == iota((experts * WIDE, experts), 1), 1.0, 0.0).astype(BF16)


def dispatch_kernel(own_ref, got_ref, stream_hbm, gain_hbm, chosen_ref, residual_ref, normed_ref, out_ref,
                    stream_ref, gain_ref, both_ref, sems):
    rows, dim = own_ref.shape
    third = out_ref.shape[1] // 3
    experts = out_ref.shape[0] // WIDE
    copies = fetch(((stream_hbm, stream_ref), (gain_hbm, gain_ref)), sems)
    table = slot_table(chosen_ref[...], experts)
    slots = mm(expert_rows(experts), table.astype(BF16))
    place = (iota(slots.shape, 0) % WIDE).astype(F32)
    both_ref[:, 0:rows] = jnp.where(slots == place + 1.0, 1.0, 0.0).astype(BF16)
    for q in range(3):
        tail = jnp.where((place >= 6.0) & (slots == 3.0 * place + (q - 17.0)), 1.0, 0.0)
        both_ref[:, rows * (q + 1) : rows * (q + 2)] = tail.astype(BF16)
    for copy in copies:
        copy.wait()
    residual = (stream_ref[...].astype(F32) + own_ref[...] + got_ref[...].astype(F32)).astype(BF16)
    residual_ref[...] = residual
    wide = residual.astype(F32)
    mean = jnp.sum(wide * wide, axis=1, keepdims=True) * (1.0 / dim)
    normed_ref[...] = (wide * lax.rsqrt(mean + 1e-06) * gain_ref[...]).astype(BF16)
    main = both_ref[:, 0:rows]
    for q in range(3):
        mats = jnp.concatenate([main, both_ref[:, rows * (q + 1) : rows * (q + 2)]], axis=1)
        source = jnp.concatenate([normed_ref[:, q * third : (q + 1) * third], normed_ref[:, 3 * third :]], axis=0)
        out_ref[:, q * third : (q + 1) * third] = mm(mats, source).astype(BF16)


def shared_kernel(normed_ref, residual_ref, gate_ref, up_ref, down_ref, chosen_ref, weight_ref, out_ref, mats_ref):
    @pl.when(pl.program_id(0) == 0)
    def _():
        out_ref[...] = residual_ref[...].astype(F32)
        rows = normed_ref.shape[0]
        experts = mats_ref.shape[1] // WIDE
        chosen = chosen_ref[...]
        expert = iota((experts, rows), 0)
        weights = jnp.zeros((experts, rows), F32)
        for k in range(chosen.shape[0]):
            weights = weights + jnp.where(chosen[k : k + 1, :] == expert, weight_ref[k : k + 1, :], 0.0)
        lanes = expert_rows(experts)
        slots = mm(slot_table(chosen, experts).T.astype(BF16), lanes, ((1,), (1,)))
        spread_weights = mm(weights.T.astype(BF16), lanes, ((1,), (1,)))
        place = (iota(slots.shape, 1) % WIDE).astype(F32)
        mats_ref[0:rows, :] = jnp.where(slots == place + 1.0, spread_weights, 0.0).astype(BF16)
        for k in range(3):
            hit = (place >= 6.0) & (slots == 3.0 * place + (k - 17.0))
            mats_ref[rows * (k + 1) : rows * (k + 2), :] = jnp.where(hit, spread_weights, 0.0).astype(BF16)

    normed = normed_ref[...]
    hidden = (silu(mm(normed, gate_ref[...])) * mm(normed, up_ref[...])).astype(BF16)
    out_ref[...] += mm(hidden, down_ref[...])


def expert_kernel(x_ref, gate_ref, up_ref, down_ref, out_hbm, full_ref, out_ref, sems):
    total, wide = x_ref.shape
    third = wide // 3
    rows = out_ref.shape[1]
    row, col = iota((LANES, LANES), 0), iota((LANES, LANES), 1)
    same = row // WIDE == col // WIDE
    r, c = row % WIDE, col % WIDE
    unpack = [jnp.where(same & (c >= 6) & (r == 3 * (c - 6) + q), 1.0, 0.0).astype(BF16) for q in range(3)]
    pack = [jnp.where(same & (r >= 6) & (c == 3 * (r - 6) + q), 1.0, 0.0).astype(BF16) for q in range(3)]
    unpack, pack = jnp.concatenate(unpack, axis=1), jnp.concatenate(pack, axis=0)
    within = iota((LANES, third), 0) % WIDE < SLOTS
    copies = []
    for n in range(total // rows):
        base = n * rows
        full_ref[:, 0:wide] = x_ref[base : base + rows, :]
        for at in range(0, rows, LANES):
            pieces = [x_ref[base + at : base + at + LANES, q * third : (q + 1) * third] for q in range(3)]
            full_ref[at : at + LANES, wide:] = mm(unpack, jnp.concatenate(pieces, axis=0)).astype(BF16)
        full = full_ref[...]
        hidden = (silu(mm(full, gate_ref[...])) * mm(full, up_ref[...])).astype(BF16)
        tail = mm(hidden, down_ref[:, wide:]).astype(BF16)
        packed = [mm(pack, tail[at : at + LANES]) for at in range(0, rows, LANES)]
        for q in range(3):
            part = slice(q * third, (q + 1) * third)
            result = mm(hidden, down_ref[:, part])
            for k, at in enumerate(range(0, rows, LANES)):
                extra = packed[k][q * LANES : (q + 1) * LANES]
                out_ref[n, at : at + LANES, part] = jnp.where(within, result[at : at + LANES], extra).astype(BF16)
        copy = pltpu.make_async_copy(out_ref.at[n], out_hbm.at[base : base + rows, :], sems.at[n])
        copy.start()
        copies.append(copy)
    for copy in copies:
        copy.wait()


def combine_kernel(got_ref, base_hbm, mats_hbm, out_ref, base_ref, mats_ref, sems):
    rows, dim = base_ref.shape
    third = got_ref.shape[1] // 3
    copies = fetch(((mats_hbm, mats_ref), (base_hbm, base_ref)), sems)
    tail = jnp.zeros((rows, third), F32)
    copies[0].wait()
    for q in range(3):
        part = slice(q * third, (q + 1) * third)
        got = got_ref[:, part]
        main = mm(mats_ref[0:rows, :], got)
        tail = tail + mm(mats_ref[rows * (q + 1) : rows * (q + 2), :], got)
        if q == 0:
            copies[1].wait()
        out_ref[:, part] = (base_ref[:, part] + main).astype(BF16)
    out_ref[:, 3 * third :] = (base_ref[:, 3 * third :] + tail).astype(BF16)


def shape(dims, dtype=F32):
    return jax.ShapeDtypeStruct(dims, dtype)


def on_device(
    stream,
    head_input_signal,
    write_input_vectors,
    read_input_vectors,
    output_gate_input,
    step_size_input,
    position_log_decay,
    signal_filter_taps,
    write_filter_taps,
    read_filter_taps,
    step_size_bias,
    head_decay_rate,
    head_direct_term,
    grouped_norm_gain,
    mixer_output_weight,
    expert_norm_gain,
    chosen_expert_index,
    chosen_expert_weight,
    routed_gate_weight,
    routed_up_weight,
    routed_down_weight,
    common_gate_weight,
    common_up_weight,
    common_down_weight,
):
    length, chans = head_input_signal.shape
    vecs = write_input_vectors.shape[1]
    rows, dim = stream.shape
    hidden = common_gate_weight.shape[1]
    experts = lax.axis_size(SP_TP)
    wide = dim * SLOTS // WIDE

    heads = step_size_input.shape[1]
    devices = lax.axis_size(SP)
    rim = pl.pallas_call(
        rim_kernel,
        in_specs=offchip(3),
        out_specs=onchip(1)[0],
        out_shape=shape((8, chans + 2 * vecs), BF16),
        scratch_shapes=[pltpu.SemaphoreType.DMA((3,))],
        compiler_params=room(2),
        name="rim",
    )(*stay(head_input_signal, write_input_vectors, read_input_vectors))
    rim = lax.ppermute(rim, SP, [(i, i + 1) for i in range(devices - 1)])
    signal, write_rows, read_rows, cum, cum_rows, dtv, first, second, begin, taps = pl.pallas_call(
        front_kernel,
        in_specs=offchip(10),
        out_specs=tuple(onchip(10)),
        out_shape=(
            shape((length, chans)), shape((length, vecs), BF16), shape((length, vecs), BF16), shape((length, LANES)),
            shape((heads, length)), shape((length, LANES)), shape((STATE, chans)), shape((STATE, chans)),
            shape((HEAD, chans + 2 * vecs)), shape((8, chans + 2 * vecs)),
        ),
        scratch_shapes=[
            pltpu.VMEM((length, chans), BF16), pltpu.VMEM((length, vecs), BF16), pltpu.VMEM((length, vecs), BF16),
            pltpu.VMEM((heads, length), BF16), pltpu.VMEM((heads, length), F32),
            pltpu.VMEM((4, chans), BF16), pltpu.VMEM((4, vecs), BF16), pltpu.VMEM((4, vecs), BF16),
            pltpu.VMEM((1, heads), F32), pltpu.VMEM((1, heads), F32),
            pltpu.VMEM((length + 8, chans + 2 * vecs), F32), pltpu.VMEM((LANES, length), F32),
            pltpu.SemaphoreType.DMA((10,)),
        ],
        cost_estimate=pl.CostEstimate(flops=800_000_000, transcendentals=1_000_000, bytes_accessed=4_000_000),
        compiler_params=room(14),
        name="front",
    )(*stay(
        head_input_signal, write_input_vectors, read_input_vectors, step_size_input.T, position_log_decay.T,
        signal_filter_taps, write_filter_taps, read_filter_taps, step_size_bias[None], head_decay_rate[None],
    ))
    sig, wv, rv, s0, send = pl.pallas_call(
        head_kernel,
        in_specs=onchip(10),
        out_specs=tuple(onchip(5)),
        out_shape=(
            shape((length, chans)), shape((length, vecs), BF16), shape((length, vecs), BF16),
            shape((STATE, chans)), shape((STATE, chans + LANES), BF16),
        ),
        scratch_shapes=[pltpu.VMEM((HEAD + 8, chans + 2 * vecs), F32)],
        compiler_params=room(8),
        name="head",
    )(rim, begin, taps, signal, write_rows, read_rows, cum, dtv, first, second)
    in_plane = lax.axis_size(PLANE)
    got = lax.all_to_all(send, PLANE, split_axis=0, concat_axis=0, tiled=True)
    near = pl.pallas_call(
        near_kernel,
        in_specs=onchip(8),
        out_specs=onchip(1)[0],
        out_shape=shape((length, chans)),
        scratch_shapes=[pltpu.VMEM((8, LANES), F32)],
        cost_estimate=pl.CostEstimate(flops=400_000_000, transcendentals=1_000_000, bytes_accessed=4_000_000),
        compiler_params=room(12),
        name="near",
    )(sig, wv, rv, cum, cum_rows, dtv, s0, head_direct_term[None])
    pin, pdec, total = pl.pallas_call(
        plane_kernel,
        in_specs=onchip(1),
        out_specs=tuple(onchip(3)),
        out_shape=(shape((STATE, chans)), shape((in_plane, chans)), shape((STATE // in_plane, chans + LANES))),
        compiler_params=room(6),
        name="plane",
    )(got)
    planes = lax.axis_size("sp_0")
    lower = [lax.ppermute(total, "sp_0", [(i, i + s) for i in range(planes - s)]) for s in (1, 2, 3)]
    back = pl.pallas_call(
        planes_kernel,
        in_specs=onchip(5),
        out_specs=onchip(1)[0],
        out_shape=shape((STATE, chans), BF16),
        compiler_params=room(6),
        name="planes",
    )(pin, pdec, *lower)
    incoming = lax.all_to_all(back, PLANE, split_axis=0, concat_axis=0, tiled=True)

    half = lax.axis_index("tp").astype(jnp.int32).reshape(1)
    own, other = pl.pallas_call(
        project_kernel,
        in_specs=[pl.BlockSpec(memory_space=pltpu.SMEM)] + onchip(4) + offchip(3),
        out_specs=tuple(onchip(2)),
        out_shape=(shape((rows, dim)), shape((rows, dim), BF16)),
        scratch_shapes=[
            pltpu.VMEM((length, chans), BF16), pltpu.VMEM((1, chans), F32), pltpu.VMEM((chans, dim), BF16),
            pltpu.VMEM((length, chans), BF16), pltpu.VMEM((length, dim // 4), F32), pltpu.SemaphoreType.DMA((6,)),
        ],
        compiler_params=room(16),
        name="project",
    )(half, near, incoming, rv, cum, *stay(output_gate_input, grouped_norm_gain[None], mixer_output_weight))
    partner = lax.ppermute(other, "tp", [(0, 1), (1, 0)])

    chosen = chosen_expert_index.T
    residual, normed, outgoing = pl.pallas_call(
        dispatch_kernel,
        in_specs=onchip(2) + offchip(2) + onchip(1),
        out_specs=tuple(onchip(3)),
        out_shape=(shape((rows, dim), BF16), shape((rows, dim), BF16), shape((experts * WIDE, wide), BF16)),
        scratch_shapes=[
            pltpu.VMEM((rows, dim), BF16), pltpu.VMEM((1, dim), F32), pltpu.VMEM((experts * WIDE, 4 * rows), BF16),
            pltpu.SemaphoreType.DMA((2,)),
        ],
        compiler_params=room(14),
        name="dispatch",
    )(own, partner, *stay(stream, expert_norm_gain[None]), chosen)
    arrived = lax.all_to_all(outgoing, SP_TP, split_axis=0, concat_axis=0, tiled=True)

    part = 128
    fanout = chosen.shape[0]
    base, mats = pl.pallas_call(
        shared_kernel,
        grid=(hidden // part,),
        in_specs=[
            whole((rows, dim)), whole((rows, dim)), pl.BlockSpec((dim, part), lambda n: (0, n)),
            pl.BlockSpec((dim, part), lambda n: (0, n)), pl.BlockSpec((part, dim), lambda n: (n, 0)),
            whole((fanout, rows)), whole((fanout, rows)),
        ],
        out_specs=(whole((rows, dim)), whole((4 * rows, experts * WIDE))),
        out_shape=(pltpu.HBM((rows, dim), F32), pltpu.HBM((4 * rows, experts * WIDE), BF16)),
        cost_estimate=pl.CostEstimate(flops=800_000_000, transcendentals=70_000, bytes_accessed=8_000_000),
        compiler_params=room(16),
        name="shared",
    )(normed, residual, *stay(common_gate_weight, common_up_weight, common_down_weight), chosen, chosen_expert_weight.T)

    chunks = 2
    tall = experts * WIDE // chunks
    served = pl.pallas_call(
        expert_kernel,
        in_specs=onchip(4),
        out_specs=offchip(1)[0],
        out_shape=pltpu.HBM((experts * WIDE, wide), BF16),
        scratch_shapes=[pltpu.VMEM((tall, dim), BF16), pltpu.VMEM((chunks, tall, wide), BF16), pltpu.SemaphoreType.DMA((chunks,))],
        compiler_params=room(24),
        name="experts",
    )(arrived, routed_gate_weight[0], routed_up_weight[0], routed_down_weight[0])
    returned = lax.all_to_all(served, SP_TP, split_axis=0, concat_axis=0, tiled=True)

    return pl.pallas_call(
        combine_kernel,
        in_specs=onchip(1) + offchip(2),
        out_specs=onchip(1)[0],
        out_shape=shape((rows, dim), BF16),
        scratch_shapes=[pltpu.VMEM((rows, dim), F32), pltpu.VMEM((4 * rows, experts * WIDE), BF16), pltpu.SemaphoreType.DMA((2,))],
        compiler_params=room(12),
        name="combine",
    )(returned, *stay(base, mats))


def solution(mesh):
    split = Mesh(mesh.devices.reshape(4, 4, 4, mesh.shape["tp"]), ("sp_0", "sp_1", "sp_2", "tp"))
    return jax.shard_map(
        on_device,
        mesh=split,
        in_specs=(
            P(SP_TP, None),
            P(SP, "tp"),
            P(SP, "tp"),
            P(SP, "tp"),
            P(SP, "tp"),
            P(SP, "tp"),
            P(SP, "tp"),
            P(None, "tp"),
            P(None, "tp"),
            P(None, "tp"),
            P("tp"),
            P("tp"),
            P("tp"),
            P("tp"),
            P("tp", None),
            P(),
            P(SP_TP, None),
            P(SP_TP, None),
            P(SP_TP, None, None),
            P(SP_TP, None, None),
            P(SP_TP, None, None),
            P(),
            P(),
            P(),
        ),
        out_specs=P(SP_TP, None),
        check_vma=False,
    )
```

time: 191 us -> 164 us (0.86)
  Pallas kernels: 49.5 us -> 33.1 us
  local copies, waits for them, and re-layouts: 10.8 us -> 2.12 us
    pallas_call x8 -> x10, Pallas kernels: 43.1 us -> 26.2 us  [the longest x1 9.42 us: on_device(): pl.pallas_call(expert_kernel, in_specs=onchip(4), out_specs=offchip(1)[0]...]
    unnamed x22 -> x20, local copies, waits for them, and re-layouts: 8.7 us -> 2.12 us
    all_to_all x1, waiting for transfers between devices: 3.51 us -> 5.99 us  [on_device(): lax.all_to_all(back, PLANE, split_axis=0, concat_axis=0, tiled=True)]
    slice x3 -> x0, local copies, waits for them, and re-layouts: 2.09 us -> none  [the longest x1 0.72 us: on_device(): head_input_signal[length - 8:]]
  transfers between devices with their start and end apart: 7 -> 7, of which waited for: 4 -> 4; matrix products, arithmetic and copies ran while one was open for 2% -> 0% of each run, Pallas kernels for 6% -> 7%
where the time goes in v2:
time: 164 us; the launch traced here: 163 us
  blocking collectives  60.1 us (37%)
  waiting for transfers between devices  41.2 us (25%)
  Pallas kernels  33.1 us (20%)
  starting transfers between devices  26.2 us (16%)
  local copies, waits for them, and re-layouts  2.12 us (1%)
    all_to_all x1, blocking collectives, on_device(): lax.all_to_all(outgoing, SP_TP, split_axis=0, concat_axis=0, tiled=True)  46.1 us
    all_to_all x1, waiting for transfers between devices, on_device(): lax.all_to_all(served, SP_TP, split_axis=0, concat_axis=0, tiled=True)  32.7 us
    all_to_all x1, blocking collectives, on_device(): got = lax.all_to_all(send, PLANE, split_axis=0, concat_axis=0, tiled=True)  14.1 us
    ppermute x3, starting transfers between devices, on_device(): lax.ppermute(total, 'sp_0', [(i, i + s) for i in range(planes - s)])  9.45 us
    pallas_call x1, Pallas kernels, on_device(): pl.pallas_call(expert_kernel, in_specs=onchip(4), out_specs=offchip(1)[0]...  9.42 us
    pallas_call x1, Pallas kernels, on_device(): pl.pallas_call(shared_kernel, grid=(hidden // part,), in_specs=[whole((ro...  6.86 us
    all_to_all x1, waiting for transfers between devices, on_device(): lax.all_to_all(back, PLANE, split_axis=0, concat_axis=0, tiled=True)  5.99 us
    all_to_all x1, starting transfers between devices, on_device(): lax.all_to_all(served, SP_TP, split_axis=0, concat_axis=0, tiled=True)  4.68 us
  transfers between devices with their start and end apart: 7, of which 4 were waited for; matrix products, arithmetic and copies ran while one was open for 0% of the time, Pallas kernels for 7%

profile of v2, /device:TPU:1, one launch (start us, length us, event | category | flops | bytes accessed | tf_op | source)
XLA Modules:
  0.0 163.2 jit_solution(12397327368596977785)
XLA Ops:
  0.0 0.7 rim.1
  0.8 3.9 %collective-permute-start = (bf16[8,1536]{1,0:T(8,128)(2,1)S(1)}, bf16[8,1536]{1,0:T(8,128)(2,1)S(1)}, u32[]{:S(2)}, u32[]{:S(2)}) collective-permute-start(bf16[8,1536]{1,0:T(8,128)(2,1)S(1)} %rim.1), channel_id=1, source_target_pairs={{0,2},{2,4},{4,6},{6,8},{8,10},{10,12},{12,14},{14,16},{16,18},{18... | collective-permute-start | bytes 73736 | tf_op jit(solution)/shard_map/ppermute | solution.py:446
  4.7 3.6 %front.1 = (f32[256,1024]{1,0:T(8,128)S(1)}, bf16[256,256]{1,0:T(8,128)(2,1)S(1)}, bf16[256,256]{1,0:T(8,128)(2,1)S(1)}, f32[256,128]{1,0:T(8,128)S(1)}, f32[16,...) custom-call(bf16[256,1024]{1,0:T(8,128)(2,1)} %x_hbm.1, ...), custom_call_target="tpu_custom_call" | custom-call | flops 800000000 | bytes 4000000 | tf_op jit(solution)/shard_map/front/pallas_call | solution.py:447
  8.9 14.1 %all_to_all.44 = bf16[16,8,1152]{2,1,0:T(8,128)(2,1)S(1)} all-to-all(bf16[16,8,1152]{2,1,0:T(8,128)(2,1)S(1)} %bitcast.29), channel_id=1, replica_groups=mesh['sp_0'=4,'sp_1'=4,'sp_2'=4,'tp'=2] {'sp_1','sp_2'}, dimensions={0} | all-to-all | bytes 589824 | tf_op jit(solution)/shard_map/all_to_all | solution.py:484
  23.2 5.7 %collective-permute-start.3 = (f32[8,1152]{1,0:T(8,128)S(1)}, f32[8,1152]{1,0:T(8,128)S(1)}, u32[]{:S(2)}, u32[]{:S(2)}) collective-permute-start(f32[8,1152]{1,0:T(8,128)S(1)} %get-tuple-element.47), channel_id=1, source_target_pairs={{0,96},{1,97},{2,98},{3,99},{4,100},{5,101},{6,102},{7,103},{8,104... | collective-permute-start | bytes 110600 | tf_op jit(solution)/shard_map/ppermute | solution.py:504
  28.9 1.3 collective-permute-start.2
  30.2 2.5 %collective-permute-start.1 = (f32[8,1152]{1,0:T(8,128)S(1)}, f32[8,1152]{1,0:T(8,128)S(1)}, u32[]{:S(2)}, u32[]{:S(2)}) collective-permute-start(f32[8,1152]{1,0:T(8,128)S(1)} %get-tuple-element.47), channel_id=1, source_target_pairs={{0,32},{32,64},{64,96},{1,33},{33,65},{65,97},{2,34},{34,66},{66,9... | collective-permute-start | bytes 110600 | tf_op jit(solution)/shard_map/ppermute | solution.py:504
  32.7 1.0 collective-permute-done.1.one_ref
  33.7 1.0 planes.1
  34.7 3.5 %all-to-all-start.1 = ((bf16[16,8,1024]{2,1,0:T(8,128)(2,1)}), bf16[16,8,1024]{2,1,0:T(8,128)(2,1)S(1)}, u32[]{:S(2)}, u32[]{:S(2)}) async-start(bf16[16,8,1024]{2,1,0:T(8,128)(2,1)} %bitcast.8), calls=%async_computation.1 | async-start | bytes 524288 | tf_op jit(solution)/shard_map/all_to_all | solution.py:513
  38.2 1.5 near.1.y_ref
  39.7 6.0 %all-to-all-done.1 = bf16[16,8,1024]{2,1,0:T(8,128)(2,1)S(1)} async-done(((bf16[16,8,1024]{2,1,0:T(8,128)(2,1)}), bf16[16,8,1024]{2,1,0:T(8,128)(2,1)S(1)}, u32[]{:S(2)}, u32[]{:S(2)}) %all-to-all-start.1) | async-done | bytes 262176 | tf_op jit(solution)/shard_map/all_to_all | solution.py:513
  45.7 3.5 %project.1 = (f32[128,2048]{1,0:T(8,128)S(1)}, bf16[128,2048]{1,0:T(8,128)(2,1)S(1)}) custom-call(s32[1]{0:T(128)} %bitcast.half_ref, f32[256,1024]{1,0:T(8,128)S(1)} %near.1.y_ref, bf16[128,1024]{1,0:T(8,128)(2,1)S(1)} %bitcast.28, bf16[256,256]{1,0:T(8,128)(2,1)S(1)} %get-tuple-element.41.rv_ref, f32[256,128]{1,0:T(8,128)S(1)} %get-tuple-element.35.cum_ref, ...), custom_call_target="tpu_custom_call" | custom-call | tf_op jit(solution)/shard_map/project/pallas_call | solution.py:516
  49.3 4.7 %collective-permute-start.4 = (bf16[128,2048]{1,0:T(8,128)(2,1)S(1)}, bf16[128,2048]{1,0:T(8,128)(2,1)S(1)}, u32[]{:S(2)}, u32[]{:S(2)}) collective-permute-start(bf16[128,2048]{1,0:T(8,128)(2,1)S(1)} %get-tuple-element.49), channel_id=1, source_target_pairs={{0,1},{1,0},{2,3},{3,2},{4,5},{5,4},{6,7},{7,6},{8,9},{9,8},{10,11... | collective-permute-start | bytes 1572872 | tf_op jit(solution)/shard_map/ppermute | solution.py:528
  53.9 1.5 collective-permute-done.4.got_ref
  55.5 2.4 %dispatch.1 = (bf16[128,2048]{1,0:T(8,128)(2,1)S(1)}, bf16[128,2048]{1,0:T(8,128)(2,1)S(1)}, bf16[1024,1536]{1,0:T(8,128)(2,1)S(1)}) custom-call(f32[128,2048]{1,0:T(8,128)S(1)} %get-tuple-element.48.own_ref, bf16[128,2048]{1,0:T(8,128)(2,1)S(1)} %collective-permute-done.4.got_ref, bf16[128,2048]{1,0:T(8,128)(2,1)} %stream_hbm.1, f32[1,2048]{1,0:T(1,128)} %bitcast.35, ...), custom_call_target="tpu_custom_call" | custom-call | tf_op jit(solution)/shard_map/dispatch/pallas_call | solution.py:531
  57.9 46.1 %all_to_all.45 = bf16[128,8,1536]{2,1,0:T(8,128)(2,1)S(1)} all-to-all(bf16[128,8,1536]{2,1,0:T(8,128)(2,1)S(1)} %bitcast.23), channel_id=1, replica_groups=mesh['sp_0'=4,'sp_1'=4,'sp_2'=4,'tp'=2] {'sp_0','sp_1','sp_2','tp'}, dimensions={0} | all-to-all | bytes 6291456 | tf_op jit(solution)/shard_map/all_to_all | solution.py:543
  104.0 9.4 %experts.1 = bf16[1024,1536]{1,0:T(8,128)(2,1)} custom-call(bf16[1024,1536]{1,0:T(8,128)(2,1)S(1)} %bitcast.22, bf16[2048,512]{1,0:T(8,128)(2,1)S(1)} %bitcast.24, bf16[2048,512]{1,0:T(8,128)(2,1)S(1)} %bitcast.25, bf16[512,2048]{1,0:T(8,128)(2,1)S(1)} %bitcast.26), custom_call_target="tpu_custom_call" | custom-call | tf_op jit(solution)/shard_map/experts/pallas_call | solution.py:564
  113.4 4.7 %all-to-all-start.3 = ((bf16[128,8,1536]{2,1,0:T(8,128)(2,1)}), bf16[128,8,1536]{2,1,0:T(8,128)(2,1)S(1)}, u32[]{:S(2)}, u32[]{:S(2)}) async-start(bf16[128,8,1536]{2,1,0:T(8,128)(2,1)} %bitcast.34), calls=%async_computation.3 | async-start | bytes 6291456 | tf_op jit(solution)/shard_map/all_to_all | solution.py:573
  118.1 1.0 copy-done.4
  119.2 1.0 copy-done.6
  120.2 6.9 %shared.1 = (f32[128,2048]{1,0:T(8,128)}, bf16[512,1024]{1,0:T(8,128)(2,1)}) custom-call(bf16[128,2048]{1,0:T(8,128)(2,1)S(1)} %copy-done.6, bf16[128,2048]{1,0:T(8,128)(2,1)S(1)} %copy-done.4, bf16[2048,512]{1,0:T(8,128)(2,1)} %gate_ref.1, bf16[2048,512]{1,0:T(8,128)(2,1)} %up_ref.1, bf16[512,2048]{1,0:T(8,128)(2,1)} %down_ref.1, s32[4,128]{1,0:T(4,128)S(1)} %bitcast.31, ...), custom_call_target="tpu_custom_call" | custom-call | flops 800000000 | bytes 8000000 | tf_op jit(solution)/shard_map/shared/pallas_call | solution.py:547
  127.1 32.7 %all-to-all-done.3 = bf16[128,8,1536]{2,1,0:T(8,128)(2,1)S(1)} async-done(((bf16[128,8,1536]{2,1,0:T(8,128)(2,1)}), bf16[128,8,1536]{2,1,0:T(8,128)(2,1)S(1)}, u32[]{:S(2)}, u32[]{:S(2)}) %all-to-all-start.3) | async-done | bytes 3145760 | tf_op jit(solution)/shard_map/all_to_all | solution.py:573
  159.7 3.3 %combine.1 = bf16[128,2048]{1,0:T(8,128)(2,1)} custom-call(bf16[1024,1536]{1,0:T(8,128)(2,1)S(1)} %bitcast.21, f32[128,2048]{1,0:T(8,128)} %get-tuple-element.53.base_hbm, bf16[512,1024]{1,0:T(8,128)(2,1)} %get-tuple-element.54.mats_hbm), custom_call_target="tpu_custom_call" | custom-call | tf_op jit(solution)/shard_map/combine/pallas_call | solution.py:575
  (23 shorter events, 0.8 us)
Async XLA Ops:
  0.8 7.6 %collective-permute-start = (bf16[8,1536]{1,0:T(8,128)(2,1)S(1)}, bf16[8,1536]{1,0:T(8,128)(2,1)S(1)}, u32[]{:S(2)}, u32[]{:S(2)}) collective-permute-start(bf16[8,1536]{1,0:T(8,128)(2,1)S(1)} %rim.1), channel_id=1, source_target_pairs={{0,2},{2,4},{4,6},{6,8},{8,10},{10,12},{12,14},{14,16},{16,18},{18... | collective-permute-start | bytes 73736 | tf_op jit(solution)/shard_map/ppermute | solution.py:446
  8.3 29.9 %copy-start.9 = (f32[16]{0:T(128)S(1)}, f32[16]{0:T(128)}, u32[]{:S(2)}) copy-start(f32[16]{0:T(128)} %param.36) | copy-start | bytes 196
  23.2 9.5 %collective-permute-start.3 = (f32[8,1152]{1,0:T(8,128)S(1)}, f32[8,1152]{1,0:T(8,128)S(1)}, u32[]{:S(2)}, u32[]{:S(2)}) collective-permute-start(f32[8,1152]{1,0:T(8,128)S(1)} %get-tuple-element.47), channel_id=1, source_target_pairs={{0,96},{1,97},{2,98},{3,99},{4,100},{5,101},{6,102},{7,103},{8,104... | collective-permute-start | bytes 110600 | tf_op jit(solution)/shard_map/ppermute | solution.py:504
  28.9 3.8 %collective-permute-start.2 = (f32[8,1152]{1,0:T(8,128)S(1)}, f32[8,1152]{1,0:T(8,128)S(1)}, u32[]{:S(2)}, u32[]{:S(2)}) collective-permute-start(f32[8,1152]{1,0:T(8,128)S(1)} %get-tuple-element.47), channel_id=1, source_target_pairs={{0,64},{32,96},{1,65},{33,97},{2,66},{34,98},{3,67},{35,99},{4,68}... | collective-permute-start | bytes 110600 | tf_op jit(solution)/shard_map/ppermute | solution.py:504
  30.2 3.5 %collective-permute-start.1 = (f32[8,1152]{1,0:T(8,128)S(1)}, f32[8,1152]{1,0:T(8,128)S(1)}, u32[]{:S(2)}, u32[]{:S(2)}) collective-permute-start(f32[8,1152]{1,0:T(8,128)S(1)} %get-tuple-element.47), channel_id=1, source_target_pairs={{0,32},{32,64},{64,96},{1,33},{33,65},{65,97},{2,34},{34,66},{66,9... | collective-permute-start | bytes 110600 | tf_op jit(solution)/shard_map/ppermute | solution.py:504
  34.7 11.0 %all-to-all-start.1 = ((bf16[16,8,1024]{2,1,0:T(8,128)(2,1)}), bf16[16,8,1024]{2,1,0:T(8,128)(2,1)S(1)}, u32[]{:S(2)}, u32[]{:S(2)}) async-start(bf16[16,8,1024]{2,1,0:T(8,128)(2,1)} %bitcast.8), calls=%async_computation.1 | async-start | bytes 524288 | tf_op jit(solution)/shard_map/all_to_all | solution.py:513
  45.7 9.8 %copy-start.7 = (s32[128,4]{0,1:T(4,128)S(1)}, s32[128,4]{0,1:T(4,128)}, u32[]{:S(2)}) copy-start(s32[128,4]{0,1:T(4,128)} %param.40) | copy-start | bytes 6148
  49.3 6.2 %collective-permute-start.4 = (bf16[128,2048]{1,0:T(8,128)(2,1)S(1)}, bf16[128,2048]{1,0:T(8,128)(2,1)S(1)}, u32[]{:S(2)}, u32[]{:S(2)}) collective-permute-start(bf16[128,2048]{1,0:T(8,128)(2,1)S(1)} %get-tuple-element.49), channel_id=1, source_target_pairs={{0,1},{1,0},{2,3},{3,2},{4,5},{5,4},{6,7},{7,6},{8,9},{9,8},{10,11... | collective-permute-start | bytes 1572872 | tf_op jit(solution)/shard_map/ppermute | solution.py:528
  57.9 46.1 %copy-start.3 = (bf16[128,2048]{1,0:T(8,128)(2,1)}, bf16[128,2048]{1,0:T(8,128)(2,1)S(1)}, u32[]{:S(2)}) copy-start(bf16[128,2048]{1,0:T(8,128)(2,1)S(1)} %get-tuple-element.52.residual_ref) | copy-start | bytes 1572868
  57.9 46.1 %copy-start.5 = (bf16[128,2048]{1,0:T(8,128)(2,1)}, bf16[128,2048]{1,0:T(8,128)(2,1)S(1)}, u32[]{:S(2)}) copy-start(bf16[128,2048]{1,0:T(8,128)(2,1)S(1)} %get-tuple-element.51.normed_ref) | copy-start | bytes 1572868
  57.9 46.1 %copy-start = (bf16[1,2048,512]{2,1,0:T(8,128)(2,1)S(1)}, bf16[1,2048,512]{2,1,0:T(8,128)(2,1)}, u32[]{:S(2)}) copy-start(bf16[1,2048,512]{2,1,0:T(8,128)(2,1)} %param.42) | copy-start | bytes 6291460
  57.9 46.1 %copy-start.1 = (bf16[1,2048,512]{2,1,0:T(8,128)(2,1)S(1)}, bf16[1,2048,512]{2,1,0:T(8,128)(2,1)}, u32[]{:S(2)}) copy-start(bf16[1,2048,512]{2,1,0:T(8,128)(2,1)} %param.43) | copy-start | bytes 6291460
  57.9 46.1 %copy-start.2 = (bf16[1,512,2048]{2,1,0:T(8,128)(2,1)S(1)}, bf16[1,512,2048]{2,1,0:T(8,128)(2,1)}, u32[]{:S(2)}) copy-start(bf16[1,512,2048]{2,1,0:T(8,128)(2,1)} %param.44) | copy-start | bytes 6291460
  113.4 4.7 %copy-start.8 = (f32[128,4]{0,1:T(4,128)S(1)}, f32[128,4]{0,1:T(4,128)}, u32[]{:S(2)}) copy-start(f32[128,4]{0,1:T(4,128)} %param.41) | copy-start | bytes 6148
  113.4 46.3 %all-to-all-start.3 = ((bf16[128,8,1536]{2,1,0:T(8,128)(2,1)}), bf16[128,8,1536]{2,1,0:T(8,128)(2,1)S(1)}, u32[]{:S(2)}, u32[]{:S(2)}) async-start(bf16[128,8,1536]{2,1,0:T(8,128)(2,1)} %bitcast.34), calls=%async_computation.3 | async-start | bytes 6291456 | tf_op jit(solution)/shard_map/all_to_all | solution.py:573
  118.1 1.0 copy-start.4
  119.2 1.0 copy-start.6

commit v3 on v2

--- a/solution.py
+++ b/solution.py
@@ -189,23 +189,35 @@
         state = state * decay[i : i + 1] + got_ref[8 * i : 8 * i + 8, 0:chans].astype(F32)
         sofar = sofar + logs[i : i + 1]
     pdec_ref[...] = spread(jnp.exp(jnp.concatenate(before, axis=0)), lanes)
-    send_ref[:, 0:chans] = state
-    send_ref[:, chans:] = jnp.broadcast_to(sofar, (8, LANES))
-
-
-def planes_kernel(pin_ref, pdec_ref, one_ref, two_ref, three_ref, out_ref):
+    for k in range(send_ref.shape[0] // 8):
+        send_ref[8 * k : 8 * k + 8, 0:chans] = state
+        send_ref[8 * k : 8 * k + 8, chans:] = jnp.broadcast_to(sofar, (8, LANES))
+
+
+def planes_kernel(plane_ref, pin_ref, pdec_ref, got_ref, out_ref):
     chans = pin_ref.shape[1]
     count = pin_ref.shape[0] // 8
     lanes = head_lanes(chans)
-    near = spread(jnp.exp(one_ref[:, chans:]), lanes)
-    far = spread(jnp.exp(two_ref[:, chans:]), lanes)
-    state = one_ref[:, 0:chans] + near * (two_ref[:, 0:chans] + far * three_ref[:, 0:chans])
+    plane = plane_ref[0]
+    state = jnp.zeros((8, chans), F32)
+    for k in range(got_ref.shape[0] // 8 - 1):
+        rows = slice(8 * k, 8 * k + 8)
+        state = jnp.where(k < plane, state * spread(jnp.exp(got_ref[rows, chans:]), lanes) + got_ref[rows, 0:chans], state)
     for i in range(0, count, 2):
         pair = [pin_ref[8 * k : 8 * k + 8, :] + state * pdec_ref[k : k + 1, :] for k in (i, i + 1)]
         out_ref[8 * i : 8 * i + 16, :] = jnp.concatenate(pair, axis=0).astype(BF16)
 
 
-def near_kernel(sig_ref, wv_ref, rv_ref, cum_ref, rows_ref, dtv_ref, s0_ref, direct_ref, y_ref, pad_ref):
+def near_kernel(sig_ref, wv_ref, rv_ref, cum_ref, rows_ref, dtv_ref, s0_ref, direct_ref, chosen_ref, y_ref, both_hbm, pad_ref, both_ref, sem):
+    experts, tokens = both_ref.shape[0] // WIDE, chosen_ref.shape[1]
+    slots = mm(expert_rows(experts), slot_table(chosen_ref[...], experts).astype(BF16))
+    place = (iota(slots.shape, 0) % WIDE).astype(F32)
+    both_ref[:, 0:tokens] = jnp.where(slots == place + 1.0, 1.0, 0.0).astype(BF16)
+    for q in range(3):
+        tail = jnp.where((place >= 6.0) & (slots == 3.0 * place + (q - 17.0)), 1.0, 0.0)
+        both_ref[:, tokens * (q + 1) : tokens * (q + 2)] = tail.astype(BF16)
+    copy = pltpu.make_async_copy(both_ref, both_hbm, sem)
+    copy.start()
     length, chans = sig_ref.shape
     heads = direct_ref.shape[1]
     groups = wv_ref.shape[1] // STATE
@@ -242,15 +254,15 @@
                 if b == 1:
                     out = out + carried[:, j * LANES : (j + 1) * LANES]
                 y_ref[rows, at : at + LANES] = out
-
-
-def project_kernel(half_ref, y_ref, state_ref, rv_ref, cum_ref, gate_hbm, gain_hbm, w_hbm, own_ref, other_ref,
-                   gate_ref, gain_ref, w_ref, mix_ref, res_ref, sems):
+    copy.wait()
+
+
+def project_kernel(half_ref, y_ref, state_ref, rv_ref, cum_ref, gate_hbm, gain_hbm, w_hbm, other_ref, mine_ref, w_ref,
+                   gate_ref, gain_ref, mix_ref, sems):
     length, chans = y_ref.shape
     groups = rv_ref.shape[1] // STATE
     width = chans // groups
-    rows = own_ref.shape[0]
-    dim = own_ref.shape[1]
+    rows, dim = other_ref.shape
     parts = 4
     pairs = [(gate_hbm, gate_ref), (gain_hbm, gain_ref)]
     for k in range(parts):
@@ -269,12 +281,20 @@
         mean = jnp.sum(gated * gated, axis=1, keepdims=True) * (1.0 / width)
         mix_ref[:, part] = (gated * lax.rsqrt(mean + 1e-06) * gain_ref[:, part]).astype(BF16)
     half = half_ref[0]
+    mine_ref[...] = mix_ref[pl.ds(pl.multiple_of(half * rows, rows), rows), :]
+    theirs = mix_ref[pl.ds(pl.multiple_of((1 - half) * rows, rows), rows), :]
     for k in range(parts):
         part = slice(k * (dim // parts), (k + 1) * (dim // parts))
         copies[2 + k].wait()
-        res_ref[...] = mm(mix_ref[...], w_ref[:, part])
-        own_ref[:, part] = res_ref[pl.ds(pl.multiple_of(half * rows, rows), rows), :]
-        other_ref[:, part] = res_ref[pl.ds(pl.multiple_of((1 - half) * rows, rows), rows), :].astype(BF16)
+        other_ref[:, part] = mm(theirs, w_ref[:, part]).astype(BF16)
+
+
+def own_kernel(mine_ref, w_ref, stream_hbm, own_ref, stream_ref, sem):
+    copy = pltpu.make_async_copy(stream_hbm, stream_ref, sem)
+    copy.start()
+    product = mm(mine_ref[...], w_ref[...])
+    copy.wait()
+    own_ref[...] = product + stream_ref[...].astype(F32)
 
 
 def slot_table(chosen, experts):
@@ -291,26 +311,17 @@
     return jnp.where(iota((experts * WIDE, experts), 0) // WIDE == iota((experts * WIDE, experts), 1), 1.0, 0.0).astype(BF16)
 
 
-def dispatch_kernel(own_ref, got_ref, stream_hbm, gain_hbm, chosen_ref, residual_ref, normed_ref, out_ref,
-                    stream_ref, gain_ref, both_ref, sems):
+def dispatch_kernel(own_ref, got_ref, gain_hbm, both_hbm, residual_ref, normed_ref, out_ref, gain_ref, both_ref, sems):
     rows, dim = own_ref.shape
     third = out_ref.shape[1] // 3
-    experts = out_ref.shape[0] // WIDE
-    copies = fetch(((stream_hbm, stream_ref), (gain_hbm, gain_ref)), sems)
-    table = slot_table(chosen_ref[...], experts)
-    slots = mm(expert_rows(experts), table.astype(BF16))
-    place = (iota(slots.shape, 0) % WIDE).astype(F32)
-    both_ref[:, 0:rows] = jnp.where(slots == place + 1.0, 1.0, 0.0).astype(BF16)
-    for q in range(3):
-        tail = jnp.where((place >= 6.0) & (slots == 3.0 * place + (q - 17.0)), 1.0, 0.0)
-        both_ref[:, rows * (q + 1) : rows * (q + 2)] = tail.astype(BF16)
-    for copy in copies:
-        copy.wait()
-    residual = (stream_ref[...].astype(F32) + own_ref[...] + got_ref[...].astype(F32)).astype(BF16)
+    copies = fetch(((gain_hbm, gain_ref), (both_hbm, both_ref)), sems)
+    residual = (own_ref[...] + got_ref[...].astype(F32)).astype(BF16)
     residual_ref[...] = residual
     wide = residual.astype(F32)
     mean = jnp.sum(wide * wide, axis=1, keepdims=True) * (1.0 / dim)
+    copies[0].wait()
     normed_ref[...] = (wide * lax.rsqrt(mean + 1e-06) * gain_ref[...]).astype(BF16)
+    copies[1].wait()
     main = both_ref[:, 0:rows]
     for q in range(3):
         mats = jnp.concatenate([main, both_ref[:, rows * (q + 1) : rows * (q + 2)]], axis=1)
@@ -343,55 +354,78 @@
     out_ref[...] += mm(hidden, down_ref[...])
 
 
+def turn(value, by):
+    return pltpu.roll(value, by % WIDE, axis=1)
+
+
+def compact(value):
+    width = value.shape[1]
+    value = value.reshape(-1, 4, WIDE, width)
+    row = iota((value.shape[0], WIDE, width), 1)
+    a, b, c = turn(value[:, 1], 6), turn(value[:, 2], 4), turn(value[:, 3], 2)
+    out = [jnp.where(row < 6, value[:, 0], a), jnp.where(row < 4, a, b), jnp.where(row < 2, b, c)]
+    return jnp.concatenate(out, axis=1).reshape(-1, width)
+
+
+def expand(value):
+    value = value.reshape(-1, 3 * WIDE, value.shape[1])
+    a, b, c = value[:, 0:WIDE], value[:, WIDE : 2 * WIDE], value[:, 2 * WIDE :]
+    row = iota(a.shape, 1)
+    return [a, jnp.where(row < 2, turn(a, 2), turn(b, 2)), jnp.where(row < 4, turn(b, 4), turn(c, 4)), turn(c, 6)]
+
+
 def expert_kernel(x_ref, gate_ref, up_ref, down_ref, out_hbm, full_ref, out_ref, sems):
     total, wide = x_ref.shape
     third = wide // 3
     rows = out_ref.shape[1]
-    row, col = iota((LANES, LANES), 0), iota((LANES, LANES), 1)
-    same = row // WIDE == col // WIDE
-    r, c = row % WIDE, col % WIDE
-    unpack = [jnp.where(same & (c >= 6) & (r == 3 * (c - 6) + q), 1.0, 0.0).astype(BF16) for q in range(3)]
-    pack = [jnp.where(same & (r >= 6) & (c == 3 * (r - 6) + q), 1.0, 0.0).astype(BF16) for q in range(3)]
-    unpack, pack = jnp.concatenate(unpack, axis=1), jnp.concatenate(pack, axis=0)
-    within = iota((LANES, third), 0) % WIDE < SLOTS
+    row = iota((LANES // WIDE, WIDE, third), 1)
     copies = []
     for n in range(total // rows):
-        base = n * rows
-        full_ref[:, 0:wide] = x_ref[base : base + rows, :]
         for at in range(0, rows, LANES):
-            pieces = [x_ref[base + at : base + at + LANES, q * third : (q + 1) * third] for q in range(3)]
-            full_ref[at : at + LANES, wide:] = mm(unpack, jnp.concatenate(pieces, axis=0)).astype(BF16)
+            dense = slice(at * SLOTS // WIDE, (at + LANES) * SLOTS // WIDE)
+            tail = jnp.zeros(row.shape, F32)
+            for q in range(3):
+                part = x_ref[n * rows + at : n * rows + at + LANES, q * third : (q + 1) * third].astype(F32)
+                full_ref[dense, q * third : (q + 1) * third] = compact(part).astype(BF16)
+                part = part.reshape(row.shape)
+                tail = jnp.where(row == q, turn(part, q - 6), jnp.where(row == 3 + q, turn(part, q - 4), tail))
+            full_ref[dense, wide:] = compact(tail.reshape(LANES, third)).astype(BF16)
         full = full_ref[...]
         hidden = (silu(mm(full, gate_ref[...])) * mm(full, up_ref[...])).astype(BF16)
-        tail = mm(hidden, down_ref[:, wide:]).astype(BF16)
-        packed = [mm(pack, tail[at : at + LANES]) for at in range(0, rows, LANES)]
+        tails = expand(mm(hidden, down_ref[:, wide:]))
         for q in range(3):
             part = slice(q * third, (q + 1) * third)
-            result = mm(hidden, down_ref[:, part])
-            for k, at in enumerate(range(0, rows, LANES)):
-                extra = packed[k][q * LANES : (q + 1) * LANES]
-                out_ref[n, at : at + LANES, part] = jnp.where(within, result[at : at + LANES], extra).astype(BF16)
-        copy = pltpu.make_async_copy(out_ref.at[n], out_hbm.at[base : base + rows, :], sems.at[n])
+            mains = expand(mm(hidden, down_ref[:, part]))
+            at = iota(mains[0].shape, 1)
+            mixed = [
+                jnp.where(at < 6, main, jnp.where(at == 6, turn(tail, 6 - q), turn(tail, 4 - q)))
+                for main, tail in zip(mains, tails)
+            ]
+            out_ref[n, :, part] = jnp.stack(mixed, axis=1).reshape(rows, third).astype(BF16)
+        copy = pltpu.make_async_copy(out_ref.at[n], out_hbm.at[n * rows : (n + 1) * rows, :], sems.at[n])
         copy.start()
         copies.append(copy)
     for copy in copies:
         copy.wait()
 
 
-def combine_kernel(got_ref, base_hbm, mats_hbm, out_ref, base_ref, mats_ref, sems):
+def combine_kernel(got_ref, base_hbm, mats_hbm, out_ref, base_ref, mats_ref, main_ref, sems):
     rows, dim = base_ref.shape
     third = got_ref.shape[1] // 3
-    copies = fetch(((mats_hbm, mats_ref), (base_hbm, base_ref)), sems)
-    tail = jnp.zeros((rows, third), F32)
+    copies = fetch((
+        (mats_hbm.at[0 : 2 * rows, :], mats_ref.at[0 : 2 * rows, :]), (mats_hbm.at[2 * rows :, :], mats_ref.at[2 * rows :, :]),
+        (base_hbm, base_ref),
+    ), sems)
     copies[0].wait()
-    for q in range(3):
-        part = slice(q * third, (q + 1) * third)
-        got = got_ref[:, part]
-        main = mm(mats_ref[0:rows, :], got)
+    both = mm(mats_ref[0 : 2 * rows, :], got_ref[:, 0:third])
+    main_ref[:, 0:third], tail = both[0:rows], both[rows:]
+    copies[1].wait()
+    for q in (1, 2):
+        got = got_ref[:, q * third : (q + 1) * third]
+        main_ref[:, q * third : (q + 1) * third] = mm(mats_ref[0:rows, :], got)
         tail = tail + mm(mats_ref[rows * (q + 1) : rows * (q + 2), :], got)
-        if q == 0:
-            copies[1].wait()
-        out_ref[:, part] = (base_ref[:, part] + main).astype(BF16)
+    copies[2].wait()
+    out_ref[:, 0 : 3 * third] = (base_ref[:, 0 : 3 * third] + main_ref[...]).astype(BF16)
     out_ref[:, 3 * third :] = (base_ref[:, 3 * third :] + tail).astype(BF16)
 
 
@@ -482,64 +516,71 @@
     )(rim, begin, taps, signal, write_rows, read_rows, cum, dtv, first, second)
     in_plane = lax.axis_size(PLANE)
     got = lax.all_to_all(send, PLANE, split_axis=0, concat_axis=0, tiled=True)
-    near = pl.pallas_call(
+    chosen = chosen_expert_index.T
+    near, both = pl.pallas_call(
         near_kernel,
-        in_specs=onchip(8),
-        out_specs=onchip(1)[0],
-        out_shape=shape((length, chans)),
-        scratch_shapes=[pltpu.VMEM((8, LANES), F32)],
+        in_specs=onchip(9),
+        out_specs=(onchip(1)[0], offchip(1)[0]),
+        out_shape=(shape((length, chans)), pltpu.HBM((experts * WIDE, 4 * rows), BF16)),
+        scratch_shapes=[pltpu.VMEM((8, LANES), F32), pltpu.VMEM((experts * WIDE, 4 * rows), BF16), pltpu.SemaphoreType.DMA],
         cost_estimate=pl.CostEstimate(flops=400_000_000, transcendentals=1_000_000, bytes_accessed=4_000_000),
-        compiler_params=room(12),
+        compiler_params=room(18),
         name="near",
-    )(sig, wv, rv, cum, cum_rows, dtv, s0, head_direct_term[None])
+    )(sig, wv, rv, cum, cum_rows, dtv, s0, head_direct_term[None], chosen)
+    planes = lax.axis_size("sp_0")
     pin, pdec, total = pl.pallas_call(
         plane_kernel,
         in_specs=onchip(1),
         out_specs=tuple(onchip(3)),
-        out_shape=(shape((STATE, chans)), shape((in_plane, chans)), shape((STATE // in_plane, chans + LANES))),
+        out_shape=(shape((STATE, chans)), shape((in_plane, chans)), shape((8 * planes, chans + LANES))),
         compiler_params=room(6),
         name="plane",
     )(got)
-    planes = lax.axis_size("sp_0")
-    lower = [lax.ppermute(total, "sp_0", [(i, i + s) for i in range(planes - s)]) for s in (1, 2, 3)]
+    lower = lax.all_to_all(total, "sp_0", split_axis=0, concat_axis=0, tiled=True)
     back = pl.pallas_call(
         planes_kernel,
-        in_specs=onchip(5),
+        in_specs=[pl.BlockSpec(memory_space=pltpu.SMEM)] + onchip(3),
         out_specs=onchip(1)[0],
         out_shape=shape((STATE, chans), BF16),
         compiler_params=room(6),
         name="planes",
-    )(pin, pdec, *lower)
+    )(lax.axis_index("sp_0").astype(jnp.int32).reshape(1), pin, pdec, lower)
     incoming = lax.all_to_all(back, PLANE, split_axis=0, concat_axis=0, tiled=True)
 
     half = lax.axis_index("tp").astype(jnp.int32).reshape(1)
-    own, other = pl.pallas_call(
+    other, mine, projection = pl.pallas_call(
         project_kernel,
         in_specs=[pl.BlockSpec(memory_space=pltpu.SMEM)] + onchip(4) + offchip(3),
-        out_specs=tuple(onchip(2)),
-        out_shape=(shape((rows, dim)), shape((rows, dim), BF16)),
+        out_specs=tuple(onchip(3)),
+        out_shape=(shape((rows, dim), BF16), shape((rows, chans), BF16), shape((chans, dim), BF16)),
         scratch_shapes=[
-            pltpu.VMEM((length, chans), BF16), pltpu.VMEM((1, chans), F32), pltpu.VMEM((chans, dim), BF16),
-            pltpu.VMEM((length, chans), BF16), pltpu.VMEM((length, dim // 4), F32), pltpu.SemaphoreType.DMA((6,)),
+            pltpu.VMEM((length, chans), BF16), pltpu.VMEM((1, chans), F32), pltpu.VMEM((length, chans), BF16),
+            pltpu.SemaphoreType.DMA((6,)),
         ],
         compiler_params=room(16),
         name="project",
     )(half, near, incoming, rv, cum, *stay(output_gate_input, grouped_norm_gain[None], mixer_output_weight))
     partner = lax.ppermute(other, "tp", [(0, 1), (1, 0)])
-
-    chosen = chosen_expert_index.T
+    own = pl.pallas_call(
+        own_kernel,
+        in_specs=onchip(2) + offchip(1),
+        out_specs=onchip(1)[0],
+        out_shape=shape((rows, dim)),
+        scratch_shapes=[pltpu.VMEM((rows, dim), BF16), pltpu.SemaphoreType.DMA],
+        cost_estimate=pl.CostEstimate(flops=600_000_000, transcendentals=0, bytes_accessed=6_000_000),
+        compiler_params=room(10),
+        name="own",
+    )(mine, projection, *stay(stream))
+
     residual, normed, outgoing = pl.pallas_call(
         dispatch_kernel,
-        in_specs=onchip(2) + offchip(2) + onchip(1),
+        in_specs=onchip(2) + offchip(2),
         out_specs=tuple(onchip(3)),
         out_shape=(shape((rows, dim), BF16), shape((rows, dim), BF16), shape((experts * WIDE, wide), BF16)),
-        scratch_shapes=[
-            pltpu.VMEM((rows, dim), BF16), pltpu.VMEM((1, dim), F32), pltpu.VMEM((experts * WIDE, 4 * rows), BF16),
-            pltpu.SemaphoreType.DMA((2,)),
-        ],
-        compiler_params=room(14),
+        scratch_shapes=[pltpu.VMEM((1, dim), F32), pltpu.VMEM((experts * WIDE, 4 * rows), BF16), pltpu.SemaphoreType.DMA((2,))],
+        compiler_params=room(16),
         name="dispatch",
-    )(own, partner, *stay(stream, expert_norm_gain[None]), chosen)
+    )(own, partner, *stay(expert_norm_gain[None], both))
     arrived = lax.all_to_all(outgoing, SP_TP, split_axis=0, concat_axis=0, tiled=True)
 
     part = 128
@@ -566,7 +607,7 @@
         in_specs=onchip(4),
         out_specs=offchip(1)[0],
         out_shape=pltpu.HBM((experts * WIDE, wide), BF16),
-        scratch_shapes=[pltpu.VMEM((tall, dim), BF16), pltpu.VMEM((chunks, tall, wide), BF16), pltpu.SemaphoreType.DMA((chunks,))],
+        scratch_shapes=[pltpu.VMEM((tall * SLOTS // WIDE, dim), BF16), pltpu.VMEM((chunks, tall, wide), BF16), pltpu.SemaphoreType.DMA((chunks,))],
         compiler_params=room(24),
         name="experts",
     )(arrived, routed_gate_weight[0], routed_up_weight[0], routed_down_weight[0])
@@ -577,8 +618,8 @@
         in_specs=onchip(1) + offchip(2),
         out_specs=onchip(1)[0],
         out_shape=shape((rows, dim), BF16),
-        scratch_shapes=[pltpu.VMEM((rows, dim), F32), pltpu.VMEM((4 * rows, experts * WIDE), BF16), pltpu.SemaphoreType.DMA((2,))],
-        compiler_params=room(12),
+        scratch_shapes=[pltpu.VMEM((rows, dim), F32), pltpu.VMEM((4 * rows, experts * WIDE), BF16), pltpu.VMEM((rows, wide), F32), pltpu.SemaphoreType.DMA((3,))],
+        compiler_params=room(16),
         name="combine",
     )(returned, *stay(base, mats))
 

time: 164 us -> 160 us (0.976)
  starting transfers between devices: 26.2 us -> 22.1 us
  waiting for transfers between devices: 41.2 us -> 43.1 us
    ppermute x3 -> x0, starting transfers between devices: 9.45 us -> none  [on_device(): lax.ppermute(total, 'sp_0', [(i, i + s) for i in range(planes - s)])]
    all_to_all x0 -> x1, starting transfers between devices: none -> 5.03 us  [on_device(): lax.all_to_all(total, 'sp_0', split_axis=0, concat_axis=0, tiled=True)]
    all_to_all x0 -> x1, waiting for transfers between devices: none -> 4.91 us  [on_device(): lax.all_to_all(total, 'sp_0', split_axis=0, concat_axis=0, tiled=True)]
    pallas_call x3 -> x4, Pallas kernels: 4.83 us -> 7.04 us  [the longest x1 2.37 us: on_device(): pl.pallas_call(dispatch_kernel, in_specs=onchip(2) + offchip(2), out_spec...]
    pallas_call x1, Pallas kernels: 9.42 us -> 7.3 us  [on_device(): pl.pallas_call(expert_kernel, in_specs=onchip(4), out_specs=offchip(1)[0]...]
  transfers between devices with their start and end apart: 7 -> 5, of which waited for: 4 -> 3; matrix products, arithmetic and copies ran while one was open for 0% -> 0% of each run, Pallas kernels for 7% -> 9%
where the time goes in v3:
time: 160 us
  blocking collectives  58.9 us (37%)
  waiting for transfers between devices  43.1 us (27%)
  Pallas kernels  33 us (21%)
  starting transfers between devices  22.1 us (14%)
  local copies, waits for them, and re-layouts  2.12 us (1%)
    all_to_all x1, blocking collectives, on_device(): lax.all_to_all(outgoing, SP_TP, split_axis=0, concat_axis=0, tiled=True)  44.8 us
    all_to_all x1, waiting for transfers between devices, on_device(): lax.all_to_all(served, SP_TP, split_axis=0, concat_axis=0, tiled=True)  32.6 us
    all_to_all x1, blocking collectives, on_device(): got = lax.all_to_all(send, PLANE, split_axis=0, concat_axis=0, tiled=True)  14.1 us
    pallas_call x1, Pallas kernels, on_device(): pl.pallas_call(expert_kernel, in_specs=onchip(4), out_specs=offchip(1)[0]...  7.3 us
    pallas_call x1, Pallas kernels, on_device(): pl.pallas_call(shared_kernel, grid=(hidden // part,), in_specs=[whole((ro...  6.9 us
    all_to_all x1, waiting for transfers between devices, on_device(): lax.all_to_all(back, PLANE, split_axis=0, concat_axis=0, tiled=True)  5.58 us
    all_to_all x1, starting transfers between devices, on_device(): lax.all_to_all(total, 'sp_0', split_axis=0, concat_axis=0, tiled=True)  5.03 us
    ppermute x1, starting transfers between devices, on_device(): partner = lax.ppermute(other, 'tp', [(0, 1), (1, 0)])  4.96 us
  transfers between devices with their start and end apart: 5, of which 3 were waited for; matrix products, arithmetic and copies ran while one was open for 0% of the time, Pallas kernels for 9%

profile of v3, /device:TPU:1, one launch (start us, length us, event | category | flops | bytes accessed | tf_op | source)
XLA Modules:
  0.0 159.6 jit_solution(7911312267817919595)
XLA Ops:
  0.0 0.7 rim.1
  0.8 3.9 %collective-permute-start = (bf16[8,1536]{1,0:T(8,128)(2,1)S(1)}, bf16[8,1536]{1,0:T(8,128)(2,1)S(1)}, u32[]{:S(2)}, u32[]{:S(2)}) collective-permute-start(bf16[8,1536]{1,0:T(8,128)(2,1)S(1)} %rim.1), channel_id=1, source_target_pairs={{0,2},{2,4},{4,6},{6,8},{8,10},{10,12},{12,14},{14,16},{16,18},{18... | collective-permute-start | bytes 73736 | tf_op jit(solution)/shard_map/ppermute | solution.py:480
  4.7 3.6 %front.1 = (f32[256,1024]{1,0:T(8,128)S(1)}, bf16[256,256]{1,0:T(8,128)(2,1)S(1)}, bf16[256,256]{1,0:T(8,128)(2,1)S(1)}, f32[256,128]{1,0:T(8,128)S(1)}, f32[16,...) custom-call(bf16[256,1024]{1,0:T(8,128)(2,1)} %x_hbm.1, ...), custom_call_target="tpu_custom_call" | custom-call | flops 800000000 | bytes 4000000 | tf_op jit(solution)/shard_map/front/pallas_call | solution.py:481
  8.4 0.5 head.1
  8.9 14.1 %all_to_all.55 = bf16[16,8,1152]{2,1,0:T(8,128)(2,1)S(1)} all-to-all(bf16[16,8,1152]{2,1,0:T(8,128)(2,1)S(1)} %bitcast.33), channel_id=1, replica_groups=mesh['sp_0'=4,'sp_1'=4,'sp_2'=4,'tp'=2] {'sp_1','sp_2'}, dimensions={0} | all-to-all | bytes 589824 | tf_op jit(solution)/shard_map/all_to_all | solution.py:518
  22.9 0.9 plane.1
  23.9 5.0 %all-to-all-start.1 = ((f32[4,8,1152]{2,1,0:T(8,128)}), f32[4,8,1152]{2,1,0:T(8,128)S(1)}, u32[]{:S(2)}, u32[]{:S(2)}) async-start(f32[4,8,1152]{2,1,0:T(8,128)} %bitcast.10), calls=%async_computation.1 | async-start | bytes 294912 | tf_op jit(solution)/shard_map/all_to_all | solution.py:539
  28.9 4.9 %all-to-all-done.1 = f32[4,8,1152]{2,1,0:T(8,128)S(1)} async-done(((f32[4,8,1152]{2,1,0:T(8,128)}), f32[4,8,1152]{2,1,0:T(8,128)S(1)}, u32[]{:S(2)}, u32[]{:S(2)}) %all-to-all-start.1) | async-done | bytes 147488 | tf_op jit(solution)/shard_map/all_to_all | solution.py:539
  33.8 1.0 planes.1
  34.8 3.5 %all-to-all-start.2 = ((bf16[16,8,1024]{2,1,0:T(8,128)(2,1)}), bf16[16,8,1024]{2,1,0:T(8,128)(2,1)S(1)}, u32[]{:S(2)}, u32[]{:S(2)}) async-start(bf16[16,8,1024]{2,1,0:T(8,128)(2,1)} %bitcast.12), calls=%async_computation.2 | async-start | bytes 524288 | tf_op jit(solution)/shard_map/all_to_all | solution.py:548
  38.4 1.9 %near.1 = (f32[256,1024]{1,0:T(8,128)S(1)}, bf16[1024,512]{1,0:T(8,128)(2,1)}) custom-call(f32[256,1024]{1,0:T(8,128)S(1)} %get-tuple-element.42.sig_ref, bf16[256,256]{1,0:T(8,128)(2,1)S(1)} %get-tuple-element.43.wv_ref, bf16[256,256]{1,0:T(8,128)(2,1)S(1)} %get-tuple-element.44.rv_ref, f32[256,128]{1,0:T(8,128)S(1)} %get-tuple-element.38.cum_ref, ...), custom_call_target="tpu_custom_call" | custom-call | flops 400000000 | bytes 4000000 | tf_op jit(solution)/shard_map/near/pallas_call | solution.py:520
  40.3 5.6 %all-to-all-done.2 = bf16[16,8,1024]{2,1,0:T(8,128)(2,1)S(1)} async-done(((bf16[16,8,1024]{2,1,0:T(8,128)(2,1)}), bf16[16,8,1024]{2,1,0:T(8,128)(2,1)S(1)}, u32[]{:S(2)}, u32[]{:S(2)}) %all-to-all-start.2) | async-done | bytes 262176 | tf_op jit(solution)/shard_map/all_to_all | solution.py:548
  45.8 2.9 %project.1 = (bf16[128,2048]{1,0:T(8,128)(2,1)S(1)}, bf16[128,1024]{1,0:T(8,128)(2,1)S(1)}, bf16[1024,2048]{1,0:T(8,128)(2,1)S(1)}) custom-call(s32[1]{0:T(128)} %bitcast.half_ref, f32[256,1024]{1,0:T(8,128)S(1)} %get-tuple-element.47.y_ref, bf16[128,1024]{1,0:T(8,128)(2,1)S(1)} %bitcast.31, bf16[256,256]{1,0:T(8,128)(2,1)S(1)} %get-tuple-element.44.rv_ref, ...), custom_call_target="tpu_custom_call" | custom-call | tf_op jit(solution)/shard_map/project/pallas_call | solution.py:551
  48.8 5.0 %collective-permute-start.1 = (bf16[128,2048]{1,0:T(8,128)(2,1)S(1)}, bf16[128,2048]{1,0:T(8,128)(2,1)S(1)}, u32[]{:S(2)}, u32[]{:S(2)}) collective-permute-start(bf16[128,2048]{1,0:T(8,128)(2,1)S(1)} %get-tuple-element.54), channel_id=1, source_target_pairs={{0,1},{1,0},{2,3},{3,2},{4,5},{5,4},{6,7},{7,6},{8,9},{9,8},{10,11... | collective-permute-start | bytes 1572872 | tf_op jit(solution)/shard_map/ppermute | solution.py:563
  53.7 1.8 %own.1.own_ref = f32[128,2048]{1,0:T(8,128)S(1)} custom-call(bf16[128,1024]{1,0:T(8,128)(2,1)S(1)} %get-tuple-element.52.mine_ref, bf16[1024,2048]{1,0:T(8,128)(2,1)S(1)} %get-tuple-element.53.w_ref, bf16[128,2048]{1,0:T(8,128)(2,1)} %stream_hbm.1), custom_call_target="tpu_custom_call" | custom-call | flops 600000000 | bytes 6000000 | tf_op jit(solution)/shard_map/own/pallas_call | solution.py:564
  55.5 2.4 %dispatch.1 = (bf16[128,2048]{1,0:T(8,128)(2,1)S(1)}, bf16[128,2048]{1,0:T(8,128)(2,1)S(1)}, bf16[1024,1536]{1,0:T(8,128)(2,1)S(1)}) custom-call(f32[128,2048]{1,0:T(8,128)S(1)} %own.1.own_ref, bf16[128,2048]{1,0:T(8,128)(2,1)S(1)} %collective-permute-done.1.got_ref, f32[1,2048]{1,0:T(1,128)} %bitcast.39, bf16[1024,512]{1,0:T(8,128)(2,1)} %get-tuple-element.55.both_hbm), custom_call_target="tpu_custom_call" | custom-call | tf_op jit(solution)/shard_map/dispatch/pallas_call | solution.py:575
  58.0 44.8 %all_to_all.56 = bf16[128,8,1536]{2,1,0:T(8,128)(2,1)S(1)} all-to-all(bf16[128,8,1536]{2,1,0:T(8,128)(2,1)S(1)} %bitcast.26), channel_id=1, replica_groups=mesh['sp_0'=4,'sp_1'=4,'sp_2'=4,'tp'=2] {'sp_0','sp_1','sp_2','tp'}, dimensions={0} | all-to-all | bytes 6291456 | tf_op jit(solution)/shard_map/all_to_all | solution.py:584
  102.8 7.3 %experts.1 = bf16[1024,1536]{1,0:T(8,128)(2,1)} custom-call(bf16[1024,1536]{1,0:T(8,128)(2,1)S(1)} %bitcast.25, bf16[2048,512]{1,0:T(8,128)(2,1)S(1)} %bitcast.27, bf16[2048,512]{1,0:T(8,128)(2,1)S(1)} %bitcast.28, bf16[512,2048]{1,0:T(8,128)(2,1)S(1)} %bitcast.29), custom_call_target="tpu_custom_call" | custom-call | tf_op jit(solution)/shard_map/experts/pallas_call | solution.py:605
  110.1 4.7 %all-to-all-start.4 = ((bf16[128,8,1536]{2,1,0:T(8,128)(2,1)}), bf16[128,8,1536]{2,1,0:T(8,128)(2,1)S(1)}, u32[]{:S(2)}, u32[]{:S(2)}) async-start(bf16[128,8,1536]{2,1,0:T(8,128)(2,1)} %bitcast.38), calls=%async_computation.4 | async-start | bytes 6291456 | tf_op jit(solution)/shard_map/all_to_all | solution.py:614
  114.8 1.0 copy-done.4
  115.8 1.0 copy-done.6
  116.9 6.9 %shared.1 = (f32[128,2048]{1,0:T(8,128)}, bf16[512,1024]{1,0:T(8,128)(2,1)}) custom-call(bf16[128,2048]{1,0:T(8,128)(2,1)S(1)} %copy-done.6, bf16[128,2048]{1,0:T(8,128)(2,1)S(1)} %copy-done.4, bf16[2048,512]{1,0:T(8,128)(2,1)} %gate_ref.1, bf16[2048,512]{1,0:T(8,128)(2,1)} %up_ref.1, bf16[512,2048]{1,0:T(8,128)(2,1)} %down_ref.1, s32[4,128]{1,0:T(4,128)S(1)} %bitcast.35, ...), custom_call_target="tpu_custom_call" | custom-call | flops 800000000 | bytes 8000000 | tf_op jit(solution)/shard_map/shared/pallas_call | solution.py:588
  123.8 32.6 %all-to-all-done.4 = bf16[128,8,1536]{2,1,0:T(8,128)(2,1)S(1)} async-done(((bf16[128,8,1536]{2,1,0:T(8,128)(2,1)}), bf16[128,8,1536]{2,1,0:T(8,128)(2,1)S(1)}, u32[]{:S(2)}, u32[]{:S(2)}) %all-to-all-start.4) | async-done | bytes 3145760 | tf_op jit(solution)/shard_map/all_to_all | solution.py:614
  156.4 3.1 %combine.1 = bf16[128,2048]{1,0:T(8,128)(2,1)} custom-call(bf16[1024,1536]{1,0:T(8,128)(2,1)S(1)} %bitcast.24, f32[128,2048]{1,0:T(8,128)} %get-tuple-element.59.base_hbm, bf16[512,1024]{1,0:T(8,128)(2,1)} %get-tuple-element.60.mats_hbm), custom_call_target="tpu_custom_call" | custom-call | tf_op jit(solution)/shard_map/combine/pallas_call | solution.py:616
  (20 shorter events, 0.1 us)
Async XLA Ops:
  0.8 7.6 %collective-permute-start = (bf16[8,1536]{1,0:T(8,128)(2,1)S(1)}, bf16[8,1536]{1,0:T(8,128)(2,1)S(1)}, u32[]{:S(2)}, u32[]{:S(2)}) collective-permute-start(bf16[8,1536]{1,0:T(8,128)(2,1)S(1)} %rim.1), channel_id=1, source_target_pairs={{0,2},{2,4},{4,6},{6,8},{8,10},{10,12},{12,14},{14,16},{16,18},{18... | collective-permute-start | bytes 73736 | tf_op jit(solution)/shard_map/ppermute | solution.py:480
  8.3 30.0 %copy-start.7 = (s32[128,4]{0,1:T(4,128)S(1)}, s32[128,4]{0,1:T(4,128)}, u32[]{:S(2)}) copy-start(s32[128,4]{0,1:T(4,128)} %param.40) | copy-start | bytes 6148
  8.3 30.0 %copy-start.9 = (f32[16]{0:T(128)S(1)}, f32[16]{0:T(128)}, u32[]{:S(2)}) copy-start(f32[16]{0:T(128)} %param.36) | copy-start | bytes 196
  23.9 9.9 %all-to-all-start.1 = ((f32[4,8,1152]{2,1,0:T(8,128)}), f32[4,8,1152]{2,1,0:T(8,128)S(1)}, u32[]{:S(2)}, u32[]{:S(2)}) async-start(f32[4,8,1152]{2,1,0:T(8,128)} %bitcast.10), calls=%async_computation.1 | async-start | bytes 294912 | tf_op jit(solution)/shard_map/all_to_all | solution.py:539
  34.8 11.0 %all-to-all-start.2 = ((bf16[16,8,1024]{2,1,0:T(8,128)(2,1)}), bf16[16,8,1024]{2,1,0:T(8,128)(2,1)S(1)}, u32[]{:S(2)}, u32[]{:S(2)}) async-start(bf16[16,8,1024]{2,1,0:T(8,128)(2,1)} %bitcast.12), calls=%async_computation.2 | async-start | bytes 524288 | tf_op jit(solution)/shard_map/all_to_all | solution.py:548
  48.8 6.7 %collective-permute-start.1 = (bf16[128,2048]{1,0:T(8,128)(2,1)S(1)}, bf16[128,2048]{1,0:T(8,128)(2,1)S(1)}, u32[]{:S(2)}, u32[]{:S(2)}) collective-permute-start(bf16[128,2048]{1,0:T(8,128)(2,1)S(1)} %get-tuple-element.54), channel_id=1, source_target_pairs={{0,1},{1,0},{2,3},{3,2},{4,5},{5,4},{6,7},{7,6},{8,9},{9,8},{10,11... | collective-permute-start | bytes 1572872 | tf_op jit(solution)/shard_map/ppermute | solution.py:563
  57.9 44.9 %copy-start.3 = (bf16[128,2048]{1,0:T(8,128)(2,1)}, bf16[128,2048]{1,0:T(8,128)(2,1)S(1)}, u32[]{:S(2)}) copy-start(bf16[128,2048]{1,0:T(8,128)(2,1)S(1)} %get-tuple-element.58.residual_ref) | copy-start | bytes 1572868
  57.9 44.8 %copy-start.5 = (bf16[128,2048]{1,0:T(8,128)(2,1)}, bf16[128,2048]{1,0:T(8,128)(2,1)S(1)}, u32[]{:S(2)}) copy-start(bf16[128,2048]{1,0:T(8,128)(2,1)S(1)} %get-tuple-element.57.normed_ref) | copy-start | bytes 1572868
  57.9 44.8 %copy-start = (bf16[1,2048,512]{2,1,0:T(8,128)(2,1)S(1)}, bf16[1,2048,512]{2,1,0:T(8,128)(2,1)}, u32[]{:S(2)}) copy-start(bf16[1,2048,512]{2,1,0:T(8,128)(2,1)} %param.42) | copy-start | bytes 6291460
  58.0 44.8 %copy-start.1 = (bf16[1,2048,512]{2,1,0:T(8,128)(2,1)S(1)}, bf16[1,2048,512]{2,1,0:T(8,128)(2,1)}, u32[]{:S(2)}) copy-start(bf16[1,2048,512]{2,1,0:T(8,128)(2,1)} %param.43) | copy-start | bytes 6291460
  58.0 44.8 %copy-start.2 = (bf16[1,512,2048]{2,1,0:T(8,128)(2,1)S(1)}, bf16[1,512,2048]{2,1,0:T(8,128)(2,1)}, u32[]{:S(2)}) copy-start(bf16[1,512,2048]{2,1,0:T(8,128)(2,1)} %param.44) | copy-start | bytes 6291460
  110.1 4.7 %copy-start.8 = (f32[128,4]{0,1:T(4,128)S(1)}, f32[128,4]{0,1:T(4,128)}, u32[]{:S(2)}) copy-start(f32[128,4]{0,1:T(4,128)} %param.41) | copy-start | bytes 6148
  110.1 46.3 %all-to-all-start.4 = ((bf16[128,8,1536]{2,1,0:T(8,128)(2,1)}), bf16[128,8,1536]{2,1,0:T(8,128)(2,1)S(1)}, u32[]{:S(2)}, u32[]{:S(2)}) async-start(bf16[128,8,1536]{2,1,0:T(8,128)(2,1)} %bitcast.38), calls=%async_computation.4 | async-start | bytes 6291456 | tf_op jit(solution)/shard_map/all_to_all | solution.py:614
  114.8 1.0 copy-start.4
  115.8 1.0 copy-start.6

commit v4 on v3

--- a/solution.py
+++ b/solution.py
@@ -289,12 +289,13 @@
         other_ref[:, part] = mm(theirs, w_ref[:, part]).astype(BF16)
 
 
-def own_kernel(mine_ref, w_ref, stream_hbm, own_ref, stream_ref, sem):
-    copy = pltpu.make_async_copy(stream_hbm, stream_ref, sem)
-    copy.start()
+def own_kernel(mine_ref, w_ref, stream_hbm, both_hbm, gain_hbm, own_ref, both_ref, gain_ref, stream_ref, sems):
+    copies = fetch(((stream_hbm, stream_ref), (both_hbm, both_ref), (gain_hbm, gain_ref)), sems)
     product = mm(mine_ref[...], w_ref[...])
-    copy.wait()
+    copies[0].wait()
     own_ref[...] = product + stream_ref[...].astype(F32)
+    for copy in copies[1:]:
+        copy.wait()
 
 
 def slot_table(chosen, experts):
@@ -311,17 +312,14 @@
     return jnp.where(iota((experts * WIDE, experts), 0) // WIDE == iota((experts * WIDE, experts), 1), 1.0, 0.0).astype(BF16)
 
 
-def dispatch_kernel(own_ref, got_ref, gain_hbm, both_hbm, residual_ref, normed_ref, out_ref, gain_ref, both_ref, sems):
+def dispatch_kernel(own_ref, got_ref, both_ref, gain_ref, residual_ref, normed_ref, out_ref):
     rows, dim = own_ref.shape
     third = out_ref.shape[1] // 3
-    copies = fetch(((gain_hbm, gain_ref), (both_hbm, both_ref)), sems)
     residual = (own_ref[...] + got_ref[...].astype(F32)).astype(BF16)
     residual_ref[...] = residual
     wide = residual.astype(F32)
     mean = jnp.sum(wide * wide, axis=1, keepdims=True) * (1.0 / dim)
-    copies[0].wait()
     normed_ref[...] = (wide * lax.rsqrt(mean + 1e-06) * gain_ref[...]).astype(BF16)
-    copies[1].wait()
     main = both_ref[:, 0:rows]
     for q in range(3):
         mats = jnp.concatenate([main, both_ref[:, rows * (q + 1) : rows * (q + 2)]], axis=1)
@@ -561,26 +559,25 @@
         name="project",
     )(half, near, incoming, rv, cum, *stay(output_gate_input, grouped_norm_gain[None], mixer_output_weight))
     partner = lax.ppermute(other, "tp", [(0, 1), (1, 0)])
-    own = pl.pallas_call(
+    own, both, gain = pl.pallas_call(
         own_kernel,
-        in_specs=onchip(2) + offchip(1),
-        out_specs=onchip(1)[0],
-        out_shape=shape((rows, dim)),
-        scratch_shapes=[pltpu.VMEM((rows, dim), BF16), pltpu.SemaphoreType.DMA],
+        in_specs=onchip(2) + offchip(3),
+        out_specs=tuple(onchip(3)),
+        out_shape=(shape((rows, dim)), shape((experts * WIDE, 4 * rows), BF16), shape((1, dim))),
+        scratch_shapes=[pltpu.VMEM((rows, dim), BF16), pltpu.SemaphoreType.DMA((3,))],
         cost_estimate=pl.CostEstimate(flops=600_000_000, transcendentals=0, bytes_accessed=6_000_000),
         compiler_params=room(10),
         name="own",
-    )(mine, projection, *stay(stream))
+    )(mine, projection, *stay(stream, both, expert_norm_gain[None]))
 
     residual, normed, outgoing = pl.pallas_call(
         dispatch_kernel,
-        in_specs=onchip(2) + offchip(2),
+        in_specs=onchip(4),
         out_specs=tuple(onchip(3)),
         out_shape=(shape((rows, dim), BF16), shape((rows, dim), BF16), shape((experts * WIDE, wide), BF16)),
-        scratch_shapes=[pltpu.VMEM((1, dim), F32), pltpu.VMEM((experts * WIDE, 4 * rows), BF16), pltpu.SemaphoreType.DMA((2,))],
-        compiler_params=room(16),
+        compiler_params=room(12),
         name="dispatch",
-    )(own, partner, *stay(expert_norm_gain[None], both))
+    )(own, partner, both, gain)
     arrived = lax.all_to_all(outgoing, SP_TP, split_axis=0, concat_axis=0, tiled=True)
 
     part = 128

time: 160 us -> 159 us (level)
  no operation moved by 1% of the time
where the time goes in v4:
time: 159 us
  blocking collectives  58.8 us (37%)
  waiting for transfers between devices  43.1 us (27%)
  Pallas kernels  31.9 us (20%)
  starting transfers between devices  22.1 us (14%)
  local copies, waits for them, and re-layouts  2.12 us (1%)
    all_to_all x1, blocking collectives, on_device(): lax.all_to_all(outgoing, SP_TP, split_axis=0, concat_axis=0, tiled=True)  44.8 us
    all_to_all x1, waiting for transfers between devices, on_device(): lax.all_to_all(served, SP_TP, split_axis=0, concat_axis=0, tiled=True)  32.6 us
    all_to_all x1, blocking collectives, on_device(): got = lax.all_to_all(send, PLANE, split_axis=0, concat_axis=0, tiled=True)  14.1 us
    pallas_call x1, Pallas kernels, on_device(): pl.pallas_call(expert_kernel, in_specs=onchip(4), out_specs=offchip(1)[0]...  7.3 us
    pallas_call x1, Pallas kernels, on_device(): pl.pallas_call(shared_kernel, grid=(hidden // part,), in_specs=[whole((ro...  6.87 us
    all_to_all x1, waiting for transfers between devices, on_device(): lax.all_to_all(back, PLANE, split_axis=0, concat_axis=0, tiled=True)  5.58 us
    all_to_all x1, starting transfers between devices, on_device(): lax.all_to_all(total, 'sp_0', split_axis=0, concat_axis=0, tiled=True)  5.03 us
    ppermute x1, starting transfers between devices, on_device(): partner = lax.ppermute(other, 'tp', [(0, 1), (1, 0)])  4.96 us
  transfers between devices with their start and end apart: 5, of which 3 were waited for; matrix products, arithmetic and copies ran while one was open for 0% of the time, Pallas kernels for 9%

profile of v4, /device:TPU:1, one launch (start us, length us, event | category | flops | bytes accessed | tf_op | source)
XLA Modules:
  0.0 158.5 jit_solution(9581447189998614852)
XLA Ops:
  0.0 0.7 rim.1
  0.8 3.9 %collective-permute-start = (bf16[8,1536]{1,0:T(8,128)(2,1)S(1)}, bf16[8,1536]{1,0:T(8,128)(2,1)S(1)}, u32[]{:S(2)}, u32[]{:S(2)}) collective-permute-start(bf16[8,1536]{1,0:T(8,128)(2,1)S(1)} %rim.1), channel_id=1, source_target_pairs={{0,2},{2,4},{4,6},{6,8},{8,10},{10,12},{12,14},{14,16},{16,18},{18... | collective-permute-start | bytes 73736 | tf_op jit(solution)/shard_map/ppermute | solution.py:478
  4.7 3.6 %front.1 = (f32[256,1024]{1,0:T(8,128)S(1)}, bf16[256,256]{1,0:T(8,128)(2,1)S(1)}, bf16[256,256]{1,0:T(8,128)(2,1)S(1)}, f32[256,128]{1,0:T(8,128)S(1)}, f32[16,...) custom-call(bf16[256,1024]{1,0:T(8,128)(2,1)} %x_hbm.1, ...), custom_call_target="tpu_custom_call" | custom-call | flops 800000000 | bytes 4000000 | tf_op jit(solution)/shard_map/front/pallas_call | solution.py:479
  8.4 0.5 head.1
  8.9 14.1 %all_to_all.55 = bf16[16,8,1152]{2,1,0:T(8,128)(2,1)S(1)} all-to-all(bf16[16,8,1152]{2,1,0:T(8,128)(2,1)S(1)} %bitcast.33), channel_id=1, replica_groups=mesh['sp_0'=4,'sp_1'=4,'sp_2'=4,'tp'=2] {'sp_1','sp_2'}, dimensions={0} | all-to-all | bytes 589824 | tf_op jit(solution)/shard_map/all_to_all | solution.py:516
  22.9 0.9 plane.1
  23.9 5.0 %all-to-all-start.1 = ((f32[4,8,1152]{2,1,0:T(8,128)}), f32[4,8,1152]{2,1,0:T(8,128)S(1)}, u32[]{:S(2)}, u32[]{:S(2)}) async-start(f32[4,8,1152]{2,1,0:T(8,128)} %bitcast.10), calls=%async_computation.1 | async-start | bytes 294912 | tf_op jit(solution)/shard_map/all_to_all | solution.py:537
  28.9 4.9 %all-to-all-done.1 = f32[4,8,1152]{2,1,0:T(8,128)S(1)} async-done(((f32[4,8,1152]{2,1,0:T(8,128)}), f32[4,8,1152]{2,1,0:T(8,128)S(1)}, u32[]{:S(2)}, u32[]{:S(2)}) %all-to-all-start.1) | async-done | bytes 147488 | tf_op jit(solution)/shard_map/all_to_all | solution.py:537
  33.8 1.0 planes.1
  34.8 3.5 %all-to-all-start.2 = ((bf16[16,8,1024]{2,1,0:T(8,128)(2,1)}), bf16[16,8,1024]{2,1,0:T(8,128)(2,1)S(1)}, u32[]{:S(2)}, u32[]{:S(2)}) async-start(bf16[16,8,1024]{2,1,0:T(8,128)(2,1)} %bitcast.12), calls=%async_computation.2 | async-start | bytes 524288 | tf_op jit(solution)/shard_map/all_to_all | solution.py:546
  38.4 1.9 %near.1 = (f32[256,1024]{1,0:T(8,128)S(1)}, bf16[1024,512]{1,0:T(8,128)(2,1)}) custom-call(f32[256,1024]{1,0:T(8,128)S(1)} %get-tuple-element.45.sig_ref, bf16[256,256]{1,0:T(8,128)(2,1)S(1)} %get-tuple-element.46.wv_ref, bf16[256,256]{1,0:T(8,128)(2,1)S(1)} %get-tuple-element.47.rv_ref, f32[256,128]{1,0:T(8,128)S(1)} %get-tuple-element.41.cum_ref, ...), custom_call_target="tpu_custom_call" | custom-call | flops 400000000 | bytes 4000000 | tf_op jit(solution)/shard_map/near/pallas_call | solution.py:518
  40.3 5.6 %all-to-all-done.2 = bf16[16,8,1024]{2,1,0:T(8,128)(2,1)S(1)} async-done(((bf16[16,8,1024]{2,1,0:T(8,128)(2,1)}), bf16[16,8,1024]{2,1,0:T(8,128)(2,1)S(1)}, u32[]{:S(2)}, u32[]{:S(2)}) %all-to-all-start.2) | async-done | bytes 262176 | tf_op jit(solution)/shard_map/all_to_all | solution.py:546
  45.8 2.9 %project.1 = (bf16[128,2048]{1,0:T(8,128)(2,1)S(1)}, bf16[128,1024]{1,0:T(8,128)(2,1)S(1)}, bf16[1024,2048]{1,0:T(8,128)(2,1)S(1)}) custom-call(s32[1]{0:T(128)} %bitcast.half_ref, f32[256,1024]{1,0:T(8,128)S(1)} %get-tuple-element.50.y_ref, bf16[128,1024]{1,0:T(8,128)(2,1)S(1)} %bitcast.31, bf16[256,256]{1,0:T(8,128)(2,1)S(1)} %get-tuple-element.47.rv_ref, ...), custom_call_target="tpu_custom_call" | custom-call | tf_op jit(solution)/shard_map/project/pallas_call | solution.py:549
  48.8 5.0 %collective-permute-start.1 = (bf16[128,2048]{1,0:T(8,128)(2,1)S(1)}, bf16[128,2048]{1,0:T(8,128)(2,1)S(1)}, u32[]{:S(2)}, u32[]{:S(2)}) collective-permute-start(bf16[128,2048]{1,0:T(8,128)(2,1)S(1)} %get-tuple-element.59), channel_id=1, source_target_pairs={{0,1},{1,0},{2,3},{3,2},{4,5},{5,4},{6,7},{7,6},{8,9},{9,8},{10,11... | collective-permute-start | bytes 1572872 | tf_op jit(solution)/shard_map/ppermute | solution.py:561
  53.7 1.8 %own.1 = (f32[128,2048]{1,0:T(8,128)S(1)}, bf16[1024,512]{1,0:T(8,128)(2,1)S(1)}, f32[1,2048]{1,0:T(1,128)S(1)}) custom-call(bf16[128,1024]{1,0:T(8,128)(2,1)S(1)} %get-tuple-element.55.mine_ref, bf16[1024,2048]{1,0:T(8,128)(2,1)S(1)} %get-tuple-element.56.w_ref, bf16[128,2048]{1,0:T(8,128)(2,1)} %stream_hbm.1, ...), custom_call_target="tpu_custom_call" | custom-call | flops 600000000 | bytes 6000000 | tf_op jit(solution)/shard_map/own/pallas_call | solution.py:562
  55.6 1.3 dispatch.1
  56.9 44.8 %all_to_all.56 = bf16[128,8,1536]{2,1,0:T(8,128)(2,1)S(1)} all-to-all(bf16[128,8,1536]{2,1,0:T(8,128)(2,1)S(1)} %bitcast.26), channel_id=1, replica_groups=mesh['sp_0'=4,'sp_1'=4,'sp_2'=4,'tp'=2] {'sp_0','sp_1','sp_2','tp'}, dimensions={0} | all-to-all | bytes 6291456 | tf_op jit(solution)/shard_map/all_to_all | solution.py:581
  101.7 7.3 %experts.1 = bf16[1024,1536]{1,0:T(8,128)(2,1)} custom-call(bf16[1024,1536]{1,0:T(8,128)(2,1)S(1)} %bitcast.25, bf16[2048,512]{1,0:T(8,128)(2,1)S(1)} %bitcast.27, bf16[2048,512]{1,0:T(8,128)(2,1)S(1)} %bitcast.28, bf16[512,2048]{1,0:T(8,128)(2,1)S(1)} %bitcast.29), custom_call_target="tpu_custom_call" | custom-call | tf_op jit(solution)/shard_map/experts/pallas_call | solution.py:602
  109.0 4.7 %all-to-all-start.4 = ((bf16[128,8,1536]{2,1,0:T(8,128)(2,1)}), bf16[128,8,1536]{2,1,0:T(8,128)(2,1)S(1)}, u32[]{:S(2)}, u32[]{:S(2)}) async-start(bf16[128,8,1536]{2,1,0:T(8,128)(2,1)} %bitcast.38), calls=%async_computation.4 | async-start | bytes 6291456 | tf_op jit(solution)/shard_map/all_to_all | solution.py:611
  113.7 1.0 copy-done.4
  114.7 1.0 copy-done.6
  115.8 6.9 %shared.1 = (f32[128,2048]{1,0:T(8,128)}, bf16[512,1024]{1,0:T(8,128)(2,1)}) custom-call(bf16[128,2048]{1,0:T(8,128)(2,1)S(1)} %copy-done.6, bf16[128,2048]{1,0:T(8,128)(2,1)S(1)} %copy-done.4, bf16[2048,512]{1,0:T(8,128)(2,1)} %gate_ref.1, bf16[2048,512]{1,0:T(8,128)(2,1)} %up_ref.1, bf16[512,2048]{1,0:T(8,128)(2,1)} %down_ref.1, s32[4,128]{1,0:T(4,128)S(1)} %bitcast.35, ...), custom_call_target="tpu_custom_call" | custom-call | flops 800000000 | bytes 8000000 | tf_op jit(solution)/shard_map/shared/pallas_call | solution.py:585
  122.6 32.6 %all-to-all-done.4 = bf16[128,8,1536]{2,1,0:T(8,128)(2,1)S(1)} async-done(((bf16[128,8,1536]{2,1,0:T(8,128)(2,1)}), bf16[128,8,1536]{2,1,0:T(8,128)(2,1)S(1)}, u32[]{:S(2)}, u32[]{:S(2)}) %all-to-all-start.4) | async-done | bytes 3145760 | tf_op jit(solution)/shard_map/all_to_all | solution.py:611
  155.3 3.1 %combine.1 = bf16[128,2048]{1,0:T(8,128)(2,1)} custom-call(bf16[1024,1536]{1,0:T(8,128)(2,1)S(1)} %bitcast.24, f32[128,2048]{1,0:T(8,128)} %get-tuple-element.65.base_hbm, bf16[512,1024]{1,0:T(8,128)(2,1)} %get-tuple-element.66.mats_hbm), custom_call_target="tpu_custom_call" | custom-call | tf_op jit(solution)/shard_map/combine/pallas_call | solution.py:613
  (20 shorter events, 0.1 us)
Async XLA Ops:
  0.8 7.6 %collective-permute-start = (bf16[8,1536]{1,0:T(8,128)(2,1)S(1)}, bf16[8,1536]{1,0:T(8,128)(2,1)S(1)}, u32[]{:S(2)}, u32[]{:S(2)}) collective-permute-start(bf16[8,1536]{1,0:T(8,128)(2,1)S(1)} %rim.1), channel_id=1, source_target_pairs={{0,2},{2,4},{4,6},{6,8},{8,10},{10,12},{12,14},{14,16},{16,18},{18... | collective-permute-start | bytes 73736 | tf_op jit(solution)/shard_map/ppermute | solution.py:478
  8.3 30.0 %copy-start.7 = (s32[128,4]{0,1:T(4,128)S(1)}, s32[128,4]{0,1:T(4,128)}, u32[]{:S(2)}) copy-start(s32[128,4]{0,1:T(4,128)} %param.40) | copy-start | bytes 6148
  8.3 30.0 %copy-start.9 = (f32[16]{0:T(128)S(1)}, f32[16]{0:T(128)}, u32[]{:S(2)}) copy-start(f32[16]{0:T(128)} %param.36) | copy-start | bytes 196
  23.9 9.9 %all-to-all-start.1 = ((f32[4,8,1152]{2,1,0:T(8,128)}), f32[4,8,1152]{2,1,0:T(8,128)S(1)}, u32[]{:S(2)}, u32[]{:S(2)}) async-start(f32[4,8,1152]{2,1,0:T(8,128)} %bitcast.10), calls=%async_computation.1 | async-start | bytes 294912 | tf_op jit(solution)/shard_map/all_to_all | solution.py:537
  34.8 11.0 %all-to-all-start.2 = ((bf16[16,8,1024]{2,1,0:T(8,128)(2,1)}), bf16[16,8,1024]{2,1,0:T(8,128)(2,1)S(1)}, u32[]{:S(2)}, u32[]{:S(2)}) async-start(bf16[16,8,1024]{2,1,0:T(8,128)(2,1)} %bitcast.12), calls=%async_computation.2 | async-start | bytes 524288 | tf_op jit(solution)/shard_map/all_to_all | solution.py:546
  48.8 6.8 %collective-permute-start.1 = (bf16[128,2048]{1,0:T(8,128)(2,1)S(1)}, bf16[128,2048]{1,0:T(8,128)(2,1)S(1)}, u32[]{:S(2)}, u32[]{:S(2)}) collective-permute-start(bf16[128,2048]{1,0:T(8,128)(2,1)S(1)} %get-tuple-element.59), channel_id=1, source_target_pairs={{0,1},{1,0},{2,3},{3,2},{4,5},{5,4},{6,7},{7,6},{8,9},{9,8},{10,11... | collective-permute-start | bytes 1572872 | tf_op jit(solution)/shard_map/ppermute | solution.py:561
  56.8 44.8 %copy-start.3 = (bf16[128,2048]{1,0:T(8,128)(2,1)}, bf16[128,2048]{1,0:T(8,128)(2,1)S(1)}, u32[]{:S(2)}) copy-start(bf16[128,2048]{1,0:T(8,128)(2,1)S(1)} %get-tuple-element.64.residual_ref) | copy-start | bytes 1572868
  56.8 44.8 %copy-start.5 = (bf16[128,2048]{1,0:T(8,128)(2,1)}, bf16[128,2048]{1,0:T(8,128)(2,1)S(1)}, u32[]{:S(2)}) copy-start(bf16[128,2048]{1,0:T(8,128)(2,1)S(1)} %get-tuple-element.63.normed_ref) | copy-start | bytes 1572868
  56.8 44.8 %copy-start = (bf16[1,2048,512]{2,1,0:T(8,128)(2,1)S(1)}, bf16[1,2048,512]{2,1,0:T(8,128)(2,1)}, u32[]{:S(2)}) copy-start(bf16[1,2048,512]{2,1,0:T(8,128)(2,1)} %param.42) | copy-start | bytes 6291460
  56.9 44.8 %copy-start.1 = (bf16[1,2048,512]{2,1,0:T(8,128)(2,1)S(1)}, bf16[1,2048,512]{2,1,0:T(8,128)(2,1)}, u32[]{:S(2)}) copy-start(bf16[1,2048,512]{2,1,0:T(8,128)(2,1)} %param.43) | copy-start | bytes 6291460
  56.9 44.8 %copy-start.2 = (bf16[1,512,2048]{2,1,0:T(8,128)(2,1)S(1)}, bf16[1,512,2048]{2,1,0:T(8,128)(2,1)}, u32[]{:S(2)}) copy-start(bf16[1,512,2048]{2,1,0:T(8,128)(2,1)} %param.44) | copy-start | bytes 6291460
  109.0 4.7 %copy-start.8 = (f32[128,4]{0,1:T(4,128)S(1)}, f32[128,4]{0,1:T(4,128)}, u32[]{:S(2)}) copy-start(f32[128,4]{0,1:T(4,128)} %param.41) | copy-start | bytes 6148
  109.0 46.3 %all-to-all-start.4 = ((bf16[128,8,1536]{2,1,0:T(8,128)(2,1)}), bf16[128,8,1536]{2,1,0:T(8,128)(2,1)S(1)}, u32[]{:S(2)}, u32[]{:S(2)}) async-start(bf16[128,8,1536]{2,1,0:T(8,128)(2,1)} %bitcast.38), calls=%async_computation.4 | async-start | bytes 6291456 | tf_op jit(solution)/shard_map/all_to_all | solution.py:611
  113.7 1.0 copy-start.4
  114.7 1.0 copy-start.6

commit v5 on v4

--- a/solution.py
+++ b/solution.py
@@ -69,7 +69,7 @@
     return copies
 
 
-def rim_kernel(x_ref, b_ref, c_ref, out_ref, sems):
+def rim_kernel(half_ref, plane_ref, x_ref, b_ref, c_ref, out_ref, sems):
     start, pairs = 0, []
     for ref in (x_ref, b_ref, c_ref):
         rows, size = ref.shape
@@ -466,15 +466,17 @@
 
     heads = step_size_input.shape[1]
     devices = lax.axis_size(SP)
+    half = lax.axis_index("tp").astype(jnp.int32).reshape(1)
+    plane = lax.axis_index("sp_0").astype(jnp.int32).reshape(1)
     rim = pl.pallas_call(
         rim_kernel,
-        in_specs=offchip(3),
+        in_specs=[pl.BlockSpec(memory_space=pltpu.SMEM)] * 2 + offchip(3),
         out_specs=onchip(1)[0],
         out_shape=shape((8, chans + 2 * vecs), BF16),
         scratch_shapes=[pltpu.SemaphoreType.DMA((3,))],
         compiler_params=room(2),
         name="rim",
-    )(*stay(head_input_signal, write_input_vectors, read_input_vectors))
+    )(half, plane, *stay(head_input_signal, write_input_vectors, read_input_vectors))
     rim = lax.ppermute(rim, SP, [(i, i + 1) for i in range(devices - 1)])
     signal, write_rows, read_rows, cum, cum_rows, dtv, first, second, begin, taps = pl.pallas_call(
         front_kernel,
@@ -542,10 +544,9 @@
         out_shape=shape((STATE, chans), BF16),
         compiler_params=room(6),
         name="planes",
-    )(lax.axis_index("sp_0").astype(jnp.int32).reshape(1), pin, pdec, lower)
+    )(plane, pin, pdec, lower)
     incoming = lax.all_to_all(back, PLANE, split_axis=0, concat_axis=0, tiled=True)
 
-    half = lax.axis_index("tp").astype(jnp.int32).reshape(1)
     other, mine, projection = pl.pallas_call(
         project_kernel,
         in_specs=[pl.BlockSpec(memory_space=pltpu.SMEM)] + onchip(4) + offchip(3),

time: 159 us -> 158 us (level)
  blocking collectives: 58.8 us -> 68.6 us
  starting transfers between devices: 22.1 us -> 17.1 us
  waiting for transfers between devices: 43.1 us -> 38.3 us
    all_to_all x0 -> x1, blocking collectives: none -> 9.75 us  [on_device(): lax.all_to_all(total, 'sp_0', split_axis=0, concat_axis=0, tiled=True)]
    all_to_all x1 -> x0, starting transfers between devices: 5.03 us -> none  [on_device(): lax.all_to_all(total, 'sp_0', split_axis=0, concat_axis=0, tiled=True)]
    all_to_all x1 -> x0, waiting for transfers between devices: 4.91 us -> none  [on_device(): lax.all_to_all(total, 'sp_0', split_axis=0, concat_axis=0, tiled=True)]
  transfers between devices with their start and end apart: 5 -> 4, of which waited for: 3 -> 2; matrix products, arithmetic and copies ran while one was open for 0% -> 0% of each run, Pallas kernels for 9% -> 9%
where the time goes in v5:
time: 158 us
  blocking collectives  68.6 us (43%)
  waiting for transfers between devices  38.3 us (24%)
  Pallas kernels  31.2 us (20%)
  starting transfers between devices  17.1 us (11%)
  local copies, waits for them, and re-layouts  2.12 us (1%)
    all_to_all x1, blocking collectives, on_device(): lax.all_to_all(outgoing, SP_TP, split_axis=0, concat_axis=0, tiled=True)  44.8 us
    all_to_all x1, waiting for transfers between devices, on_device(): lax.all_to_all(served, SP_TP, split_axis=0, concat_axis=0, tiled=True)  32.7 us
    all_to_all x1, blocking collectives, on_device(): got = lax.all_to_all(send, PLANE, split_axis=0, concat_axis=0, tiled=True)  14.1 us
    all_to_all x1, blocking collectives, on_device(): lax.all_to_all(total, 'sp_0', split_axis=0, concat_axis=0, tiled=True)  9.75 us
    pallas_call x1, Pallas kernels, on_device(): pl.pallas_call(expert_kernel, in_specs=onchip(4), out_specs=offchip(1)[0]...  7.29 us
    pallas_call x1, Pallas kernels, on_device(): pl.pallas_call(shared_kernel, grid=(hidden // part,), in_specs=[whole((ro...  6.84 us
    all_to_all x1, waiting for transfers between devices, on_device(): lax.all_to_all(back, PLANE, split_axis=0, concat_axis=0, tiled=True)  5.57 us
    ppermute x1, starting transfers between devices, on_device(): partner = lax.ppermute(other, 'tp', [(0, 1), (1, 0)])  4.96 us
  transfers between devices with their start and end apart: 4, of which 2 were waited for; matrix products, arithmetic and copies ran while one was open for 0% of the time, Pallas kernels for 9%

profile of v5, /device:TPU:1, one launch (start us, length us, event | category | flops | bytes accessed | tf_op | source)
XLA Modules:
  0.0 157.6 jit_solution(8439289784291498137)
XLA Ops:
  0.0 0.7 rim.1
  0.8 3.9 %collective-permute-start = (bf16[8,1536]{1,0:T(8,128)(2,1)S(1)}, bf16[8,1536]{1,0:T(8,128)(2,1)S(1)}, u32[]{:S(2)}, u32[]{:S(2)}) collective-permute-start(bf16[8,1536]{1,0:T(8,128)(2,1)S(1)} %rim.1), channel_id=1, source_target_pairs={{0,2},{2,4},{4,6},{6,8},{8,10},{10,12},{12,14},{14,16},{16,18},{18... | collective-permute-start | bytes 73736 | tf_op jit(solution)/shard_map/ppermute | solution.py:480
  4.7 3.6 %front.1 = (f32[256,1024]{1,0:T(8,128)S(1)}, bf16[256,256]{1,0:T(8,128)(2,1)S(1)}, bf16[256,256]{1,0:T(8,128)(2,1)S(1)}, f32[256,128]{1,0:T(8,128)S(1)}, f32[16,...) custom-call(bf16[256,1024]{1,0:T(8,128)(2,1)} %x_hbm.1, ...), custom_call_target="tpu_custom_call" | custom-call | flops 800000000 | bytes 4000000 | tf_op jit(solution)/shard_map/front/pallas_call | solution.py:481
  8.3 0.0 copy-start.9
  8.4 0.5 head.1
  8.9 14.1 %all_to_all.55 = bf16[16,8,1152]{2,1,0:T(8,128)(2,1)S(1)} all-to-all(bf16[16,8,1152]{2,1,0:T(8,128)(2,1)S(1)} %bitcast.33), channel_id=1, replica_groups=mesh['sp_0'=4,'sp_1'=4,'sp_2'=4,'tp'=2] {'sp_1','sp_2'}, dimensions={0} | all-to-all | bytes 589824 | tf_op jit(solution)/shard_map/all_to_all | solution.py:518
  22.9 0.3 plane.1
  23.2 9.8 %all_to_all.56 = f32[4,8,1152]{2,1,0:T(8,128)S(1)} all-to-all(f32[4,8,1152]{2,1,0:T(8,128)S(1)} %bitcast.34), channel_id=1, replica_groups=mesh['sp_0'=4,'sp_1'=4,'sp_2'=4,'tp'=2] {'sp_0'}, dimensions={0} | all-to-all | bytes 294912 | tf_op jit(solution)/shard_map/all_to_all | solution.py:539
  32.9 1.0 planes.1
  33.9 3.5 %all-to-all-start.2 = ((bf16[16,8,1024]{2,1,0:T(8,128)(2,1)}), bf16[16,8,1024]{2,1,0:T(8,128)(2,1)S(1)}, u32[]{:S(2)}, u32[]{:S(2)}) async-start(bf16[16,8,1024]{2,1,0:T(8,128)(2,1)} %bitcast.12), calls=%async_computation.2 | async-start | bytes 524288 | tf_op jit(solution)/shard_map/all_to_all | solution.py:548
  37.5 1.9 %near.1 = (f32[256,1024]{1,0:T(8,128)S(1)}, bf16[1024,512]{1,0:T(8,128)(2,1)}) custom-call(f32[256,1024]{1,0:T(8,128)S(1)} %get-tuple-element.45.sig_ref, bf16[256,256]{1,0:T(8,128)(2,1)S(1)} %get-tuple-element.46.wv_ref, bf16[256,256]{1,0:T(8,128)(2,1)S(1)} %get-tuple-element.47.rv_ref, f32[256,128]{1,0:T(8,128)S(1)} %get-tuple-element.41.cum_ref, ...), custom_call_target="tpu_custom_call" | custom-call | flops 400000000 | bytes 4000000 | tf_op jit(solution)/shard_map/near/pallas_call | solution.py:520
  39.4 5.6 %all-to-all-done.2 = bf16[16,8,1024]{2,1,0:T(8,128)(2,1)S(1)} async-done(((bf16[16,8,1024]{2,1,0:T(8,128)(2,1)}), bf16[16,8,1024]{2,1,0:T(8,128)(2,1)S(1)}, u32[]{:S(2)}, u32[]{:S(2)}) %all-to-all-start.2) | async-done | bytes 262176 | tf_op jit(solution)/shard_map/all_to_all | solution.py:548
  45.0 2.9 %project.1 = (bf16[128,2048]{1,0:T(8,128)(2,1)S(1)}, bf16[128,1024]{1,0:T(8,128)(2,1)S(1)}, bf16[1024,2048]{1,0:T(8,128)(2,1)S(1)}) custom-call(s32[1]{0:T(128)} %bitcast.half_ref, f32[256,1024]{1,0:T(8,128)S(1)} %get-tuple-element.50.y_ref, bf16[128,1024]{1,0:T(8,128)(2,1)S(1)} %bitcast.31, bf16[256,256]{1,0:T(8,128)(2,1)S(1)} %get-tuple-element.47.rv_ref, ...), custom_call_target="tpu_custom_call" | custom-call | tf_op jit(solution)/shard_map/project/pallas_call | solution.py:550
  47.9 5.0 %collective-permute-start.1 = (bf16[128,2048]{1,0:T(8,128)(2,1)S(1)}, bf16[128,2048]{1,0:T(8,128)(2,1)S(1)}, u32[]{:S(2)}, u32[]{:S(2)}) collective-permute-start(bf16[128,2048]{1,0:T(8,128)(2,1)S(1)} %get-tuple-element.59), channel_id=1, source_target_pairs={{0,1},{1,0},{2,3},{3,2},{4,5},{5,4},{6,7},{7,6},{8,9},{9,8},{10,11... | collective-permute-start | bytes 1572872 | tf_op jit(solution)/shard_map/ppermute | solution.py:562
  52.9 1.8 %own.1 = (f32[128,2048]{1,0:T(8,128)S(1)}, bf16[1024,512]{1,0:T(8,128)(2,1)S(1)}, f32[1,2048]{1,0:T(1,128)S(1)}) custom-call(bf16[128,1024]{1,0:T(8,128)(2,1)S(1)} %get-tuple-element.55.mine_ref, bf16[1024,2048]{1,0:T(8,128)(2,1)S(1)} %get-tuple-element.56.w_ref, bf16[128,2048]{1,0:T(8,128)(2,1)} %stream_hbm.1, ...), custom_call_target="tpu_custom_call" | custom-call | flops 600000000 | bytes 6000000 | tf_op jit(solution)/shard_map/own/pallas_call | solution.py:563
  54.7 1.3 dispatch.1
  56.0 44.8 %all_to_all.57 = bf16[128,8,1536]{2,1,0:T(8,128)(2,1)S(1)} all-to-all(bf16[128,8,1536]{2,1,0:T(8,128)(2,1)S(1)} %bitcast.26), channel_id=1, replica_groups=mesh['sp_0'=4,'sp_1'=4,'sp_2'=4,'tp'=2] {'sp_0','sp_1','sp_2','tp'}, dimensions={0} | all-to-all | bytes 6291456 | tf_op jit(solution)/shard_map/all_to_all | solution.py:582
  100.8 7.3 %experts.1 = bf16[1024,1536]{1,0:T(8,128)(2,1)} custom-call(bf16[1024,1536]{1,0:T(8,128)(2,1)S(1)} %bitcast.25, bf16[2048,512]{1,0:T(8,128)(2,1)S(1)} %bitcast.27, bf16[2048,512]{1,0:T(8,128)(2,1)S(1)} %bitcast.28, bf16[512,2048]{1,0:T(8,128)(2,1)S(1)} %bitcast.29), custom_call_target="tpu_custom_call" | custom-call | tf_op jit(solution)/shard_map/experts/pallas_call | solution.py:603
  108.1 4.7 %all-to-all-start.4 = ((bf16[128,8,1536]{2,1,0:T(8,128)(2,1)}), bf16[128,8,1536]{2,1,0:T(8,128)(2,1)S(1)}, u32[]{:S(2)}, u32[]{:S(2)}) async-start(bf16[128,8,1536]{2,1,0:T(8,128)(2,1)} %bitcast.39), calls=%async_computation.4 | async-start | bytes 6291456 | tf_op jit(solution)/shard_map/all_to_all | solution.py:612
  112.8 1.0 copy-done.4
  113.9 1.0 copy-done.6
  114.9 6.8 %shared.1 = (f32[128,2048]{1,0:T(8,128)}, bf16[512,1024]{1,0:T(8,128)(2,1)}) custom-call(bf16[128,2048]{1,0:T(8,128)(2,1)S(1)} %copy-done.6, bf16[128,2048]{1,0:T(8,128)(2,1)S(1)} %copy-done.4, bf16[2048,512]{1,0:T(8,128)(2,1)} %gate_ref.1, bf16[2048,512]{1,0:T(8,128)(2,1)} %up_ref.1, bf16[512,2048]{1,0:T(8,128)(2,1)} %down_ref.1, s32[4,128]{1,0:T(4,128)S(1)} %bitcast.36, ...), custom_call_target="tpu_custom_call" | custom-call | flops 800000000 | bytes 8000000 | tf_op jit(solution)/shard_map/shared/pallas_call | solution.py:586
  121.7 32.7 %all-to-all-done.4 = bf16[128,8,1536]{2,1,0:T(8,128)(2,1)S(1)} async-done(((bf16[128,8,1536]{2,1,0:T(8,128)(2,1)}), bf16[128,8,1536]{2,1,0:T(8,128)(2,1)S(1)}, u32[]{:S(2)}, u32[]{:S(2)}) %all-to-all-start.4) | async-done | bytes 3145760 | tf_op jit(solution)/shard_map/all_to_all | solution.py:612
  154.4 3.1 %combine.1 = bf16[128,2048]{1,0:T(8,128)(2,1)} custom-call(bf16[1024,1536]{1,0:T(8,128)(2,1)S(1)} %bitcast.24, f32[128,2048]{1,0:T(8,128)} %get-tuple-element.65.base_hbm, bf16[512,1024]{1,0:T(8,128)(2,1)} %get-tuple-element.66.mats_hbm), custom_call_target="tpu_custom_call" | custom-call | tf_op jit(solution)/shard_map/combine/pallas_call | solution.py:614
  (19 shorter events, 0.1 us)
Async XLA Ops:
  0.8 7.6 %collective-permute-start = (bf16[8,1536]{1,0:T(8,128)(2,1)S(1)}, bf16[8,1536]{1,0:T(8,128)(2,1)S(1)}, u32[]{:S(2)}, u32[]{:S(2)}) collective-permute-start(bf16[8,1536]{1,0:T(8,128)(2,1)S(1)} %rim.1), channel_id=1, source_target_pairs={{0,2},{2,4},{4,6},{6,8},{8,10},{10,12},{12,14},{14,16},{16,18},{18... | collective-permute-start | bytes 73736 | tf_op jit(solution)/shard_map/ppermute | solution.py:480
  8.3 29.2 %copy-start.7 = (s32[128,4]{0,1:T(4,128)S(1)}, s32[128,4]{0,1:T(4,128)}, u32[]{:S(2)}) copy-start(s32[128,4]{0,1:T(4,128)} %param.40) | copy-start | bytes 6148
  8.3 29.2 %copy-start.9 = (f32[16]{0:T(128)S(1)}, f32[16]{0:T(128)}, u32[]{:S(2)}) copy-start(f32[16]{0:T(128)} %param.36) | copy-start | bytes 196
  33.9 11.0 %all-to-all-start.2 = ((bf16[16,8,1024]{2,1,0:T(8,128)(2,1)}), bf16[16,8,1024]{2,1,0:T(8,128)(2,1)S(1)}, u32[]{:S(2)}, u32[]{:S(2)}) async-start(bf16[16,8,1024]{2,1,0:T(8,128)(2,1)} %bitcast.12), calls=%async_computation.2 | async-start | bytes 524288 | tf_op jit(solution)/shard_map/all_to_all | solution.py:548
  47.9 6.8 %collective-permute-start.1 = (bf16[128,2048]{1,0:T(8,128)(2,1)S(1)}, bf16[128,2048]{1,0:T(8,128)(2,1)S(1)}, u32[]{:S(2)}, u32[]{:S(2)}) collective-permute-start(bf16[128,2048]{1,0:T(8,128)(2,1)S(1)} %get-tuple-element.59), channel_id=1, source_target_pairs={{0,1},{1,0},{2,3},{3,2},{4,5},{5,4},{6,7},{7,6},{8,9},{9,8},{10,11... | collective-permute-start | bytes 1572872 | tf_op jit(solution)/shard_map/ppermute | solution.py:562
  56.0 44.8 %copy-start.3 = (bf16[128,2048]{1,0:T(8,128)(2,1)}, bf16[128,2048]{1,0:T(8,128)(2,1)S(1)}, u32[]{:S(2)}) copy-start(bf16[128,2048]{1,0:T(8,128)(2,1)S(1)} %get-tuple-element.64.residual_ref) | copy-start | bytes 1572868
  56.0 44.8 %copy-start.5 = (bf16[128,2048]{1,0:T(8,128)(2,1)}, bf16[128,2048]{1,0:T(8,128)(2,1)S(1)}, u32[]{:S(2)}) copy-start(bf16[128,2048]{1,0:T(8,128)(2,1)S(1)} %get-tuple-element.63.normed_ref) | copy-start | bytes 1572868
  56.0 44.8 %copy-start = (bf16[1,2048,512]{2,1,0:T(8,128)(2,1)S(1)}, bf16[1,2048,512]{2,1,0:T(8,128)(2,1)}, u32[]{:S(2)}) copy-start(bf16[1,2048,512]{2,1,0:T(8,128)(2,1)} %param.42) | copy-start | bytes 6291460
  56.0 44.8 %copy-start.1 = (bf16[1,2048,512]{2,1,0:T(8,128)(2,1)S(1)}, bf16[1,2048,512]{2,1,0:T(8,128)(2,1)}, u32[]{:S(2)}) copy-start(bf16[1,2048,512]{2,1,0:T(8,128)(2,1)} %param.43) | copy-start | bytes 6291460
  56.0 44.8 %copy-start.2 = (bf16[1,512,2048]{2,1,0:T(8,128)(2,1)S(1)}, bf16[1,512,2048]{2,1,0:T(8,128)(2,1)}, u32[]{:S(2)}) copy-start(bf16[1,512,2048]{2,1,0:T(8,128)(2,1)} %param.44) | copy-start | bytes 6291460
  108.1 4.7 %copy-start.8 = (f32[128,4]{0,1:T(4,128)S(1)}, f32[128,4]{0,1:T(4,128)}, u32[]{:S(2)}) copy-start(f32[128,4]{0,1:T(4,128)} %param.41) | copy-start | bytes 6148
  108.1 46.3 %all-to-all-start.4 = ((bf16[128,8,1536]{2,1,0:T(8,128)(2,1)}), bf16[128,8,1536]{2,1,0:T(8,128)(2,1)S(1)}, u32[]{:S(2)}, u32[]{:S(2)}) async-start(bf16[128,8,1536]{2,1,0:T(8,128)(2,1)} %bitcast.39), calls=%async_computation.4 | async-start | bytes 6291456 | tf_op jit(solution)/shard_map/all_to_all | solution.py:612
  112.8 1.0 copy-start.4
  113.8 1.0 copy-start.6
